TPU v7x, 32 devices: a whole 2x2x4 slice. The times are simulated.
32 devices in a mesh: grp: 2 (over y), sp: 4 (over z), tp: 4 (over x, core).
Axes of the slice: x: 2, y: 2, z: 4, core: 2. Of those that a mesh axis runs over, the one named last changes fastest.
Arguments:
- tokens: bfloat16 [4096, 4096], P(('grp', 'sp', 'tp')), parts along dimension 0, may hold values from -6 to 6
- norm_gain: float32 [4096], replicated, may hold values from 0.1 to 1.9
- query_diff: bfloat16 [4096, 2048], P('sp', 'tp'), may hold values from -1.25 to 1.25
- key_diff: bfloat16 [4096, 2048], P('sp', 'tp'), may hold values from -1.25 to 1.25
- value_diff: bfloat16 [4096, 2048], P('sp', 'tp'), may hold values from -0.09375 to 0.09375
- lam: float32 [8], P('tp'), may hold values from 0.3 to 0.8
- output_norm_gain: float32 [256], replicated, may hold values from 0.1 to 1.9
- query_win: bfloat16 [4096, 2048], P('sp', 'tp'), may hold values from -1.25 to 1.25
- keyval_win: bfloat16 [4, 4096, 256], P(None, 'sp'), may hold values from -1.25 to 1.25
- sink: float32 [16], P('tp'), may hold values from 4 to 7
- proj_diff: bfloat16 [2048, 4096], P('tp'), may hold values from -0.125 to 0.125
- proj_win: bfloat16 [2048, 4096], P('tp'), may hold values from -0.79296875 to 0.79296875
Outputs:
- mixed: bfloat16 [4096, 4096], P(('grp', 'sp', 'tp')), parts along dimension 0
There are 2 independent parts, one for each index of `grp`. A program takes and returns all parts, laid end to end along the dimension named above; an argument that names none is the same for every part. Nothing has to cross between parts.
All inputs are finite; a program needn't handle non-finite values.
Results may differ from a plain program's by a relative error of at most 0.015.
Values may be sent and summed in bfloat16 or wider, within the bound.
No kernel may reach another device: no remote copies, remote signals or barrier semaphores. Data moves between devices by JAX's collectives and lax.ppermute only.
A program may use at most 128 MiB of HBM per device.

v0:
```python
import math

import jax
import jax.numpy as jnp
from jax import lax
from jax.experimental import pallas as pl
from jax.experimental.pallas import tpu as pltpu
from jax.sharding import PartitionSpec as P


HEAD = 128
WIN_HEADS = 16
KV_HEADS = 4
WINDOW = 128
VDIM = 256
EPS = 1e-06
AXES = ("grp", "sp", "tp")

BF = jnp.bfloat16
F32 = jnp.float32


def padded_2(x, sides, width):
    for axis, dim in sides:
        devices, length = (lax.axis_size(axis), x.shape[dim])
        up = [(i, (i + 1) % devices) for i in range(devices - 1)]
        down = [(j, i) for i, j in up]
        last = lax.slice_in_dim(x, length - width, length, axis=dim)
        first = lax.slice_in_dim(x, 0, width, axis=dim)
        before = lax.ppermute(last, axis, up)
        after = lax.ppermute(first, axis, down)
        x = jnp.concatenate([before, x, after], axis=dim)
    return x


def root_mean_square_rows(values, gain):
    return values * lax.rsqrt(jnp.mean(values * values, axis=-1, keepdims=True) + EPS) * gain


def general_body(
    tokens,
    norm_gain,
    query_diff,
    key_diff,
    value_diff,
    lam,
    output_norm_gain,
    query_win,
    keyval_win,
    sink,
    proj_diff,
    proj_win,
):
    normed = root_mean_square_rows(tokens.astype(jnp.float32), norm_gain).astype(jnp.bfloat16)
    heads_diff = lam.shape[0]
    heads_win = sink.shape[0]
    group = WIN_HEADS // KV_HEADS
    kv_index = lax.axis_index("tp") * heads_win // group
    kv_local = lax.dynamic_index_in_dim(keyval_win, kv_index, 0, keepdims=False)
    pieces = [query_diff, key_diff, value_diff, query_win, kv_local]
    stacked = jnp.concatenate(pieces, axis=1)
    whole = lax.all_gather(stacked, "sp", axis=0, tiled=True)
    projected = jnp.dot(
        lax.all_gather(normed, "tp", axis=0, tiled=True), whole, preferred_element_type=jnp.float32
    )
    projected = projected.astype(jnp.bfloat16)
    output_list = []
    offset = 0
    for piece in pieces:
        output_list.append(projected[:, offset : offset + piece.shape[1]])
        offset = offset + piece.shape[1]
    q_diff, k_diff, v_diff, q_win, kv_win = output_list
    tok = projected.shape[0]
    scale = HEAD ** (-0.5)
    q_four = q_diff.reshape(tok, heads_diff, 2, HEAD)
    start_state = (
        jnp.full((heads_diff, 2, tok), -jnp.inf, jnp.float32),
        jnp.zeros((heads_diff, 2, tok), jnp.float32),
        jnp.zeros((heads_diff, 2, tok, VDIM), jnp.float32),
    )
    carry = start_state
    keys = lax.all_gather(k_diff, "sp", axis=0, tiled=True)
    values = lax.all_gather(v_diff, "sp", axis=0, tiled=True)
    rows = keys.shape[0]
    step = math.gcd(rows, 1024)
    key_blocks = keys.reshape(rows // step, step, heads_diff, 2, HEAD)
    value_blocks = values.reshape(rows // step, step, heads_diff, VDIM)

    def one(state, block):
        top, total, acc = state
        key_part, value_part = block
        scores = (
            jnp.einsum("qhmd,khmd->hmqk", q_four, key_part, preferred_element_type=jnp.float32)
            * scale
        )
        new_top = jnp.maximum(top, jnp.max(scores, axis=-1))
        expo = jnp.exp(scores - new_top[..., None])
        fade = jnp.exp(top - new_top)
        total = total * fade + jnp.sum(expo, axis=-1)
        acc = acc * fade[..., None] + jnp.einsum(
            "hmqk,khe->hmqe",
            expo.astype(jnp.bfloat16),
            value_part,
            preferred_element_type=jnp.float32,
        )
        return ((new_top, total, acc), None)

    carry, _ = lax.scan(one, carry, (key_blocks, value_blocks))
    _, total, acc = carry
    attention_maps = acc / total[..., None]
    difference_output = attention_maps[:, 0] - lam[:, None, None] * attention_maps[:, 1]
    differential_output = root_mean_square_rows(difference_output, output_norm_gain).astype(
        jnp.bfloat16
    )
    differential_output = jnp.transpose(differential_output, (1, 0, 2)).reshape(
        tok, heads_diff * VDIM
    )
    padded = padded_2(kv_win, (("sp", 0),), WINDOW)
    nblocks = tok // WINDOW
    blocks = padded.reshape(nblocks + 2, WINDOW, 2 * HEAD)
    band = jnp.concatenate([blocks[:-2], blocks[1:-1], blocks[2:]], axis=1)
    q_blocks = q_win.reshape(nblocks, WINDOW, heads_win, HEAD)
    scores = (
        jnp.einsum("nqhd,nkd->nhqk", q_blocks, band[..., :HEAD], preferred_element_type=jnp.float32)
        * scale
    )
    q_index = jnp.arange(WINDOW)
    k_index = jnp.arange(3 * WINDOW)
    relative = k_index[None, :] - WINDOW - q_index[:, None]
    first_key = lax.axis_index("sp") * tok - WINDOW
    key_pos = first_key + jnp.arange(nblocks)[:, None] * WINDOW + k_index[None, :]
    inside = (key_pos >= 0) & (key_pos < tok * lax.axis_size("sp"))
    valid = (jnp.abs(relative) <= WINDOW)[None] & inside[:, None, :]
    scores = jnp.where(valid[:, None], scores, -jnp.inf)
    sink_logit = sink[None, :, None, None]
    top_win = jnp.maximum(jnp.max(scores, axis=-1, keepdims=True), sink_logit)
    expo = jnp.exp(scores - top_win)
    weights = expo / (jnp.sum(expo, axis=-1, keepdims=True) + jnp.exp(sink_logit - top_win))
    y_win = jnp.einsum(
        "nhqk,nkd->nqhd",
        weights.astype(jnp.bfloat16),
        band[..., HEAD:],
        preferred_element_type=jnp.float32,
    ).astype(jnp.bfloat16)
    y_win = y_win.reshape(tok, heads_win * HEAD)
    summed = jnp.dot(differential_output, proj_diff, preferred_element_type=jnp.float32)
    return lax.psum_scatter(
        (summed + jnp.dot(y_win, proj_win, preferred_element_type=jnp.float32)).astype(
            jnp.bfloat16
        ),
        "tp",
        scatter_dimension=0,
        tiled=True,
    )


def attention_kernel(
    place, lam, sink, gain, q_ref, own_ref, oth_ref, out_ref, *, nx, flip, scale, blocks
):
    step = pl.program_id(0)
    s, x, c = place[0], place[1], place[2]
    rows = own_ref.shape[0]
    nt = (((1,), (1,)), ((), ()))
    maps = []
    for m in range(2):
        lanes = slice(m * HEAD, (m + 1) * HEAD)
        q = q_ref[:, lanes]
        sa = lax.dot_general(q, own_ref[:, lanes], nt, preferred_element_type=F32) * scale
        sb = lax.dot_general(q, oth_ref[:, lanes], nt, preferred_element_type=F32) * scale
        top = jnp.maximum(
            jnp.max(sa, axis=-1, keepdims=True), jnp.max(sb, axis=-1, keepdims=True)
        )
        ea = jnp.exp(sa - top)
        eb = jnp.exp(sb - top)
        total = jnp.sum(ea, axis=-1, keepdims=True) + jnp.sum(eb, axis=-1, keepdims=True)
        acc = jnp.dot(ea.astype(BF), own_ref[:, 256:512], preferred_element_type=F32)
        acc = acc + jnp.dot(eb.astype(BF), oth_ref[:, 256:512], preferred_element_type=F32)
        maps.append(acc / total)
    d = maps[0] - lam[0] * maps[1]
    y = d * lax.rsqrt(jnp.mean(d * d, axis=-1, keepdims=True) + EPS) * gain[...]
    out_ref[:, 0:VDIM] = y.astype(BF)

    def row_of(i):
        return ((i % nx) ^ x) * (rows // nx) + ((i // nx) ^ s) * WINDOW

    last = rows // WINDOW - 1
    kw = slice(512, 512 + HEAD)
    vw = slice(512 + HEAD, 512 + 2 * HEAD)
    q_at = lax.broadcasted_iota(jnp.int32, (WINDOW, WINDOW), 0)
    k_at = lax.broadcasted_iota(jnp.int32, (WINDOW, WINDOW), 1)
    for block in range(blocks):
        slot = step * blocks + block
        here = slice(block * WINDOW, (block + 1) * WINDOW)
        i = (slot ^ s) * nx + (x ^ flip)
        before = i - 1 + c
        after = i + c
        r_own = pl.multiple_of(row_of(i), WINDOW)
        r_bef = pl.multiple_of(row_of(jnp.maximum(before, 0)), WINDOW)
        r_aft = pl.multiple_of(row_of(jnp.minimum(after, last)), WINDOW)
        k0 = oth_ref[pl.ds(r_bef, WINDOW), kw]
        k1 = own_ref[pl.ds(r_own, WINDOW), kw]
        k2 = oth_ref[pl.ds(r_aft, WINDOW), kw]
        v0 = oth_ref[pl.ds(r_bef, WINDOW), vw]
        v1 = own_ref[pl.ds(r_own, WINDOW), vw]
        v2 = oth_ref[pl.ds(r_aft, WINDOW), vw]
        ok0 = (k_at >= q_at) & (before >= 0)
        ok2 = (k_at <= q_at) & (after <= last)
        for h in range(2):
            q = q_ref[here, 256 + h * HEAD : 256 + (h + 1) * HEAD]
            z0 = lax.dot_general(q, k0, nt, preferred_element_type=F32) * scale
            z1 = lax.dot_general(q, k1, nt, preferred_element_type=F32) * scale
            z2 = lax.dot_general(q, k2, nt, preferred_element_type=F32) * scale
            z0 = jnp.where(ok0, z0, -jnp.inf)
            z2 = jnp.where(ok2, z2, -jnp.inf)
            top = jnp.max(jnp.maximum(jnp.maximum(z0, z1), z2), axis=-1, keepdims=True)
            top = jnp.maximum(top, sink[h])
            e0, e1, e2 = jnp.exp(z0 - top), jnp.exp(z1 - top), jnp.exp(z2 - top)
            total = jnp.sum(e0 + e1 + e2, axis=-1, keepdims=True) + jnp.exp(sink[h] - top)
            w = 1.0 / total
            acc = jnp.dot((e0 * w).astype(BF), v0, preferred_element_type=F32)
            acc = acc + jnp.dot((e1 * w).astype(BF), v1, preferred_element_type=F32)
            acc = acc + jnp.dot((e2 * w).astype(BF), v2, preferred_element_type=F32)
            out_ref[here, VDIM + h * HEAD : VDIM + (h + 1) * HEAD] = acc.astype(BF)


def attention(place, lam, sink, gain, q, own, oth, sp, nx, flip, blocks=2):
    rows = own.shape[0]
    smem = pl.BlockSpec(memory_space=pltpu.SMEM)
    whole = pl.BlockSpec(own.shape, lambda i: (0, 0))
    steps = sp // blocks
    size = blocks * WINDOW

    def kernel(*refs):
        attention_kernel(*refs, nx=nx, flip=flip, scale=HEAD**-0.5, blocks=blocks)

    return pl.pallas_call(
        kernel,
        grid=(steps,),
        in_specs=[
            smem,
            smem,
            smem,
            pl.BlockSpec((1, VDIM), lambda i: (0, 0)),
            pl.BlockSpec((size, 512), lambda i: (flip * steps + i, 0)),
            whole,
            whole,
        ],
        out_specs=pl.BlockSpec((size, 512), lambda i: (i, 0)),
        out_shape=jax.ShapeDtypeStruct((sp * WINDOW, 512), BF),
        compiler_params=pltpu.CompilerParams(dimension_semantics=("arbitrary",)),
        cost_estimate=pl.CostEstimate(
            flops=4 * sp * WINDOW * rows * 2 * 384, bytes_accessed=4 * 2**20, transcendentals=0
        ),
        name="attend",
    )(place, lam, sink, gain, q, own, oth)


def project(where, acts, pieces, acc, first, count, kind):
    rows = acts.shape[0]
    size = pieces[0].shape[0]
    wide = size * len(pieces)

    def kernel(where_ref, acts_ref, *refs):
        weights, rest = refs[: len(pieces)], refs[len(pieces) :]
        total = rest[0][...] if acc is not None else None
        for j, w in enumerate(weights):
            if len(pieces) == 1:
                a = acts_ref[...]
            else:
                a = acts_ref[:, pl.ds(pl.multiple_of(where_ref[1 + j], size), size)]
            part = jnp.dot(a, w[...], preferred_element_type=F32)
            total = part if total is None else total + part
        rest[-1][...] = total.astype(kind)

    in_specs = [pl.BlockSpec((rows, wide), lambda n, at: (0, at[0]))]
    in_specs += [pl.BlockSpec((size, 256), lambda n, at: (0, n + first)) for _ in pieces]
    operands = [acts, *pieces]
    if acc is not None:
        in_specs.append(pl.BlockSpec((rows, 256), lambda n, at: (0, n + first)))
        operands.append(acc)
    return pl.pallas_call(
        kernel,
        grid_spec=pltpu.PrefetchScalarGridSpec(
            num_scalar_prefetch=1,
            grid=(count,),
            in_specs=in_specs,
            out_specs=pl.BlockSpec((rows, 256), lambda n, at: (0, n)),
        ),
        out_shape=jax.ShapeDtypeStruct((rows, count * 256), kind),
        compiler_params=pltpu.CompilerParams(dimension_semantics=("arbitrary",)),
        cost_estimate=pl.CostEstimate(
            flops=2 * rows * wide * 256 * count,
            bytes_accessed=rows * 256 * count * 8,
            transcendentals=0,
        ),
        name="project",
    )(where, *operands)


def output_projection(place, heads, weights, extra):
    sp = len(heads)
    width = weights[0].shape[1]
    tile = 512

    def kernel(place_ref, *refs):
        ys, ws, rest = refs[:sp], refs[sp : sp + 4], refs[sp + 4 :]
        ordered, out = rest[-1], rest[-2]
        s, c = place_ref[0], place_ref[2]

        @pl.when(pl.program_id(0) == 0)
        def _():
            for k, y in enumerate(ys):
                ordered[(s ^ k) ^ (2 * c)] = y[...]

        total = rest[0][...].astype(F32) if extra is not None else None
        for j, w in enumerate(ws):
            lanes = slice((j % 2) * VDIM, (j % 2 + 1) * VDIM)
            for local in range(2):
                part = jnp.dot(
                    ordered[(j // 2) * 2 + local, :, lanes],
                    w[local * VDIM : (local + 1) * VDIM],
                    preferred_element_type=F32,
                )
                total = part if total is None else total + part
        out[...] = total.astype(out.dtype)

    whole = pl.BlockSpec((WINDOW, 2 * VDIM), lambda n: (0, 0))
    column = pl.BlockSpec((WINDOW, tile), lambda n: (0, n))
    in_specs = [pl.BlockSpec(memory_space=pltpu.SMEM)] + [whole] * sp
    in_specs += [pl.BlockSpec((2 * VDIM, tile), lambda n: (0, n))] * 4
    operands = [place, *heads, *weights]
    if extra is not None:
        in_specs.append(column)
        operands.append(extra)
    return pl.pallas_call(
        kernel,
        grid=(width // tile,),
        in_specs=in_specs,
        out_specs=column,
        out_shape=jax.ShapeDtypeStruct((WINDOW, width), BF),
        scratch_shapes=[pltpu.VMEM((sp, WINDOW, 2 * VDIM), BF)],
        compiler_params=pltpu.CompilerParams(dimension_semantics=("arbitrary",)),
        cost_estimate=pl.CostEstimate(
            flops=2 * WINDOW * 2048 * width, bytes_accessed=2048 * width * 2, transcendentals=0
        ),
        name="output",
    )(*operands)


def chip_body(
    tokens,
    norm_gain,
    query_diff,
    key_diff,
    value_diff,
    lam,
    output_norm_gain,
    query_win,
    keyval_win,
    sink,
    proj_diff,
    proj_win,
):
    ng, sp, tp = (lax.axis_size(a) for a in AXES)
    nx = tp // 2
    g, s, t = (lax.axis_index(a) for a in AXES)
    x, c = t // 2, t % 2

    def send(value, target, only=None):
        pairs = []
        for i in range(ng * sp * tp):
            at = (i // (sp * tp), i // tp % sp, i % tp // 2, i % 2)
            if only is None or only(*at):
                a, b, d, e = target(*at)
                pairs.append((i, ((a * sp + b) * nx + d) * 2 + e))
        return lax.ppermute(value, AXES, pairs)

    def over_core(v):
        return send(v, lambda a, b, d, e: (a, b, d, e ^ 1))

    def over_x(v):
        return send(v, lambda a, b, d, e: (a, b, d ^ 1, e))

    def over_y(v):
        return send(v, lambda a, b, d, e: (a ^ 1, b, d, e))

    def over_z(v, k):
        return send(v, lambda a, b, d, e: (a, b ^ k, d, e))

    def mids(v, k):
        return send(v, lambda a, b, d, e: (a, b ^ k, d, e), lambda a, b, d, e: b in (1, 2))

    mid = (s == 1) | (s == 2)
    normed = root_mean_square_rows(tokens.astype(F32), norm_gain).astype(BF)
    one = over_z(normed, 1)
    near = mids(normed, 3)
    tx0 = over_x(normed)
    far = mids(near, 1)
    cross = mids(one, 3)
    tx1 = over_x(one)
    last = mids(cross, 1)
    slot2 = jnp.where(mid, cross, far)
    tx2 = over_x(slot2)
    slot3 = jnp.where(mid, near, last)
    tx3 = over_x(slot3)
    acts = jnp.concatenate([normed, one, slot2, slot3, tx0, tx1, tx2, tx3], axis=0)

    rows_w = query_diff.shape[0]
    quarter = rows_w // 4

    def pack(lo, size, head):
        parts = []
        for w in (key_diff, value_diff, query_diff, query_win):
            parts.append(lax.dynamic_slice(w, (lo, head * VDIM), (size, VDIM)))
        return jnp.concatenate(parts, axis=1)

    def kv_pack(lo, size, h):
        kv = lax.dynamic_slice(keyval_win, (nx * x + h // 2, lo, 0), (1, size, 2 * HEAD))
        return kv[0]

    def with_kv(four, kv):
        return jnp.concatenate([four[:, : 2 * VDIM], kv, four[:, 2 * VDIM :]], axis=1)

    mine_lo = (g * 2 + c) * quarter
    give_lo = (g * 2 + 1 - c) * quarter
    give = jnp.stack([pack(give_lo, quarter, 0), pack(give_lo, quarter, 1)])
    keep = jnp.stack([pack(mine_lo, quarter, 0), pack(mine_lo, quarter, 1)])
    both = jnp.concatenate([keep, over_core(give)], axis=0)
    local = pack(0, rows_w, s % 2)
    moved = send(local, lambda a, b, d, e: (a, b, d, e ^ 1), lambda a, b, d, e: e == b // 2)
    own = with_kv(jnp.where(c == s // 2, local, moved), kv_pack(0, rows_w, s))

    def chunk(k):
        h = s ^ k
        pick = lax.dynamic_index_in_dim(both, ((h // 2) ^ c) * 2 + h % 2, 0, keepdims=False)
        part = with_kv(pick, kv_pack(mine_lo, quarter, h))
        got = over_z(part, k)
        got_c = over_core(got)
        got_y = over_y(got)
        got_yc = over_core(got_y)
        return [got, got_y, got_c, got_yc]

    def offset(gg, cc):
        return (gg * 2 + cc) * quarter

    def spot(k):
        return jnp.stack(
            [s ^ k, offset(g, c), offset(1 - g, c), offset(g, 1 - c), offset(1 - g, 1 - c)]
        ).astype(jnp.int32)

    chunks = {k: chunk(k) for k in (3, 2, 1)}
    acc = project(spot(0), acts, [own], None, 0, 5, F32)
    acc = project(spot(3), acts, chunks[3], acc, 0, 5, F32)
    acc = project(spot(2), acts, chunks[2], acc, 0, 5, F32)
    kv_own = project(spot(1), acts, chunks[1], acc, 0, 3, BF)
    kv_oth = over_core(kv_own)
    queries = project(spot(1), acts, chunks[1], acc, 3, 2, BF)

    lam_both = jnp.concatenate([lam, over_core(lam)])
    sink_both = jnp.concatenate([sink, over_core(sink)])
    at = ((s // 2) ^ c) * 2 + s % 2
    lam_one = lax.dynamic_slice(lam_both, (at,), (1,))
    sink_two = lax.dynamic_slice(sink_both, (at * 2,), (2,))
    place = jnp.stack([s, x, c]).astype(jnp.int32)
    gain = output_norm_gain.reshape(1, VDIM)
    weights = [proj_diff, proj_win, over_core(proj_diff), over_core(proj_win)]

    def spread(y):
        y = y.reshape(sp, WINDOW, 2 * VDIM)
        return [y[0]] + [over_z(y[k], k) for k in range(1, sp)]

    y_far = attention(place, lam_one, sink_two, gain, queries, kv_own, kv_oth, sp, nx, 1)
    y_near = attention(place, lam_one, sink_two, gain, queries, kv_own, kv_oth, sp, nx, 0)
    part = output_projection(place, spread(y_far), weights, None)
    received = over_x(part)
    return output_projection(place, spread(y_near), weights, received)


def solution(mesh):
    placed = (
        P(("grp", "sp", "tp"), None),
        P(),
        P("sp", "tp"),
        P("sp", "tp"),
        P("sp", "tp"),
        P("tp"),
        P(),
        P("sp", "tp"),
        P(None, "sp", None),
        P("tp"),
        P("tp", None),
        P("tp", None),
    )
    sizes = dict(mesh.shape)

    def body(*args):
        tokens, lam, sink = args[0], args[5], args[9]
        fits = (
            sizes["grp"] == 2
            and sizes["sp"] == 4
            and sizes["tp"] == 4
            and tokens.shape[0] == WINDOW
            and lam.shape[0] == 2
            and sink.shape[0] == 4
        )
        return (chip_body if fits else general_body)(*args)

    return jax.shard_map(
        body, mesh=mesh, in_specs=placed, out_specs=P(("grp", "sp", "tp"), None), check_vma=False
    )
```

profile of v0, /device:TPU:0, one launch (start us, length us, event | category | flops | bytes accessed | tf_op | source)
XLA Modules:
  0.0 315.2 jit_solution(2661298795226381908)
XLA Ops:
  0.0 2.1 constant_dynamic-slice_fusion.10
  2.1 2.0 constant_dynamic-slice_fusion.8
  6.1 1.8 constant_dynamic-update-slice_fusion.7
  7.9 2.7 collective-permute-start.2
  16.9 3.1 collective-permute-start.24
  28.5 6.1 %collective-permute-done.2 = bf16[128,4096]{1,0:T(8,128)(2,1)} collective-permute-done((bf16[128,4096]{1,0:T(8,128)(2,1)}, bf16[128,4096]{1,0:T(8,128)(2,1)}, u32[]{:S(2)}, u32[]{:S(2)}) %collective-permute-start.2) | collective-permute-done | bytes 1048608 | tf_op jit(solution)/shard_map/ppermute | solution.py:376
  36.9 2.3 constant_dynamic-update-slice_fusion.6
  39.2 51.8 %collective-permute-start.16 = (bf16[256,1280]{1,0:T(8,128)(2,1)S(1)}, bf16[256,1280]{1,0:T(8,128)(2,1)S(1)}, u32[]{:S(2)}, u32[]{:S(2)}) collective-permute-start(bf16[256,1280]{1,0:T(8,128)(2,1)S(1)} %pad_maximum_fusion.5), channel_id=1, source_target_pairs={{0,8},{1,9},{2,10},{3,11},{4,12},{5,13},{6,14},{7,15},{8,0},{9,1},... | collective-permute-start | bytes 1966088 | tf_op jit(solution)/shard_map/ppermute | solution.py:376
  99.1 20.1 %collective-permute-done.16.refs_0_ = bf16[256,1280]{1,0:T(8,128)(2,1)S(1)} collective-permute-done((bf16[256,1280]{1,0:T(8,128)(2,1)S(1)}, bf16[256,1280]{1,0:T(8,128)(2,1)S(1)}, u32[]{:S(2)}, u32[]{:S(2)}) %collective-permute-start.16) | collective-permute-done | bytes 655392 | tf_op jit(solution)/shard_map/ppermute | solution.py:376
  119.3 2.1 collective-permute-done.12.refs_0_
  122.9 18.9 %collective-permute-done.6 = bf16[128,4096]{1,0:T(8,128)(2,1)S(1)} collective-permute-done((bf16[128,4096]{1,0:T(8,128)(2,1)S(1)}, bf16[128,4096]{1,0:T(8,128)(2,1)S(1)}, u32[]{:S(2)}, u32[]{:S(2)}) %collective-permute-start.6) | collective-permute-done | bytes 1048608 | tf_op jit(solution)/shard_map/ppermute | solution.py:376
  145.1 2.3 constant_dynamic-update-slice_fusion.3
  150.6 17.2 %collective-permute-done.9 = bf16[128,4096]{1,0:T(8,128)(2,1)S(1)} collective-permute-done((bf16[128,4096]{1,0:T(8,128)(2,1)S(1)}, bf16[128,4096]{1,0:T(8,128)(2,1)S(1)}, u32[]{:S(2)}, u32[]{:S(2)}) %collective-permute-start.9) | collective-permute-done | bytes 1048608 | tf_op jit(solution)/shard_map/ppermute | solution.py:376
  168.9 18.5 %collective-permute-done.10 = bf16[128,4096]{1,0:T(8,128)(2,1)S(1)} collective-permute-done((bf16[128,4096]{1,0:T(8,128)(2,1)S(1)}, bf16[128,4096]{1,0:T(8,128)(2,1)S(1)}, u32[]{:S(2)}, u32[]{:S(2)}) %collective-permute-start.10) | collective-permute-done | bytes 1048608 | tf_op jit(solution)/shard_map/ppermute | solution.py:376
  190.1 8.7 %project.5.refs_4_ = f32[1024,1280]{1,0:T(8,128)} custom-call(s32[5]{0:T(128)} %stack.98.where_ref, bf16[1024,4096]{1,0:T(8,128)(2,1)} %constant_dynamic-update-slice_fusion.acts_ref, bf16[1024,1280]{1,0:T(8,128)(2,1)} %pad_maximum_fusion.refs_0_), custom_call_target="tpu_custom_call" | custom-call | flops 2684354560 | bytes 10485760 | tf_op jit(solution)/shard_map/project/pallas_call | solution.py:281
  198.8 10.7 %project.6.refs_4_ = f32[1024,1280]{1,0:T(8,128)} custom-call(s32[5]{0:T(128)} %stack.97.where_ref, bf16[1024,4096]{1,0:T(8,128)(2,1)} %constant_dynamic-update-slice_fusion.acts_ref, bf16[256,1280]{1,0:T(8,128)(2,1)} %copy-done.9, bf16[256,1280]{1,0:T(8,128)(2,1)} %copy-done.11, bf16[256,1280]{1,0:T(8,128)(2,1)} %copy-done.12, ...), custom_call_target="tpu_custom_call" | custom-call | flops 2684354560 | bytes 10485760 | tf_op jit(solution)/shard_map/project/pallas_call | solution.py:281
  209.5 10.7 %project.7.refs_4_ = f32[1024,1280]{1,0:T(8,128)} custom-call(s32[5]{0:T(128)} %stack.95.where_ref, bf16[1024,4096]{1,0:T(8,128)(2,1)} %constant_dynamic-update-slice_fusion.acts_ref, bf16[256,1280]{1,0:T(8,128)(2,1)} %copy-done.10, bf16[256,1280]{1,0:T(8,128)(2,1)} %collective-permute-done.17.refs_1_, bf16[256,1280]{1,0:T(8,128)(2,1)} %copy-done.13, ...), custom_call_target="tpu_custom_call" | custom-call | flops 2684354560 | bytes 10485760 | tf_op jit(solution)/shard_map/project/pallas_call | solution.py:281
  221.9 7.0 %project.9.refs_5_ = bf16[1024,768]{1,0:T(8,128)(2,1)} custom-call(s32[5]{0:T(128)} %stack.88.where_ref, bf16[1024,4096]{1,0:T(8,128)(2,1)} %constant_dynamic-update-slice_fusion.acts_ref, bf16[256,1280]{1,0:T(8,128)(2,1)} %copy-done.1, bf16[256,1280]{1,0:T(8,128)(2,1)} %copy-done.2, bf16[256,1280]{1,0:T(8,128)(2,1)} %copy-done.3, ...), custom_call_target="tpu_custom_call" | custom-call | flops 1610612736 | bytes 6291456 | tf_op jit(solution)/shard_map/project/pallas_call | solution.py:281
  230.4 2.2 collective-permute-done
  233.9 5.3 %project.8.refs_4_ = bf16[1024,512]{1,0:T(8,128)(2,1)} custom-call(s32[5]{0:T(128)} %stack.88.where_ref, bf16[1024,4096]{1,0:T(8,128)(2,1)} %constant_dynamic-update-slice_fusion.acts_ref, bf16[256,1280]{1,0:T(8,128)(2,1)} %copy-done.1, bf16[256,1280]{1,0:T(8,128)(2,1)} %copy-done.2, bf16[256,1280]{1,0:T(8,128)(2,1)} %copy-done.3, ...), custom_call_target="tpu_custom_call" | custom-call | flops 1073741824 | bytes 4194304 | tf_op jit(solution)/shard_map/project/pallas_call | solution.py:281
  240.4 9.6 %attend.3 = bf16[512,512]{1,0:T(8,128)(2,1)} custom-call(s32[3]{0:T(128)} %pad_add_fusion.refs_0_.place_ref, f32[1]{0:T(128)} %dynamic_slice.88.refs_1_, f32[2]{0:T(128)} %dynamic_slice.89.refs_2_, f32[1,256]{1,0:T(1,128)} %bitcast.33, bf16[1024,512]{1,0:T(8,128)(2,1)} %project.8.refs_4_, bf16[1024,768]{1,0:T(8,128)(2,1)} %project.9.refs_5_, ...), custom_call_target="tpu_custom_call" | custom-call | flops 1610612736 | bytes 4194304 | tf_op jit(solution)/shard_map/attend/pallas_call | solution.py:236
  250.0 1.8 fusion.5
  251.8 2.9 collective-permute-start.32
  256.1 3.7 %collective-permute-done.31.refs_1_ = bf16[128,512]{1,0:T(8,128)(2,1)S(1)} collective-permute-done((bf16[128,512]{1,0:T(8,128)(2,1)S(1)}, bf16[128,512]{1,0:T(8,128)(2,1)S(1)}, u32[]{:S(2)}, u32[]{:S(2)}) %collective-permute-start.31) | collective-permute-done | bytes 131104 | tf_op jit(solution)/shard_map/ppermute | solution.py:376
  259.8 4.9 %collective-permute-done.32.refs_2_ = bf16[128,512]{1,0:T(8,128)(2,1)S(1)} collective-permute-done((bf16[128,512]{1,0:T(8,128)(2,1)S(1)}, bf16[128,512]{1,0:T(8,128)(2,1)S(1)}, u32[]{:S(2)}, u32[]{:S(2)}) %collective-permute-start.32) | collective-permute-done | bytes 131104 | tf_op jit(solution)/shard_map/ppermute | solution.py:376
  265.4 10.3 %output.2 = bf16[128,4096]{1,0:T(8,128)(2,1)} custom-call(s32[3]{0:T(128)} %pad_add_fusion.refs_0_.place_ref, bf16[128,512]{1,0:T(8,128)(2,1)} %get-tuple-element.38.refs_0_, bf16[128,512]{1,0:T(8,128)(2,1)} %copy-done.17, bf16[128,512]{1,0:T(8,128)(2,1)} %copy-done.19, bf16[128,512]{1,0:T(8,128)(2,1)} %copy-done.21, bf16[512,4096]{1,0:T(8,128)(2,1)} %refs_4_.3, ...), custom_call_target="tpu_custom_call" | custom-call | flops 2147483648 | bytes 16777216 | tf_op jit(solution)/shard_map/output/pallas_call | solution.py:335
  277.2 9.6 %attend.2 = bf16[512,512]{1,0:T(8,128)(2,1)} custom-call(s32[3]{0:T(128)} %pad_add_fusion.refs_0_.place_ref, f32[1]{0:T(128)} %dynamic_slice.88.refs_1_, f32[2]{0:T(128)} %dynamic_slice.89.refs_2_, f32[1,256]{1,0:T(1,128)} %bitcast.34, bf16[1024,512]{1,0:T(8,128)(2,1)} %project.8.refs_4_, bf16[1024,768]{1,0:T(8,128)(2,1)} %project.9.refs_5_, ...), custom_call_target="tpu_custom_call" | custom-call | flops 1610612736 | bytes 4194304 | tf_op jit(solution)/shard_map/attend/pallas_call | solution.py:236
  286.8 1.8 fusion.6
  288.6 2.7 collective-permute-start.26
  293.6 1.7 collective-permute-done.26.refs_1_
  295.3 8.1 %collective-permute-done.27.refs_2_ = bf16[128,512]{1,0:T(8,128)(2,1)S(1)} collective-permute-done((bf16[128,512]{1,0:T(8,128)(2,1)S(1)}, bf16[128,512]{1,0:T(8,128)(2,1)S(1)}, u32[]{:S(2)}, u32[]{:S(2)}) %collective-permute-start.27) | collective-permute-done | bytes 131104 | tf_op jit(solution)/shard_map/ppermute | solution.py:376
  304.6 10.6 %output.3 = bf16[128,4096]{1,0:T(8,128)(2,1)} custom-call(s32[3]{0:T(128)} %pad_add_fusion.refs_0_.place_ref, bf16[128,512]{1,0:T(8,128)(2,1)} %get-tuple-element.42.refs_0_, bf16[128,512]{1,0:T(8,128)(2,1)} %copy-done.16, bf16[128,512]{1,0:T(8,128)(2,1)} %copy-done.18, bf16[128,512]{1,0:T(8,128)(2,1)} %copy-done.20, bf16[512,4096]{1,0:T(8,128)(2,1)} %refs_4_.3, ...), custom_call_target="tpu_custom_call" | custom-call | flops 2147483648 | bytes 16777216 | tf_op jit(solution)/shard_map/output/pallas_call | solution.py:335
  (143 shorter events, 51.6 us)
Async XLA Ops:
  5.3 20.6 %collective-permute-start.11 = (bf16[2,256,1024]{2,1,0:T(8,128)(2,1)}, bf16[2,256,1024]{2,1,0:T(8,128)(2,1)}, u32[]{:S(2)}, u32[]{:S(2)}) collective-permute-start(bf16[2,256,1024]{2,1,0:T(8,128)(2,1)} %pad_maximum_fusion.3), channel_id=1, source_target_pairs={{0,1},{1,0},{2,3},{3,2},{4,5},{5,4},{6,7},{7,6},{8,9},{9,8},{10,11... | collective-permute-start | bytes 3145736 | tf_op jit(solution)/shard_map/ppermute | solution.py:376
  7.9 26.7 %collective-permute-start.2 = (bf16[128,4096]{1,0:T(8,128)(2,1)}, bf16[128,4096]{1,0:T(8,128)(2,1)}, u32[]{:S(2)}, u32[]{:S(2)}) collective-permute-start(bf16[128,4096]{1,0:T(8,128)(2,1)} %get-tuple-element.10), channel_id=1, source_target_pairs={{0,4},{1,5},{2,6},{3,7},{4,0},{5,1},{6,2},{7,3},{8,12},{9,13},{10,... | collective-permute-start | bytes 3145736 | tf_op jit(solution)/shard_map/ppermute | solution.py:376
  10.6 24.7 %collective-permute-start.4 = (bf16[128,4096]{1,0:T(8,128)(2,1)}, bf16[128,4096]{1,0:T(8,128)(2,1)S(1)}, u32[]{:S(2)}, u32[]{:S(2)}) collective-permute-start(bf16[128,4096]{1,0:T(8,128)(2,1)} %get-tuple-element.10), channel_id=1, source_target_pairs={{4,8},{5,9},{6,10},{7,11},{8,4},{9,5},{10,6},{11,7},{20,24},{21,25... | collective-permute-start | bytes 3145736 | tf_op jit(solution)/shard_map/ppermute | solution.py:376
  11.4 83.0 %collective-permute-start.7 = (bf16[128,4096]{1,0:T(8,128)(2,1)}, bf16[128,4096]{1,0:T(8,128)(2,1)}, u32[]{:S(2)}, u32[]{:S(2)}) collective-permute-start(bf16[128,4096]{1,0:T(8,128)(2,1)} %get-tuple-element.10), channel_id=1, source_target_pairs={{0,2},{1,3},{2,0},{3,1},{4,6},{5,7},{6,4},{7,5},{8,10},{9,11},{10,... | collective-permute-start | bytes 3145736 | tf_op jit(solution)/shard_map/ppermute | solution.py:376
  16.9 75.3 %collective-permute-start.24 = (bf16[1024,1024]{1,0:T(8,128)(2,1)}, bf16[1024,1024]{1,0:T(8,128)(2,1)}, u32[]{:S(2)}, u32[]{:S(2)}) collective-permute-start(bf16[1024,1024]{1,0:T(8,128)(2,1)} %pad_maximum_fusion.2), channel_id=1, source_target_pairs={{0,1},{2,3},{4,5},{6,7},{9,8},{11,10},{13,12},{15,14},{16,17},{18,... | collective-permute-start | bytes 6291464 | tf_op jit(solution)/shard_map/ppermute | solution.py:376
  27.6 70.0 %collective-permute-start.20 = (bf16[256,1280]{1,0:T(8,128)(2,1)S(1)}, bf16[256,1280]{1,0:T(8,128)(2,1)S(1)}, u32[]{:S(2)}, u32[]{:S(2)}) collective-permute-start(bf16[256,1280]{1,0:T(8,128)(2,1)S(1)} %pad_maximum_fusion.6), channel_id=1, source_target_pairs={{0,12},{1,13},{2,14},{3,15},{4,8},{5,9},{6,10},{7,11},{8,4},{9,5},... | collective-permute-start | bytes 1966088 | tf_op jit(solution)/shard_map/ppermute | solution.py:376
  35.4 55.6 %collective-permute-start.5 = (bf16[128,4096]{1,0:T(8,128)(2,1)S(1)}, bf16[128,4096]{1,0:T(8,128)(2,1)S(1)}, u32[]{:S(2)}, u32[]{:S(2)}) collective-permute-start(bf16[128,4096]{1,0:T(8,128)(2,1)S(1)} %collective-permute-done.4), channel_id=1, source_target_pairs={{4,0},{5,1},{6,2},{7,3},{8,12},{9,13},{10,14},{11,15},{20,16},{21,... | collective-permute-start | bytes 3145736 | tf_op jit(solution)/shard_map/ppermute | solution.py:376
  39.2 80.1 %collective-permute-start.16 = (bf16[256,1280]{1,0:T(8,128)(2,1)S(1)}, bf16[256,1280]{1,0:T(8,128)(2,1)S(1)}, u32[]{:S(2)}, u32[]{:S(2)}) collective-permute-start(bf16[256,1280]{1,0:T(8,128)(2,1)S(1)} %pad_maximum_fusion.5), channel_id=1, source_target_pairs={{0,8},{1,9},{2,10},{3,11},{4,12},{5,13},{6,14},{7,15},{8,0},{9,1},... | collective-permute-start | bytes 1966088 | tf_op jit(solution)/shard_map/ppermute | solution.py:376
  91.0 30.4 %collective-permute-start.12 = (bf16[256,1280]{1,0:T(8,128)(2,1)S(1)}, bf16[256,1280]{1,0:T(8,128)(2,1)S(1)}, u32[]{:S(2)}, u32[]{:S(2)}) collective-permute-start(bf16[256,1280]{1,0:T(8,128)(2,1)S(1)} %pad_maximum_fusion.4), channel_id=1, source_target_pairs={{0,4},{1,5},{2,6},{3,7},{4,0},{5,1},{6,2},{7,3},{8,12},{9,13},{10,... | collective-permute-start | bytes 1966088 | tf_op jit(solution)/shard_map/ppermute | solution.py:376
  92.3 49.5 %collective-permute-start.6 = (bf16[128,4096]{1,0:T(8,128)(2,1)S(1)}, bf16[128,4096]{1,0:T(8,128)(2,1)S(1)}, u32[]{:S(2)}, u32[]{:S(2)}) collective-permute-start(bf16[128,4096]{1,0:T(8,128)(2,1)S(1)} %collective-permute-done.3), channel_id=1, source_target_pairs={{4,0},{5,1},{6,2},{7,3},{8,12},{9,13},{10,14},{11,15},{20,16},{21,... | collective-permute-start | bytes 3145736 | tf_op jit(solution)/shard_map/ppermute | solution.py:376
  94.4 50.1 %collective-permute-start.8 = (bf16[128,4096]{1,0:T(8,128)(2,1)}, bf16[128,4096]{1,0:T(8,128)(2,1)S(1)}, u32[]{:S(2)}, u32[]{:S(2)}) collective-permute-start(bf16[128,4096]{1,0:T(8,128)(2,1)} %collective-permute-done.2), channel_id=1, source_target_pairs={{0,2},{1,3},{2,0},{3,1},{4,6},{5,7},{6,4},{7,5},{8,10},{9,11},{10,... | collective-permute-start | bytes 3145736 | tf_op jit(solution)/shard_map/ppermute | solution.py:376
  97.6 46.9 %collective-permute-start.21 = (bf16[256,1280]{1,0:T(8,128)(2,1)S(1)}, bf16[256,1280]{1,0:T(8,128)(2,1)S(1)}, u32[]{:S(2)}, u32[]{:S(2)}) collective-permute-start(bf16[256,1280]{1,0:T(8,128)(2,1)S(1)} %collective-permute-done.20.refs_0_), channel_id=1, source_target_pairs={{0,16},{1,17},{2,18},{3,19},{4,20},{5,21},{6,22},{7,23},{8,24},{9,... | collective-permute-start | bytes 1966088 | tf_op jit(solution)/shard_map/ppermute | solution.py:376
  119.3 28.2 %collective-permute-start.22 = (bf16[256,1280]{1,0:T(8,128)(2,1)S(1)}, bf16[256,1280]{1,0:T(8,128)(2,1)S(1)}, u32[]{:S(2)}, u32[]{:S(2)}) collective-permute-start(bf16[256,1280]{1,0:T(8,128)(2,1)S(1)} %collective-permute-done.20.refs_0_), channel_id=1, source_target_pairs={{0,1},{1,0},{2,3},{3,2},{4,5},{5,4},{6,7},{7,6},{8,9},{9,8},{10,11... | collective-permute-start | bytes 1966088 | tf_op jit(solution)/shard_map/ppermute | solution.py:376
  121.4 26.3 %collective-permute-start.17 = (bf16[256,1280]{1,0:T(8,128)(2,1)S(1)}, bf16[256,1280]{1,0:T(8,128)(2,1)}, u32[]{:S(2)}, u32[]{:S(2)}) collective-permute-start(bf16[256,1280]{1,0:T(8,128)(2,1)S(1)} %collective-permute-done.16.refs_0_), channel_id=1, source_target_pairs={{0,16},{1,17},{2,18},{3,19},{4,20},{5,21},{6,22},{7,23},{8,24},{9,... | collective-permute-start | bytes 1966088 | tf_op jit(solution)/shard_map/ppermute | solution.py:376
  141.8 26.0 %collective-permute-start.9 = (bf16[128,4096]{1,0:T(8,128)(2,1)S(1)}, bf16[128,4096]{1,0:T(8,128)(2,1)S(1)}, u32[]{:S(2)}, u32[]{:S(2)}) collective-permute-start(bf16[128,4096]{1,0:T(8,128)(2,1)S(1)} %get-tuple-element.8), channel_id=1, source_target_pairs={{0,2},{1,3},{2,0},{3,1},{4,6},{5,7},{6,4},{7,5},{8,10},{9,11},{10,... | collective-permute-start | bytes 3145736 | tf_op jit(solution)/shard_map/ppermute | solution.py:376
  144.5 4.6 %collective-permute-start.18 = (bf16[256,1280]{1,0:T(8,128)(2,1)S(1)}, bf16[256,1280]{1,0:T(8,128)(2,1)S(1)}, u32[]{:S(2)}, u32[]{:S(2)}) collective-permute-start(bf16[256,1280]{1,0:T(8,128)(2,1)S(1)} %collective-permute-done.16.refs_0_), channel_id=1, source_target_pairs={{0,1},{1,0},{2,3},{3,2},{4,5},{5,4},{6,7},{7,6},{8,9},{9,8},{10,11... | collective-permute-start | bytes 1966088 | tf_op jit(solution)/shard_map/ppermute | solution.py:376
  144.5 42.9 %collective-permute-start.10 = (bf16[128,4096]{1,0:T(8,128)(2,1)S(1)}, bf16[128,4096]{1,0:T(8,128)(2,1)S(1)}, u32[]{:S(2)}, u32[]{:S(2)}) collective-permute-start(bf16[128,4096]{1,0:T(8,128)(2,1)S(1)} %get-tuple-element.6), channel_id=1, source_target_pairs={{0,2},{1,3},{2,0},{3,1},{4,6},{5,7},{6,4},{7,5},{8,10},{9,11},{10,... | collective-permute-start | bytes 3145736 | tf_op jit(solution)/shard_map/ppermute | solution.py:376
  147.5 108.7 %collective-permute-start.29 = (bf16[512,4096]{1,0:T(8,128)(2,1)}, bf16[512,4096]{1,0:T(8,128)(2,1)}, u32[]{:S(2)}, u32[]{:S(2)}) collective-permute-start(bf16[512,4096]{1,0:T(8,128)(2,1)} %refs_4_.3), channel_id=1, source_target_pairs={{0,1},{1,0},{2,3},{3,2},{4,5},{5,4},{6,7},{7,6},{8,9},{9,8},{10,11... | collective-permute-start | bytes 12582920 | tf_op jit(solution)/shard_map/ppermute | solution.py:376
  147.7 108.5 %collective-permute-start.30 = (bf16[512,4096]{1,0:T(8,128)(2,1)}, bf16[512,4096]{1,0:T(8,128)(2,1)}, u32[]{:S(2)}, u32[]{:S(2)}) collective-permute-start(bf16[512,4096]{1,0:T(8,128)(2,1)} %refs_5_.3), channel_id=1, source_target_pairs={{0,1},{1,0},{2,3},{3,2},{4,5},{5,4},{6,7},{7,6},{8,9},{9,8},{10,11... | collective-permute-start | bytes 12582920 | tf_op jit(solution)/shard_map/ppermute | solution.py:376
  149.1 39.4 %collective-permute-start.13 = (bf16[256,1280]{1,0:T(8,128)(2,1)S(1)}, bf16[256,1280]{1,0:T(8,128)(2,1)S(1)}, u32[]{:S(2)}, u32[]{:S(2)}) collective-permute-start(bf16[256,1280]{1,0:T(8,128)(2,1)S(1)} %collective-permute-done.12.refs_0_), channel_id=1, source_target_pairs={{0,16},{1,17},{2,18},{3,19},{4,20},{5,21},{6,22},{7,23},{8,24},{9,... | collective-permute-start | bytes 1966088 | tf_op jit(solution)/shard_map/ppermute | solution.py:376
  167.8 21.3 %collective-permute-start.23 = (bf16[256,1280]{1,0:T(8,128)(2,1)S(1)}, bf16[256,1280]{1,0:T(8,128)(2,1)S(1)}, u32[]{:S(2)}, u32[]{:S(2)}) collective-permute-start(bf16[256,1280]{1,0:T(8,128)(2,1)S(1)} %collective-permute-done.21.refs_1_), channel_id=1, source_target_pairs={{0,1},{1,0},{2,3},{3,2},{4,5},{5,4},{6,7},{7,6},{8,9},{9,8},{10,11... | collective-permute-start | bytes 1966088 | tf_op jit(solution)/shard_map/ppermute | solution.py:376
  187.4 22.1 %collective-permute-start.19 = (bf16[256,1280]{1,0:T(8,128)(2,1)}, bf16[256,1280]{1,0:T(8,128)(2,1)}, u32[]{:S(2)}, u32[]{:S(2)}) collective-permute-start(bf16[256,1280]{1,0:T(8,128)(2,1)} %collective-permute-done.17.refs_1_), channel_id=1, source_target_pairs={{0,1},{1,0},{2,3},{3,2},{4,5},{5,4},{6,7},{7,6},{8,9},{9,8},{10,11... | collective-permute-start | bytes 1966088 | tf_op jit(solution)/shard_map/ppermute | solution.py:376
  188.5 31.6 %collective-permute-start.14 = (bf16[256,1280]{1,0:T(8,128)(2,1)S(1)}, bf16[256,1280]{1,0:T(8,128)(2,1)S(1)}, u32[]{:S(2)}, u32[]{:S(2)}) collective-permute-start(bf16[256,1280]{1,0:T(8,128)(2,1)S(1)} %collective-permute-done.12.refs_0_), channel_id=1, source_target_pairs={{0,1},{1,0},{2,3},{3,2},{4,5},{5,4},{6,7},{7,6},{8,9},{9,8},{10,11... | collective-permute-start | bytes 1966088 | tf_op jit(solution)/shard_map/ppermute | solution.py:376
  190.0 30.2 %collective-permute-start.15 = (bf16[256,1280]{1,0:T(8,128)(2,1)S(1)}, bf16[256,1280]{1,0:T(8,128)(2,1)S(1)}, u32[]{:S(2)}, u32[]{:S(2)}) collective-permute-start(bf16[256,1280]{1,0:T(8,128)(2,1)S(1)} %collective-permute-done.13.refs_1_), channel_id=1, source_target_pairs={{0,1},{1,0},{2,3},{3,2},{4,5},{5,4},{6,7},{7,6},{8,9},{9,8},{10,11... | collective-permute-start | bytes 1966088 | tf_op jit(solution)/shard_map/ppermute | solution.py:376
  228.9 10.3 %collective-permute-start.25 = (bf16[1024,768]{1,0:T(8,128)(2,1)}, bf16[1024,768]{1,0:T(8,128)(2,1)S(1)}, u32[]{:S(2)}, u32[]{:S(2)}) collective-permute-start(bf16[1024,768]{1,0:T(8,128)(2,1)} %project.9.refs_5_), channel_id=1, source_target_pairs={{0,1},{1,0},{2,3},{3,2},{4,5},{5,4},{6,7},{7,6},{8,9},{9,8},{10,11... | collective-permute-start | bytes 4718600 | tf_op jit(solution)/shard_map/ppermute | solution.py:376
  251.8 8.1 %collective-permute-start.31 = (bf16[128,512]{1,0:T(8,128)(2,1)S(1)}, bf16[128,512]{1,0:T(8,128)(2,1)S(1)}, u32[]{:S(2)}, u32[]{:S(2)}) collective-permute-start(bf16[128,512]{1,0:T(8,128)(2,1)S(1)} %get-tuple-element.37), channel_id=1, source_target_pairs={{0,4},{1,5},{2,6},{3,7},{4,0},{5,1},{6,2},{7,3},{8,12},{9,13},{10,... | collective-permute-start | bytes 393224 | tf_op jit(solution)/shard_map/ppermute | solution.py:376
  251.8 12.9 %collective-permute-start.32 = (bf16[128,512]{1,0:T(8,128)(2,1)S(1)}, bf16[128,512]{1,0:T(8,128)(2,1)S(1)}, u32[]{:S(2)}, u32[]{:S(2)}) collective-permute-start(bf16[128,512]{1,0:T(8,128)(2,1)S(1)} %get-tuple-element.36), channel_id=1, source_target_pairs={{0,8},{1,9},{2,10},{3,11},{4,12},{5,13},{6,14},{7,15},{8,0},{9,1},... | collective-permute-start | bytes 393224 | tf_op jit(solution)/shard_map/ppermute | solution.py:376
  254.6 10.1 %collective-permute-start.33 = (bf16[128,512]{1,0:T(8,128)(2,1)S(1)}, bf16[128,512]{1,0:T(8,128)(2,1)S(1)}, u32[]{:S(2)}, u32[]{:S(2)}) collective-permute-start(bf16[128,512]{1,0:T(8,128)(2,1)S(1)} %get-tuple-element.35), channel_id=1, source_target_pairs={{0,12},{1,13},{2,14},{3,15},{4,8},{5,9},{6,10},{7,11},{8,4},{9,5},... | collective-permute-start | bytes 393224 | tf_op jit(solution)/shard_map/ppermute | solution.py:376
  275.7 27.8 %collective-permute-start.34 = (bf16[128,4096]{1,0:T(8,128)(2,1)}, bf16[128,4096]{1,0:T(8,128)(2,1)S(1)}, u32[]{:S(2)}, u32[]{:S(2)}) collective-permute-start(bf16[128,4096]{1,0:T(8,128)(2,1)} %output.2), channel_id=1, source_target_pairs={{0,2},{1,3},{2,0},{3,1},{4,6},{5,7},{6,4},{7,5},{8,10},{9,11},{10,... | collective-permute-start | bytes 3145736 | tf_op jit(solution)/shard_map/ppermute | solution.py:376
  288.6 6.7 %collective-permute-start.26 = (bf16[128,512]{1,0:T(8,128)(2,1)S(1)}, bf16[128,512]{1,0:T(8,128)(2,1)S(1)}, u32[]{:S(2)}, u32[]{:S(2)}) collective-permute-start(bf16[128,512]{1,0:T(8,128)(2,1)S(1)} %get-tuple-element.41), channel_id=1, source_target_pairs={{0,4},{1,5},{2,6},{3,7},{4,0},{5,1},{6,2},{7,3},{8,12},{9,13},{10,... | collective-permute-start | bytes 393224 | tf_op jit(solution)/shard_map/ppermute | solution.py:376
  291.3 12.2 %collective-permute-start.27 = (bf16[128,512]{1,0:T(8,128)(2,1)S(1)}, bf16[128,512]{1,0:T(8,128)(2,1)S(1)}, u32[]{:S(2)}, u32[]{:S(2)}) collective-permute-start(bf16[128,512]{1,0:T(8,128)(2,1)S(1)} %get-tuple-element.40), channel_id=1, source_target_pairs={{0,8},{1,9},{2,10},{3,11},{4,12},{5,13},{6,14},{7,15},{8,0},{9,1},... | collective-permute-start | bytes 393224 | tf_op jit(solution)/shard_map/ppermute | solution.py:376
  292.1 11.4 %collective-permute-start.28 = (bf16[128,512]{1,0:T(8,128)(2,1)S(1)}, bf16[128,512]{1,0:T(8,128)(2,1)S(1)}, u32[]{:S(2)}, u32[]{:S(2)}) collective-permute-start(bf16[128,512]{1,0:T(8,128)(2,1)S(1)} %get-tuple-element.39), channel_id=1, source_target_pairs={{0,12},{1,13},{2,14},{3,15},{4,8},{5,9},{6,10},{7,11},{8,4},{9,5},... | collective-permute-start | bytes 393224 | tf_op jit(solution)/shard_map/ppermute | solution.py:376
  (29 other events, 377.2 us)
where the time goes:
time: 316 us; the launch traced here: 315 us
  waiting for transfers between devices  104 us (33%)
  starting transfers between devices  86 us (27%)
  Pallas kernels  82.4 us (26%)
  local copies, waits for them, and re-layouts  29.8 us (9%)
  other arithmetic  13.2 us (4%)
    ppermute x35, waiting for transfers between devices, send(): return lax.ppermute(value, AXES, pairs)  104 us
    ppermute x35, starting transfers between devices, send(): return lax.ppermute(value, AXES, pairs)  86 us
    pallas_call x5, Pallas kernels, project(): pl.pallas_call(kernel, grid_spec=pltpu.PrefetchScalarGridSpec(num_scalar_...  42.3 us
    pallas_call x2, Pallas kernels, output_projection(): pl.pallas_call(kernel, grid=(width // tile,), in_specs=in_specs, out_spec...  20.9 us
    pallas_call x2, Pallas kernels, attention(): pl.pallas_call(kernel, grid=(steps,), in_specs=[smem, smem, smem, pl.Bloc...  19.2 us
    unnamed x56, local copies, waits for them, and re-layouts  12.3 us
    dynamic_slice x4, local copies, waits for them, and re-layouts, pack(): parts.append(lax.dynamic_slice(w, (lo, head * VDIM), (size, VDIM)))  6.51 us
  transfers between devices with their start and end apart: 35, of which 11 were waited for; matrix products, arithmetic and copies ran while one was open for 10% of the time, Pallas kernels for 20%

commit v1 on v0

--- a/solution.py
+++ b/solution.py
@@ -14,8 +14,10 @@
 WINDOW = 128
 VDIM = 256
 EPS = 1e-06
+LOG2E = math.log2(math.e)
 AXES = ("grp", "sp", "tp")
 
+OUT_TILE = 1024
 BF = jnp.bfloat16
 F32 = jnp.float32
 
@@ -154,49 +156,64 @@
     )
 
 
+def row_of(i, s, x, nx, rows):
+    slot = (i // nx) ^ s
+    side = (i % nx) ^ x
+    early = rows // WINDOW // nx - 1
+    row = jnp.where(slot < early, side * early + slot, nx * early + side) * WINDOW
+    return pl.multiple_of(row, WINDOW)
+
+
 def attention_kernel(
-    place, lam, sink, gain, q_ref, own_ref, oth_ref, out_ref, *, nx, flip, scale, blocks
+    place, lam_a, lam_b, sink_a, sink_b, gain, q_ref, own_ref, oth_ref, *outs, nx, flip
 ):
     step = pl.program_id(0)
     s, x, c = place[0], place[1], place[2]
     rows = own_ref.shape[0]
+    blocks = 2
+    scale = HEAD**-0.5
+    swapped = ((s // 2) ^ c) == 1
+    lam = jnp.where(swapped, lam_b[s % 2], lam_a[s % 2])
+    sinks = [
+        jnp.where(swapped, sink_b[(s % 2) * 2 + h], sink_a[(s % 2) * 2 + h]) for h in range(2)
+    ]
     nt = (((1,), (1,)), ((), ()))
+    at = [((step * blocks + j) ^ s) * nx + (x ^ flip) for j in range(blocks)]
+    places = [row_of(i, s, x, nx, rows) for i in at]
+
+    def q_of(lanes):
+        return jnp.concatenate([q_ref[pl.ds(r, WINDOW), lanes] for r in places], axis=0)
+
     maps = []
     for m in range(2):
         lanes = slice(m * HEAD, (m + 1) * HEAD)
-        q = q_ref[:, lanes]
-        sa = lax.dot_general(q, own_ref[:, lanes], nt, preferred_element_type=F32) * scale
-        sb = lax.dot_general(q, oth_ref[:, lanes], nt, preferred_element_type=F32) * scale
+        q = q_of(lanes)
+        sa = lax.dot_general(q, own_ref[:, lanes], nt, preferred_element_type=F32)
+        sb = lax.dot_general(q, oth_ref[:, lanes], nt, preferred_element_type=F32)
         top = jnp.maximum(
             jnp.max(sa, axis=-1, keepdims=True), jnp.max(sb, axis=-1, keepdims=True)
         )
-        ea = jnp.exp(sa - top)
-        eb = jnp.exp(sb - top)
+        top = top * (scale * LOG2E)
+        ea = jnp.exp2(sa * (scale * LOG2E) - top)
+        eb = jnp.exp2(sb * (scale * LOG2E) - top)
         total = jnp.sum(ea, axis=-1, keepdims=True) + jnp.sum(eb, axis=-1, keepdims=True)
         acc = jnp.dot(ea.astype(BF), own_ref[:, 256:512], preferred_element_type=F32)
         acc = acc + jnp.dot(eb.astype(BF), oth_ref[:, 256:512], preferred_element_type=F32)
         maps.append(acc / total)
-    d = maps[0] - lam[0] * maps[1]
+    d = maps[0] - lam * maps[1]
     y = d * lax.rsqrt(jnp.mean(d * d, axis=-1, keepdims=True) + EPS) * gain[...]
-    out_ref[:, 0:VDIM] = y.astype(BF)
-
-    def row_of(i):
-        return ((i % nx) ^ x) * (rows // nx) + ((i // nx) ^ s) * WINDOW
-
+    y = y.astype(BF)
     last = rows // WINDOW - 1
     kw = slice(512, 512 + HEAD)
     vw = slice(512 + HEAD, 512 + 2 * HEAD)
     q_at = lax.broadcasted_iota(jnp.int32, (WINDOW, WINDOW), 0)
     k_at = lax.broadcasted_iota(jnp.int32, (WINDOW, WINDOW), 1)
-    for block in range(blocks):
-        slot = step * blocks + block
-        here = slice(block * WINDOW, (block + 1) * WINDOW)
-        i = (slot ^ s) * nx + (x ^ flip)
+    wins = []
+    for i, r_own in zip(at, places):
         before = i - 1 + c
         after = i + c
-        r_own = pl.multiple_of(row_of(i), WINDOW)
-        r_bef = pl.multiple_of(row_of(jnp.maximum(before, 0)), WINDOW)
-        r_aft = pl.multiple_of(row_of(jnp.minimum(after, last)), WINDOW)
+        r_bef = row_of(jnp.maximum(before, 0), s, x, nx, rows)
+        r_aft = row_of(jnp.minimum(after, last), s, x, nx, rows)
         k0 = oth_ref[pl.ds(r_bef, WINDOW), kw]
         k1 = own_ref[pl.ds(r_own, WINDOW), kw]
         k2 = oth_ref[pl.ds(r_aft, WINDOW), kw]
@@ -206,113 +223,206 @@
         ok0 = (k_at >= q_at) & (before >= 0)
         ok2 = (k_at <= q_at) & (after <= last)
         for h in range(2):
-            q = q_ref[here, 256 + h * HEAD : 256 + (h + 1) * HEAD]
+            q = q_ref[pl.ds(r_own, WINDOW), 256 + h * HEAD : 256 + (h + 1) * HEAD]
             z0 = lax.dot_general(q, k0, nt, preferred_element_type=F32) * scale
             z1 = lax.dot_general(q, k1, nt, preferred_element_type=F32) * scale
             z2 = lax.dot_general(q, k2, nt, preferred_element_type=F32) * scale
             z0 = jnp.where(ok0, z0, -jnp.inf)
             z2 = jnp.where(ok2, z2, -jnp.inf)
             top = jnp.max(jnp.maximum(jnp.maximum(z0, z1), z2), axis=-1, keepdims=True)
-            top = jnp.maximum(top, sink[h])
+            top = jnp.maximum(top, sinks[h])
             e0, e1, e2 = jnp.exp(z0 - top), jnp.exp(z1 - top), jnp.exp(z2 - top)
-            total = jnp.sum(e0 + e1 + e2, axis=-1, keepdims=True) + jnp.exp(sink[h] - top)
+            total = jnp.sum(e0 + e1 + e2, axis=-1, keepdims=True) + jnp.exp(sinks[h] - top)
             w = 1.0 / total
             acc = jnp.dot((e0 * w).astype(BF), v0, preferred_element_type=F32)
             acc = acc + jnp.dot((e1 * w).astype(BF), v1, preferred_element_type=F32)
             acc = acc + jnp.dot((e2 * w).astype(BF), v2, preferred_element_type=F32)
-            out_ref[here, VDIM + h * HEAD : VDIM + (h + 1) * HEAD] = acc.astype(BF)
-
-
-def attention(place, lam, sink, gain, q, own, oth, sp, nx, flip, blocks=2):
+            wins.append(acc.astype(BF))
+    for t in range(len(outs) // blocks):
+
+        @pl.when(step == t)
+        def _(t=t):
+            for j in range(blocks):
+                out = outs[t * blocks + j]
+                out[:, 0:VDIM] = y[j * WINDOW : (j + 1) * WINDOW]
+                out[:, VDIM : VDIM + HEAD] = wins[2 * j]
+                out[:, VDIM + HEAD : VDIM + 2 * HEAD] = wins[2 * j + 1]
+
+
+def attention(place, scalars, gain, q, own, oth, sp, nx, flip):
     rows = own.shape[0]
     smem = pl.BlockSpec(memory_space=pltpu.SMEM)
     whole = pl.BlockSpec(own.shape, lambda i: (0, 0))
-    steps = sp // blocks
-    size = blocks * WINDOW
+    block = pl.BlockSpec((WINDOW, 2 * VDIM), lambda i: (0, 0))
 
     def kernel(*refs):
-        attention_kernel(*refs, nx=nx, flip=flip, scale=HEAD**-0.5, blocks=blocks)
+        attention_kernel(*refs, nx=nx, flip=flip)
 
     return pl.pallas_call(
         kernel,
-        grid=(steps,),
-        in_specs=[
-            smem,
-            smem,
-            smem,
-            pl.BlockSpec((1, VDIM), lambda i: (0, 0)),
-            pl.BlockSpec((size, 512), lambda i: (flip * steps + i, 0)),
-            whole,
-            whole,
-        ],
-        out_specs=pl.BlockSpec((size, 512), lambda i: (i, 0)),
-        out_shape=jax.ShapeDtypeStruct((sp * WINDOW, 512), BF),
+        grid=(sp // 2,),
+        in_specs=[smem] * 5
+        + [pl.BlockSpec((1, VDIM), lambda i: (0, 0)), pl.BlockSpec(q.shape, lambda i: (0, 0))]
+        + [whole, whole],
+        out_specs=[block] * sp,
+        out_shape=[jax.ShapeDtypeStruct((WINDOW, 2 * VDIM), BF)] * sp,
         compiler_params=pltpu.CompilerParams(dimension_semantics=("arbitrary",)),
         cost_estimate=pl.CostEstimate(
-            flops=4 * sp * WINDOW * rows * 2 * 384, bytes_accessed=4 * 2**20, transcendentals=0
+            flops=4 * sp * WINDOW * rows * 2 * 384,
+            bytes_accessed=4 * 2**20,
+            transcendentals=0,
         ),
         name="attend",
-    )(place, lam, sink, gain, q, own, oth)
-
-
-def project(where, acts, pieces, acc, first, count, kind):
+    )(place, *scalars, gain, q, own, oth)
+
+
+def assemble(scratch, row, pieces, g, c):
+    size = pieces[0].shape[0]
+    parts = []
+    for p in pieces:
+        for lo in range(0, p.shape[0], size):
+            parts.append(p[lo : lo + size, :])
+    if len(parts) == 1:
+        scratch[row : row + size, :] = parts[0]
+        return
+    for j, part in enumerate(parts):
+        quarter = (g ^ (j & 1)) * 2 + (c ^ (j >> 1))
+        scratch[pl.ds(pl.multiple_of(row + quarter * size, size), size), :] = part
+
+
+ROWS = 256
+
+
+def project_early(place, acts, own, pieces, split):
     rows = acts.shape[0]
-    size = pieces[0].shape[0]
-    wide = size * len(pieces)
-
-    def kernel(where_ref, acts_ref, *refs):
-        weights, rest = refs[: len(pieces)], refs[len(pieces) :]
-        total = rest[0][...] if acc is not None else None
-        for j, w in enumerate(weights):
-            if len(pieces) == 1:
-                a = acts_ref[...]
-            else:
-                a = acts_ref[:, pl.ds(pl.multiple_of(where_ref[1 + j], size), size)]
-            part = jnp.dot(a, w[...], preferred_element_type=F32)
-            total = part if total is None else total + part
-        rest[-1][...] = total.astype(kind)
-
-    in_specs = [pl.BlockSpec((rows, wide), lambda n, at: (0, at[0]))]
-    in_specs += [pl.BlockSpec((size, 256), lambda n, at: (0, n + first)) for _ in pieces]
-    operands = [acts, *pieces]
-    if acc is not None:
-        in_specs.append(pl.BlockSpec((rows, 256), lambda n, at: (0, n + first)))
-        operands.append(acc)
+    wide, cols = own.shape
+
+    def kernel(place_ref, a0, a1, own_ref, *refs):
+        (*ws, left, right, scratch) = refs
+
+        @pl.when(pl.program_id(0) == 0)
+        def _():
+            assemble(scratch, 0, ws, place_ref[3], place_ref[2])
+
+        total = jnp.dot(a0[...], own_ref[...], preferred_element_type=F32)
+        total = total + jnp.dot(a1[...], scratch[...], preferred_element_type=F32)
+        left[...] = total[:, :split]
+        right[...] = total[:, split:]
+
+    def chunk_of(k):
+        return pl.BlockSpec((ROWS, wide), lambda m, at: (m, at[0] ^ k))
+
+    whole = [pl.BlockSpec(p.shape, lambda m, at: (0, 0)) for p in (own, *pieces)]
+    widths = (split, cols - split)
     return pl.pallas_call(
         kernel,
         grid_spec=pltpu.PrefetchScalarGridSpec(
             num_scalar_prefetch=1,
-            grid=(count,),
-            in_specs=in_specs,
-            out_specs=pl.BlockSpec((rows, 256), lambda n, at: (0, n)),
+            grid=(rows // ROWS,),
+            in_specs=[chunk_of(0), chunk_of(1), *whole],
+            out_specs=[pl.BlockSpec((ROWS, w), lambda m, at: (m, 0)) for w in widths],
+            scratch_shapes=[pltpu.VMEM((wide, cols), BF)],
         ),
-        out_shape=jax.ShapeDtypeStruct((rows, count * 256), kind),
+        out_shape=[jax.ShapeDtypeStruct((rows, w), F32) for w in widths],
         compiler_params=pltpu.CompilerParams(dimension_semantics=("arbitrary",)),
         cost_estimate=pl.CostEstimate(
-            flops=2 * rows * wide * 256 * count,
-            bytes_accessed=rows * 256 * count * 8,
+            flops=4 * rows * wide * cols, bytes_accessed=rows * cols * 8, transcendentals=0
+        ),
+        name="project",
+    )(place, acts, acts, own, *pieces)
+
+
+def project_rest(place, early, late, acc, chunks, begin, cols):
+    wide = sum(p.shape[0] for p in chunks[0][0])
+    steps = early.shape[0] // ROWS
+    order = sorted(chunks)
+    counts = [len(chunks[k][0]) for k in order]
+
+    def kernel(place_ref, acc_ref, e2, e3, *refs):
+        acts = refs[: len(order)]
+        refs = refs[len(order) :]
+        out, scratch = refs[-2], refs[-1]
+        m = pl.program_id(0)
+
+        @pl.when(m == 0)
+        def _():
+            at = 0
+            for j, n in enumerate(counts):
+                assemble(scratch, j * wide, refs[at : at + n], place_ref[3], place_ref[2])
+                at += n
+
+        def part(a, j):
+            return jnp.dot(
+                a[...], scratch[j * wide : (j + 1) * wide], preferred_element_type=F32
+            )
+
+        @pl.when(m < steps)
+        def _():
+            out[...] = (acc_ref[...] + part(e2, 2) + part(e3, 3)).astype(BF)
+
+        @pl.when(m == steps)
+        def _():
+            total = part(acts[0], 0)
+            for j in range(1, len(order)):
+                total = total + part(acts[j], j)
+            out[...] = total.astype(BF)
+
+    def early_of(k):
+        return pl.BlockSpec(
+            (ROWS, wide), lambda m, at: (jnp.minimum(m, steps - 1), at[0] ^ k)
+        )
+
+    in_specs = [pl.BlockSpec((ROWS, cols), lambda m, at: (jnp.minimum(m, steps - 1), 0))]
+    in_specs += [early_of(2), early_of(3)]
+    in_specs += [pl.BlockSpec((ROWS, wide), lambda m, at, k=k: (0, at[0] ^ k)) for k in order]
+    operands = [acc, early, early] + [late] * len(order)
+    for k in order:
+        pieces, start = chunks[k]
+        for p in pieces:
+            in_specs.append(
+                pl.BlockSpec(
+                    (pl.Element(p.shape[0]), pl.Element(cols)),
+                    lambda m, at, lo=begin - start: (0, lo),
+                )
+                if p.shape[1] != cols
+                else pl.BlockSpec(p.shape, lambda m, at: (0, 0))
+            )
+            operands.append(p)
+    return pl.pallas_call(
+        kernel,
+        grid_spec=pltpu.PrefetchScalarGridSpec(
+            num_scalar_prefetch=1,
+            grid=(steps + 1,),
+            in_specs=in_specs,
+            out_specs=pl.BlockSpec((ROWS, cols), lambda m, at: (m, 0)),
+            scratch_shapes=[pltpu.VMEM((len(order) * wide, cols), BF)],
+        ),
+        out_shape=jax.ShapeDtypeStruct((early.shape[0] + late.shape[0], cols), BF),
+        compiler_params=pltpu.CompilerParams(dimension_semantics=("arbitrary",)),
+        cost_estimate=pl.CostEstimate(
+            flops=2 * (2 * early.shape[0] + 4 * late.shape[0]) * wide * cols,
+            bytes_accessed=16 * 2**20,
             transcendentals=0,
         ),
         name="project",
-    )(where, *operands)
-
-
-def output_projection(place, heads, weights, extra):
+    )(place, *operands)
+
+
+def output_projection(place, heads, weights, first, count, kind):
     sp = len(heads)
-    width = weights[0].shape[1]
-    tile = 512
+    tile = OUT_TILE
 
     def kernel(place_ref, *refs):
-        ys, ws, rest = refs[:sp], refs[sp : sp + 4], refs[sp + 4 :]
-        ordered, out = rest[-1], rest[-2]
+        ys, ws, (out, ordered) = refs[:sp], refs[sp : sp + 4], refs[sp + 4 :]
         s, c = place_ref[0], place_ref[2]
-
-        @pl.when(pl.program_id(0) == 0)
+        n = pl.program_id(0)
+
+        @pl.when(n == 0)
         def _():
             for k, y in enumerate(ys):
                 ordered[(s ^ k) ^ (2 * c)] = y[...]
 
-        total = rest[0][...].astype(F32) if extra is not None else None
+        total = None
         for j, w in enumerate(ws):
             lanes = slice((j % 2) * VDIM, (j % 2 + 1) * VDIM)
             for local in range(2):
@@ -325,23 +435,21 @@
         out[...] = total.astype(out.dtype)
 
     whole = pl.BlockSpec((WINDOW, 2 * VDIM), lambda n: (0, 0))
-    column = pl.BlockSpec((WINDOW, tile), lambda n: (0, n))
     in_specs = [pl.BlockSpec(memory_space=pltpu.SMEM)] + [whole] * sp
-    in_specs += [pl.BlockSpec((2 * VDIM, tile), lambda n: (0, n))] * 4
+    in_specs += [pl.BlockSpec((2 * VDIM, tile), lambda n: (0, n + first))] * 4
     operands = [place, *heads, *weights]
-    if extra is not None:
-        in_specs.append(column)
-        operands.append(extra)
     return pl.pallas_call(
         kernel,
-        grid=(width // tile,),
+        grid=(count,),
         in_specs=in_specs,
-        out_specs=column,
-        out_shape=jax.ShapeDtypeStruct((WINDOW, width), BF),
+        out_specs=pl.BlockSpec((WINDOW, tile), lambda n: (0, n)),
+        out_shape=jax.ShapeDtypeStruct((WINDOW, count * tile), kind),
         scratch_shapes=[pltpu.VMEM((sp, WINDOW, 2 * VDIM), BF)],
         compiler_params=pltpu.CompilerParams(dimension_semantics=("arbitrary",)),
         cost_estimate=pl.CostEstimate(
-            flops=2 * WINDOW * 2048 * width, bytes_accessed=2048 * width * 2, transcendentals=0
+            flops=2 * WINDOW * 2048 * count * tile,
+            bytes_accessed=2048 * count * tile * 2,
+            transcendentals=0,
         ),
         name="output",
     )(*operands)
@@ -403,7 +511,8 @@
     tx2 = over_x(slot2)
     slot3 = jnp.where(mid, near, last)
     tx3 = over_x(slot3)
-    acts = jnp.concatenate([normed, one, slot2, slot3, tx0, tx1, tx2, tx3], axis=0)
+    early = jnp.concatenate([normed, one, slot2, tx0, tx1, tx2], axis=0)
+    late = jnp.concatenate([slot3, tx3], axis=0)
 
     rows_w = query_diff.shape[0]
     quarter = rows_w // 4
@@ -430,50 +539,52 @@
     moved = send(local, lambda a, b, d, e: (a, b, d, e ^ 1), lambda a, b, d, e: e == b // 2)
     own = with_kv(jnp.where(c == s // 2, local, moved), kv_pack(0, rows_w, s))
 
-    def chunk(k):
+    place = jnp.stack([s, x, c, g]).astype(jnp.int32)
+
+    def package(k):
         h = s ^ k
         pick = lax.dynamic_index_in_dim(both, ((h // 2) ^ c) * 2 + h % 2, 0, keepdims=False)
-        part = with_kv(pick, kv_pack(mine_lo, quarter, h))
+        return pick, kv_pack(mine_lo, quarter, h)
+
+    def chunk(part, k):
         got = over_z(part, k)
-        got_c = over_core(got)
         got_y = over_y(got)
-        got_yc = over_core(got_y)
-        return [got, got_y, got_c, got_yc]
-
-    def offset(gg, cc):
-        return (gg * 2 + cc) * quarter
-
-    def spot(k):
-        return jnp.stack(
-            [s ^ k, offset(g, c), offset(1 - g, c), offset(g, 1 - c), offset(1 - g, 1 - c)]
-        ).astype(jnp.int32)
-
-    chunks = {k: chunk(k) for k in (3, 2, 1)}
-    acc = project(spot(0), acts, [own], None, 0, 5, F32)
-    acc = project(spot(3), acts, chunks[3], acc, 0, 5, F32)
-    acc = project(spot(2), acts, chunks[2], acc, 0, 5, F32)
-    kv_own = project(spot(1), acts, chunks[1], acc, 0, 3, BF)
+        return [got, got_y, over_core(jnp.concatenate([got, got_y], axis=0))]
+
+    w1 = chunk(with_kv(*package(1)), 1)
+    w3 = chunk(with_kv(*package(3)), 3)
+    four, kv = package(2)
+    w2a = chunk(jnp.concatenate([four[:, : 2 * VDIM], kv], axis=1), 2)
+    w2b = chunk(four[:, 2 * VDIM :], 2)
+    split = 3 * VDIM
+    acc_kv, acc_q = project_early(place, early, own, w1, split)
+    every = {0: ([own], 0), 1: (w1, 0), 3: (w3, 0)}
+    kv_own = project_rest(place, early, late, acc_kv, every | {2: (w2a, 0)}, 0, split)
     kv_oth = over_core(kv_own)
-    queries = project(spot(1), acts, chunks[1], acc, 3, 2, BF)
-
-    lam_both = jnp.concatenate([lam, over_core(lam)])
-    sink_both = jnp.concatenate([sink, over_core(sink)])
-    at = ((s // 2) ^ c) * 2 + s % 2
-    lam_one = lax.dynamic_slice(lam_both, (at,), (1,))
-    sink_two = lax.dynamic_slice(sink_both, (at * 2,), (2,))
-    place = jnp.stack([s, x, c]).astype(jnp.int32)
+    queries = project_rest(
+        place, early, late, acc_q, every | {2: (w2b, split)}, split, own.shape[1] - split
+    )
+
+    scalars = (lam, over_core(lam), sink, over_core(sink))
     gain = output_norm_gain.reshape(1, VDIM)
     weights = [proj_diff, proj_win, over_core(proj_diff), over_core(proj_win)]
 
-    def spread(y):
-        y = y.reshape(sp, WINDOW, 2 * VDIM)
-        return [y[0]] + [over_z(y[k], k) for k in range(1, sp)]
-
-    y_far = attention(place, lam_one, sink_two, gain, queries, kv_own, kv_oth, sp, nx, 1)
-    y_near = attention(place, lam_one, sink_two, gain, queries, kv_own, kv_oth, sp, nx, 0)
-    part = output_projection(place, spread(y_far), weights, None)
-    received = over_x(part)
-    return output_projection(place, spread(y_near), weights, received)
+    def spread(ys):
+        return [ys[0]] + [over_z(ys[k], k) for k in range(1, sp)]
+
+    def attend(flip):
+        return attention(place, scalars, gain, queries, kv_own, kv_oth, sp, nx, flip)
+
+    far_heads = spread(attend(1))
+    y_near = attend(0)
+    near_heads = spread(y_near)
+    received = []
+    tiles = proj_diff.shape[1] // OUT_TILE
+    for begin, end in ((0, 1), (1, tiles)):
+        part = output_projection(place, far_heads, weights, begin, end - begin, BF)
+        received.append(over_x(part))
+    kept = output_projection(place, near_heads, weights, 0, tiles, F32)
+    return (kept + jnp.concatenate(received, axis=1).astype(F32)).astype(BF)
 
 
 def solution(mesh):

time: 316 us -> 277 us (0.88)
  starting transfers between devices: 86 us -> 52.7 us
  Pallas kernels: 82.4 us -> 68.5 us
  other arithmetic: 13.2 us -> 22.7 us
  local copies, waits for them, and re-layouts: 29.8 us -> 20.3 us
  waiting for transfers between devices: 104 us -> 111 us
    ppermute x35 -> x36, starting transfers between devices: 86 us -> 52.7 us  [send(): return lax.ppermute(value, AXES, pairs)]
    pallas_call x9 -> x8, Pallas kernels: 82.4 us -> 68.5 us  [the longest x2 20.9 us: project_rest(): pl.pallas_call(kernel, grid_spec=pltpu.PrefetchScalarGridSpec(num_scalar_...]
    ppermute x35 -> x36, waiting for transfers between devices: 104 us -> 111 us  [send(): return lax.ppermute(value, AXES, pairs)]
    concatenate x2 -> x6, other arithmetic: 0.15 us -> 5.41 us  [the longest x1 3.07 us: chip_body(): late = jnp.concatenate([slot3, tx3], axis=0)]
    dynamic_slice x4, local copies, waits for them, and re-layouts: 6.51 us -> 2.97 us  [pack(): parts.append(lax.dynamic_slice(w, (lo, head * VDIM), (size, VDIM)))]
    unnamed x56 -> x79, local copies, waits for them, and re-layouts: 12.3 us -> 12.2 us
  transfers between devices with their start and end apart: 35 -> 36, of which waited for: 11 -> 14; matrix products, arithmetic and copies ran while one was open for 10% -> 10% of each run, Pallas kernels for 20% -> 22%
where the time goes in v1:
time: 277 us; the launch traced here: 276 us
  waiting for transfers between devices  111 us (40%)
  Pallas kernels  68.5 us (25%)
  starting transfers between devices  52.7 us (19%)
  other arithmetic  22.7 us (8%)
  local copies, waits for them, and re-layouts  20.3 us (7%)
    ppermute x36, waiting for transfers between devices, send(): return lax.ppermute(value, AXES, pairs)  111 us
    ppermute x36, starting transfers between devices, send(): return lax.ppermute(value, AXES, pairs)  52.7 us
    pallas_call x2, Pallas kernels, project_rest(): pl.pallas_call(kernel, grid_spec=pltpu.PrefetchScalarGridSpec(num_scalar_...  20.9 us
    pallas_call x3, Pallas kernels, output_projection(): pl.pallas_call(kernel, grid=(count,), in_specs=in_specs, out_specs=pl.Blo...  20.1 us
    pallas_call x2, Pallas kernels, attention(): pl.pallas_call(kernel, grid=(sp // 2,), in_specs=[smem] * 5 + [pl.BlockSp...  18 us
    unnamed x79, local copies, waits for them, and re-layouts  12.2 us
    pallas_call x1, Pallas kernels, project_early(): pl.pallas_call(kernel, grid_spec=pltpu.PrefetchScalarGridSpec(num_scalar_...  9.44 us
  transfers between devices with their start and end apart: 36, of which 14 were waited for; matrix products, arithmetic and copies ran while one was open for 10% of the time, Pallas kernels for 22%

profile of v1, /device:TPU:0, one launch (start us, length us, event | category | flops | bytes accessed | tf_op | source)
XLA Modules:
  0.0 275.8 jit_solution(17586769903608901541)
XLA Ops:
  1.7 3.0 %constant_dynamic-update-slice_fusion.5 = (bf16[768,4096]{1,0:T(8,128)(2,1)}, bf16[128,4096]{1,0:T(8,128)(2,1)}) fusion(f32[4096]{0:T(1024)} %param.13, f32[128]{0:T(128)S(1)} %add_rsqrt_fusion, bf16[128,4096]{1,0:T(8,128)(2,1)} %param.12), kind=kLoop, calls=%fused_computation.37 | loop fusion | flops 2097151 | bytes 3162624
  4.7 3.1 %collective-permute-start.2 = (bf16[128,4096]{1,0:T(8,128)(2,1)}, bf16[128,4096]{1,0:T(8,128)(2,1)}, u32[]{:S(2)}, u32[]{:S(2)}) collective-permute-start(bf16[128,4096]{1,0:T(8,128)(2,1)} %get-tuple-element.28), channel_id=1, source_target_pairs={{0,4},{1,5},{2,6},{3,7},{4,0},{5,1},{6,2},{7,3},{8,12},{9,13},{10,... | collective-permute-start | bytes 3145736 | tf_op jit(solution)/shard_map/ppermute | solution.py:484
  17.3 4.0 %collective-permute-start.9 = (bf16[1024,1024]{1,0:T(8,128)(2,1)}, bf16[1024,1024]{1,0:T(8,128)(2,1)}, u32[]{:S(2)}, u32[]{:S(2)}) collective-permute-start(bf16[1024,1024]{1,0:T(8,128)(2,1)} %pad_maximum_fusion.1), channel_id=1, source_target_pairs={{0,1},{2,3},{4,5},{6,7},{9,8},{11,10},{13,12},{15,14},{16,17},{18,... | collective-permute-start | bytes 6291464 | tf_op jit(solution)/shard_map/ppermute | solution.py:484
  28.0 3.2 %collective-permute-done.2 = bf16[128,4096]{1,0:T(8,128)(2,1)} collective-permute-done((bf16[128,4096]{1,0:T(8,128)(2,1)}, bf16[128,4096]{1,0:T(8,128)(2,1)}, u32[]{:S(2)}, u32[]{:S(2)}) %collective-permute-start.2) | collective-permute-done | bytes 1048608 | tf_op jit(solution)/shard_map/ppermute | solution.py:484
  33.5 19.9 %collective-permute-done.22.refs_8_ = bf16[256,768]{1,0:T(8,128)(2,1)S(1)} collective-permute-done((bf16[256,768]{1,0:T(8,128)(2,1)S(1)}, bf16[256,768]{1,0:T(8,128)(2,1)S(1)}, u32[]{:S(2)}, u32[]{:S(2)}) %collective-permute-start.22) | collective-permute-done | bytes 393248 | tf_op jit(solution)/shard_map/ppermute | solution.py:484
  54.9 2.3 constant_dynamic-update-slice_fusion.4
  57.2 5.0 %collective-permute-done.23.refs_9_ = bf16[256,768]{1,0:T(8,128)(2,1)S(1)} collective-permute-done((bf16[256,768]{1,0:T(8,128)(2,1)S(1)}, bf16[256,768]{1,0:T(8,128)(2,1)S(1)}, u32[]{:S(2)}, u32[]{:S(2)}) %collective-permute-start.23) | collective-permute-done | bytes 393248 | tf_op jit(solution)/shard_map/ppermute | solution.py:484
  63.3 12.0 %collective-permute-start.11 = (bf16[256,1280]{1,0:T(8,128)(2,1)S(1)}, bf16[256,1280]{1,0:T(8,128)(2,1)S(1)}, u32[]{:S(2)}, u32[]{:S(2)}) collective-permute-start(bf16[256,1280]{1,0:T(8,128)(2,1)S(1)} %pad_maximum_fusion.8), channel_id=1, source_target_pairs={{0,4},{1,5},{2,6},{3,7},{4,0},{5,1},{6,2},{7,3},{8,12},{9,13},{10,... | collective-permute-start | bytes 1966088 | tf_op jit(solution)/shard_map/ppermute | solution.py:484
  75.3 2.7 collective-permute-start.19
  80.7 9.7 %collective-permute-done.11.refs_0_.refs_5_ = bf16[256,1280]{1,0:T(8,128)(2,1)S(1)} collective-permute-done((bf16[256,1280]{1,0:T(8,128)(2,1)S(1)}, bf16[256,1280]{1,0:T(8,128)(2,1)S(1)}, u32[]{:S(2)}, u32[]{:S(2)}) %collective-permute-start.11) | collective-permute-done | bytes 655392 | tf_op jit(solution)/shard_map/ppermute | solution.py:484
  91.9 2.3 constant_dynamic-update-slice_fusion.2
  99.0 6.4 %collective-permute-done.19.refs_11_ = bf16[256,1280]{1,0:T(8,128)(2,1)S(1)} collective-permute-done((bf16[256,1280]{1,0:T(8,128)(2,1)S(1)}, bf16[256,1280]{1,0:T(8,128)(2,1)S(1)}, u32[]{:S(2)}, u32[]{:S(2)}) %collective-permute-start.19) | collective-permute-done | bytes 655392 | tf_op jit(solution)/shard_map/ppermute | solution.py:484
  109.6 18.1 %collective-permute-done.14 = bf16[128,4096]{1,0:T(8,128)(2,1)S(1)} collective-permute-done((bf16[128,4096]{1,0:T(8,128)(2,1)S(1)}, bf16[128,4096]{1,0:T(8,128)(2,1)S(1)}, u32[]{:S(2)}, u32[]{:S(2)}) %collective-permute-start.14) | collective-permute-done | bytes 1048608 | tf_op jit(solution)/shard_map/ppermute | solution.py:484
  131.6 2.5 collective-permute-done.8
  136.2 9.4 %project.3 = (f32[768,768]{1,0:T(8,128)}, f32[768,512]{1,0:T(8,128)}) custom-call(s32[4]{0:T(128)} %pad_add_fusion.place_ref.refs_0_, bf16[768,4096]{1,0:T(8,128)(2,1)} %constant_dynamic-update-slice_fusion.a0.a1.e2.e3, bf16[768,4096]{1,0:T(8,128)(2,1)} %constant_dynamic-update-slice_fusion.a0.a1.e2.e3, bf16[1024,1280]{1,0:T(8,128)(2,1)} %pad_maximum_fusion.own_ref.refs_4_, ...), custom_call_target="tpu_custom_call" | custom-call | flops 4026531840 | bytes 7864320 | tf_op jit(solution)/shard_map/project/pallas_call | solution.py:317
  145.6 10.2 %collective-permute-done.15 = bf16[128,4096]{1,0:T(8,128)(2,1)} collective-permute-done((bf16[128,4096]{1,0:T(8,128)(2,1)}, bf16[128,4096]{1,0:T(8,128)(2,1)}, u32[]{:S(2)}, u32[]{:S(2)}) %collective-permute-start.15) | collective-permute-done | bytes 1048608 | tf_op jit(solution)/shard_map/ppermute | solution.py:484
  155.8 3.1 %pad_maximum_fusion.3.refs_0_.refs_1_.refs_2_.refs_3_ = bf16[256,4096]{1,0:T(8,128)(2,1)} fusion(bf16[128,4096]{1,0:T(8,128)(2,1)} %collective-permute-done.15, bf16[128,4096]{1,0:T(8,128)(2,1)} %broadcast_select_fusion.1), kind=kLoop, calls=%fused_computation.8 | loop fusion | flops 4194304 | bytes 4194304 | tf_op jit(solution)/shard_map/concatenate | solution.py:515
  160.2 11.5 %project.5.refs_7_ = bf16[1024,768]{1,0:T(8,128)(2,1)} custom-call(s32[4]{0:T(128)} %pad_add_fusion.place_ref.refs_0_, f32[768,768]{1,0:T(8,128)} %get-tuple-element.16.acc_ref, bf16[768,4096]{1,0:T(8,128)(2,1)} %constant_dynamic-update-slice_fusion.a0.a1.e2.e3, bf16[768,4096]{1,0:T(8,128)(2,1)} %constant_dynamic-update-slice_fusion.a0.a1.e2.e3, ...), custom_call_target="tpu_custom_call" | custom-call | flops 4026531840 | bytes 16777216 | tf_op jit(solution)/shard_map/project/pallas_call | solution.py:391
  172.7 13.5 %collective-permute-done.16.refs_8_ = bf16[256,512]{1,0:T(8,128)(2,1)S(1)} collective-permute-done((bf16[256,512]{1,0:T(8,128)(2,1)S(1)}, bf16[256,512]{1,0:T(8,128)(2,1)S(1)}, u32[]{:S(2)}, u32[]{:S(2)}) %collective-permute-start.16) | collective-permute-done | bytes 262176 | tf_op jit(solution)/shard_map/ppermute | solution.py:484
  187.5 7.0 %collective-permute-done.17.refs_9_ = bf16[256,512]{1,0:T(8,128)(2,1)S(1)} collective-permute-done((bf16[256,512]{1,0:T(8,128)(2,1)S(1)}, bf16[256,512]{1,0:T(8,128)(2,1)S(1)}, u32[]{:S(2)}, u32[]{:S(2)}) %collective-permute-start.17) | collective-permute-done | bytes 262176 | tf_op jit(solution)/shard_map/ppermute | solution.py:484
  197.3 9.4 %project.4.refs_6_ = bf16[1024,512]{1,0:T(8,128)(2,1)} custom-call(s32[4]{0:T(128)} %pad_add_fusion.place_ref.refs_0_, f32[768,512]{1,0:T(8,128)} %get-tuple-element.15.acc_ref, bf16[768,4096]{1,0:T(8,128)(2,1)} %constant_dynamic-update-slice_fusion.a0.a1.e2.e3, bf16[768,4096]{1,0:T(8,128)(2,1)} %constant_dynamic-update-slice_fusion.a0.a1.e2.e3, ...), custom_call_target="tpu_custom_call" | custom-call | flops 2684354560 | bytes 16777216 | tf_op jit(solution)/shard_map/project/pallas_call | solution.py:391
  207.9 9.0 %attend.3 = (bf16[128,512]{1,0:T(8,128)(2,1)}, bf16[128,512]{1,0:T(8,128)(2,1)}, bf16[128,512]{1,0:T(8,128)(2,1)}, bf16[128,512]{1,0:T(8,128)(2,1)}) custom-call(s32[4]{0:T(128)} %pad_add_fusion.place_ref.refs_0_, f32[2]{0:T(128)} %refs_1_.3, f32[2]{0:T(128)} %copy-done.36, f32[4]{0:T(128)} %refs_3_.3, f32[4]{0:T(128)} %copy-done.37, f32[1,256]{1,0:T(1,128)} %bitcast.27, ...), custom_call_target="tpu_custom_call" | custom-call | flops 1610612736 | bytes 4194304 | tf_op jit(solution)/shard_map/attend/pallas_call | solution.py:261
  216.9 2.7 collective-permute-start.32
  221.3 3.5 %collective-permute-done.31.refs_1_ = bf16[128,512]{1,0:T(8,128)(2,1)S(1)} collective-permute-done((bf16[128,512]{1,0:T(8,128)(2,1)}, bf16[128,512]{1,0:T(8,128)(2,1)S(1)}, u32[]{:S(2)}, u32[]{:S(2)}) %collective-permute-start.31) | collective-permute-done | bytes 131104 | tf_op jit(solution)/shard_map/ppermute | solution.py:484
  224.8 5.3 %collective-permute-done.32.refs_2_ = bf16[128,512]{1,0:T(8,128)(2,1)S(1)} collective-permute-done((bf16[128,512]{1,0:T(8,128)(2,1)}, bf16[128,512]{1,0:T(8,128)(2,1)S(1)}, u32[]{:S(2)}, u32[]{:S(2)}) %collective-permute-start.32) | collective-permute-done | bytes 131104 | tf_op jit(solution)/shard_map/ppermute | solution.py:484
  230.8 7.4 %output.5 = bf16[128,3072]{1,0:T(8,128)(2,1)} custom-call(s32[4]{0:T(128)} %pad_add_fusion.place_ref.refs_0_, bf16[128,512]{1,0:T(8,128)(2,1)} %get-tuple-element.21.refs_0_, bf16[128,512]{1,0:T(8,128)(2,1)} %copy-done.21, bf16[128,512]{1,0:T(8,128)(2,1)} %copy-done.22, bf16[128,512]{1,0:T(8,128)(2,1)} %copy-done.23, bf16[512,4096]{1,0:T(8,128)(2,1)} %refs_4_.5, ...), custom_call_target="tpu_custom_call" | custom-call | flops 1610612736 | bytes 12582912 | tf_op jit(solution)/shard_map/output/pallas_call | solution.py:441
  239.7 9.0 %attend.2 = (bf16[128,512]{1,0:T(8,128)(2,1)}, bf16[128,512]{1,0:T(8,128)(2,1)}, bf16[128,512]{1,0:T(8,128)(2,1)}, bf16[128,512]{1,0:T(8,128)(2,1)}) custom-call(s32[4]{0:T(128)} %pad_add_fusion.place_ref.refs_0_, f32[2]{0:T(128)} %refs_1_.3, f32[2]{0:T(128)} %copy-done.36, f32[4]{0:T(128)} %refs_3_.3, f32[4]{0:T(128)} %copy-done.37, f32[1,256]{1,0:T(1,128)} %bitcast.28, ...), custom_call_target="tpu_custom_call" | custom-call | flops 1610612736 | bytes 4194304 | tf_op jit(solution)/shard_map/attend/pallas_call | solution.py:261
  248.7 2.5 collective-permute-start.26
  253.6 3.9 %output.4 = bf16[128,1024]{1,0:T(8,128)(2,1)} custom-call(s32[4]{0:T(128)} %pad_add_fusion.place_ref.refs_0_, bf16[128,512]{1,0:T(8,128)(2,1)} %get-tuple-element.21.refs_0_, bf16[128,512]{1,0:T(8,128)(2,1)} %copy-done.21, bf16[128,512]{1,0:T(8,128)(2,1)} %copy-done.22, bf16[128,512]{1,0:T(8,128)(2,1)} %copy-done.23, bf16[512,4096]{1,0:T(8,128)(2,1)} %refs_4_.5, ...), custom_call_target="tpu_custom_call" | custom-call | flops 536870912 | bytes 4194304 | tf_op jit(solution)/shard_map/output/pallas_call | solution.py:441
  258.0 5.3 %collective-permute-done.27.refs_2_ = bf16[128,512]{1,0:T(8,128)(2,1)S(1)} collective-permute-done((bf16[128,512]{1,0:T(8,128)(2,1)}, bf16[128,512]{1,0:T(8,128)(2,1)S(1)}, u32[]{:S(2)}, u32[]{:S(2)}) %collective-permute-start.27) | collective-permute-done | bytes 131104 | tf_op jit(solution)/shard_map/ppermute | solution.py:484
  264.0 8.9 %output.3 = f32[128,4096]{1,0:T(8,128)} custom-call(s32[4]{0:T(128)} %pad_add_fusion.place_ref.refs_0_, bf16[128,512]{1,0:T(8,128)(2,1)} %get-tuple-element.17.refs_0_, bf16[128,512]{1,0:T(8,128)(2,1)} %copy-done.30, bf16[128,512]{1,0:T(8,128)(2,1)} %copy-done.31, bf16[128,512]{1,0:T(8,128)(2,1)} %copy-done.32, bf16[512,4096]{1,0:T(8,128)(2,1)} %refs_4_.5, ...), custom_call_target="tpu_custom_call" | custom-call | flops 2147483648 | bytes 16777216 | tf_op jit(solution)/shard_map/output/pallas_call | solution.py:441
  273.0 2.8 %add_convert_fusion = bf16[128,4096]{1,0:T(8,128)(2,1)} fusion(f32[128,4096]{1,0:T(8,128)} %output.3, bf16[128,3072]{1,0:T(8,128)(2,1)S(1)} %collective-permute-done.35, bf16[128,1024]{1,0:T(8,128)(2,1)S(1)} %collective-permute-done.34), kind=kLoop, calls=%fused_computation.9 | loop fusion | flops 3145728 | bytes 4194304 | tf_op jit(solution)/shard_map/convert_element_type | solution.py:587
  (163 shorter events, 56.6 us)
Async XLA Ops:
  4.7 26.5 %collective-permute-start.2 = (bf16[128,4096]{1,0:T(8,128)(2,1)}, bf16[128,4096]{1,0:T(8,128)(2,1)}, u32[]{:S(2)}, u32[]{:S(2)}) collective-permute-start(bf16[128,4096]{1,0:T(8,128)(2,1)} %get-tuple-element.28), channel_id=1, source_target_pairs={{0,4},{1,5},{2,6},{3,7},{4,0},{5,1},{6,2},{7,3},{8,12},{9,13},{10,... | collective-permute-start | bytes 3145736 | tf_op jit(solution)/shard_map/ppermute | solution.py:484
  7.8 24.3 %collective-permute-start.4 = (bf16[128,4096]{1,0:T(8,128)(2,1)}, bf16[128,4096]{1,0:T(8,128)(2,1)}, u32[]{:S(2)}, u32[]{:S(2)}) collective-permute-start(bf16[128,4096]{1,0:T(8,128)(2,1)} %get-tuple-element.28), channel_id=1, source_target_pairs={{4,8},{5,9},{6,10},{7,11},{8,4},{9,5},{10,6},{11,7},{20,24},{21,25... | collective-permute-start | bytes 3145736 | tf_op jit(solution)/shard_map/ppermute | solution.py:484
  9.4 69.8 %collective-permute-start.6 = (bf16[128,4096]{1,0:T(8,128)(2,1)}, bf16[128,4096]{1,0:T(8,128)(2,1)}, u32[]{:S(2)}, u32[]{:S(2)}) collective-permute-start(bf16[128,4096]{1,0:T(8,128)(2,1)} %get-tuple-element.28), channel_id=1, source_target_pairs={{0,2},{1,3},{2,0},{3,1},{4,6},{5,7},{6,4},{7,5},{8,10},{9,11},{10,... | collective-permute-start | bytes 3145736 | tf_op jit(solution)/shard_map/ppermute | solution.py:484
  14.3 10.8 %collective-permute-start.10 = (bf16[2,256,1024]{2,1,0:T(8,128)(2,1)}, bf16[2,256,1024]{2,1,0:T(8,128)(2,1)}, u32[]{:S(2)}, u32[]{:S(2)}) collective-permute-start(bf16[2,256,1024]{2,1,0:T(8,128)(2,1)} %pad_maximum_fusion.6), channel_id=1, source_target_pairs={{0,1},{1,0},{2,3},{3,2},{4,5},{5,4},{6,7},{7,6},{8,9},{9,8},{10,11... | collective-permute-start | bytes 3145736 | tf_op jit(solution)/shard_map/ppermute | solution.py:484
  17.3 76.9 %collective-permute-start.9 = (bf16[1024,1024]{1,0:T(8,128)(2,1)}, bf16[1024,1024]{1,0:T(8,128)(2,1)}, u32[]{:S(2)}, u32[]{:S(2)}) collective-permute-start(bf16[1024,1024]{1,0:T(8,128)(2,1)} %pad_maximum_fusion.1), channel_id=1, source_target_pairs={{0,1},{2,3},{4,5},{6,7},{9,8},{11,10},{13,12},{15,14},{16,17},{18,... | collective-permute-start | bytes 6291464 | tf_op jit(solution)/shard_map/ppermute | solution.py:484
  27.5 25.9 %collective-permute-start.22 = (bf16[256,768]{1,0:T(8,128)(2,1)S(1)}, bf16[256,768]{1,0:T(8,128)(2,1)S(1)}, u32[]{:S(2)}, u32[]{:S(2)}) collective-permute-start(bf16[256,768]{1,0:T(8,128)(2,1)S(1)} %pad_maximum_fusion.11), channel_id=1, source_target_pairs={{0,8},{1,9},{2,10},{3,11},{4,12},{5,13},{6,14},{7,15},{8,0},{9,1},... | collective-permute-start | bytes 1179656 | tf_op jit(solution)/shard_map/ppermute | solution.py:484
  31.3 32.0 %collective-permute-start.3 = (bf16[128,4096]{1,0:T(8,128)(2,1)}, bf16[128,4096]{1,0:T(8,128)(2,1)S(1)}, u32[]{:S(2)}, u32[]{:S(2)}) collective-permute-start(bf16[128,4096]{1,0:T(8,128)(2,1)} %collective-permute-done.2), channel_id=1, source_target_pairs={{4,8},{5,9},{6,10},{7,11},{8,4},{9,5},{10,6},{11,7},{20,24},{21,25... | collective-permute-start | bytes 3145736 | tf_op jit(solution)/shard_map/ppermute | solution.py:484
  32.1 43.2 %collective-permute-start.5 = (bf16[128,4096]{1,0:T(8,128)(2,1)}, bf16[128,4096]{1,0:T(8,128)(2,1)S(1)}, u32[]{:S(2)}, u32[]{:S(2)}) collective-permute-start(bf16[128,4096]{1,0:T(8,128)(2,1)} %collective-permute-done.4), channel_id=1, source_target_pairs={{4,0},{5,1},{6,2},{7,3},{8,12},{9,13},{10,14},{11,15},{20,16},{21,... | collective-permute-start | bytes 3145736 | tf_op jit(solution)/shard_map/ppermute | solution.py:484
  53.4 8.9 %collective-permute-start.23 = (bf16[256,768]{1,0:T(8,128)(2,1)S(1)}, bf16[256,768]{1,0:T(8,128)(2,1)S(1)}, u32[]{:S(2)}, u32[]{:S(2)}) collective-permute-start(bf16[256,768]{1,0:T(8,128)(2,1)S(1)} %collective-permute-done.22.refs_8_), channel_id=1, source_target_pairs={{0,16},{1,17},{2,18},{3,19},{4,20},{5,21},{6,22},{7,23},{8,24},{9,... | collective-permute-start | bytes 1179656 | tf_op jit(solution)/shard_map/ppermute | solution.py:484
  62.3 159.0 %collective-permute-start.29 = (bf16[512,4096]{1,0:T(8,128)(2,1)}, bf16[512,4096]{1,0:T(8,128)(2,1)}, u32[]{:S(2)}, u32[]{:S(2)}) collective-permute-start(bf16[512,4096]{1,0:T(8,128)(2,1)} %refs_4_.5), channel_id=1, source_target_pairs={{0,1},{1,0},{2,3},{3,2},{4,5},{5,4},{6,7},{7,6},{8,9},{9,8},{10,11... | collective-permute-start | bytes 12582920 | tf_op jit(solution)/shard_map/ppermute | solution.py:484
  63.3 27.1 %collective-permute-start.11 = (bf16[256,1280]{1,0:T(8,128)(2,1)S(1)}, bf16[256,1280]{1,0:T(8,128)(2,1)S(1)}, u32[]{:S(2)}, u32[]{:S(2)}) collective-permute-start(bf16[256,1280]{1,0:T(8,128)(2,1)S(1)} %pad_maximum_fusion.8), channel_id=1, source_target_pairs={{0,4},{1,5},{2,6},{3,7},{4,0},{5,1},{6,2},{7,3},{8,12},{9,13},{10,... | collective-permute-start | bytes 1966088 | tf_op jit(solution)/shard_map/ppermute | solution.py:484
  75.3 30.1 %collective-permute-start.19 = (bf16[256,1280]{1,0:T(8,128)(2,1)S(1)}, bf16[256,1280]{1,0:T(8,128)(2,1)S(1)}, u32[]{:S(2)}, u32[]{:S(2)}) collective-permute-start(bf16[256,1280]{1,0:T(8,128)(2,1)S(1)} %pad_maximum_fusion.9), channel_id=1, source_target_pairs={{0,12},{1,13},{2,14},{3,15},{4,8},{5,9},{6,10},{7,11},{8,4},{9,5},... | collective-permute-start | bytes 1966088 | tf_op jit(solution)/shard_map/ppermute | solution.py:484
  79.2 26.2 %collective-permute-start.7 = (bf16[128,4096]{1,0:T(8,128)(2,1)}, bf16[128,4096]{1,0:T(8,128)(2,1)S(1)}, u32[]{:S(2)}, u32[]{:S(2)}) collective-permute-start(bf16[128,4096]{1,0:T(8,128)(2,1)} %collective-permute-done.2), channel_id=1, source_target_pairs={{0,2},{1,3},{2,0},{3,1},{4,6},{5,7},{6,4},{7,5},{8,10},{9,11},{10,... | collective-permute-start | bytes 3145736 | tf_op jit(solution)/shard_map/ppermute | solution.py:484
  90.4 17.6 %collective-permute-start.12 = (bf16[256,1280]{1,0:T(8,128)(2,1)S(1)}, bf16[256,1280]{1,0:T(8,128)(2,1)S(1)}, u32[]{:S(2)}, u32[]{:S(2)}) collective-permute-start(bf16[256,1280]{1,0:T(8,128)(2,1)S(1)} %collective-permute-done.11.refs_0_.refs_5_), channel_id=1, source_target_pairs={{0,16},{1,17},{2,18},{3,19},{4,20},{5,21},{6,22},{7,23},{8,24},{9,... | collective-permute-start | bytes 1966088 | tf_op jit(solution)/shard_map/ppermute | solution.py:484
  94.2 33.5 %collective-permute-start.14 = (bf16[128,4096]{1,0:T(8,128)(2,1)S(1)}, bf16[128,4096]{1,0:T(8,128)(2,1)S(1)}, u32[]{:S(2)}, u32[]{:S(2)}) collective-permute-start(bf16[128,4096]{1,0:T(8,128)(2,1)S(1)} %collective-permute-done.3), channel_id=1, source_target_pairs={{4,0},{5,1},{6,2},{7,3},{8,12},{9,13},{10,14},{11,15},{20,16},{21,... | collective-permute-start | bytes 3145736 | tf_op jit(solution)/shard_map/ppermute | solution.py:484
  105.4 115.9 %collective-permute-start.30 = (bf16[512,4096]{1,0:T(8,128)(2,1)}, bf16[512,4096]{1,0:T(8,128)(2,1)}, u32[]{:S(2)}, u32[]{:S(2)}) collective-permute-start(bf16[512,4096]{1,0:T(8,128)(2,1)} %refs_5_.5), channel_id=1, source_target_pairs={{0,1},{1,0},{2,3},{3,2},{4,5},{5,4},{6,7},{7,6},{8,9},{9,8},{10,11... | collective-permute-start | bytes 12582920 | tf_op jit(solution)/shard_map/ppermute | solution.py:484
  105.4 23.5 %collective-permute-start.20 = (bf16[256,1280]{1,0:T(8,128)(2,1)S(1)}, bf16[256,1280]{1,0:T(8,128)(2,1)S(1)}, u32[]{:S(2)}, u32[]{:S(2)}) collective-permute-start(bf16[256,1280]{1,0:T(8,128)(2,1)S(1)} %collective-permute-done.19.refs_11_), channel_id=1, source_target_pairs={{0,16},{1,17},{2,18},{3,19},{4,20},{5,21},{6,22},{7,23},{8,24},{9,... | collective-permute-start | bytes 1966088 | tf_op jit(solution)/shard_map/ppermute | solution.py:484
  108.0 26.0 %collective-permute-start.8 = (bf16[128,4096]{1,0:T(8,128)(2,1)S(1)}, bf16[128,4096]{1,0:T(8,128)(2,1)S(1)}, u32[]{:S(2)}, u32[]{:S(2)}) collective-permute-start(bf16[128,4096]{1,0:T(8,128)(2,1)S(1)} %get-tuple-element.26), channel_id=1, source_target_pairs={{0,2},{1,3},{2,0},{3,1},{4,6},{5,7},{6,4},{7,5},{8,10},{9,11},{10,... | collective-permute-start | bytes 3145736 | tf_op jit(solution)/shard_map/ppermute | solution.py:484
  128.9 27.0 %collective-permute-start.15 = (bf16[128,4096]{1,0:T(8,128)(2,1)}, bf16[128,4096]{1,0:T(8,128)(2,1)}, u32[]{:S(2)}, u32[]{:S(2)}) collective-permute-start(bf16[128,4096]{1,0:T(8,128)(2,1)} %broadcast_select_fusion.1), channel_id=1, source_target_pairs={{0,2},{1,3},{2,0},{3,1},{4,6},{5,7},{6,4},{7,5},{8,10},{9,11},{10,... | collective-permute-start | bytes 3145736 | tf_op jit(solution)/shard_map/ppermute | solution.py:484
  134.1 24.9 %collective-permute-start.21 = (bf16[512,1280]{1,0:T(8,128)(2,1)}, bf16[512,1280]{1,0:T(8,128)(2,1)S(1)}, u32[]{:S(2)}, u32[]{:S(2)}) collective-permute-start(bf16[512,1280]{1,0:T(8,128)(2,1)} %pad_maximum_fusion.5), channel_id=1, source_target_pairs={{0,1},{1,0},{2,3},{3,2},{4,5},{5,4},{6,7},{7,6},{8,9},{9,8},{10,11... | collective-permute-start | bytes 3932168 | tf_op jit(solution)/shard_map/ppermute | solution.py:484
  135.1 23.8 %collective-permute-start.24 = (bf16[512,768]{1,0:T(8,128)(2,1)}, bf16[512,768]{1,0:T(8,128)(2,1)S(1)}, u32[]{:S(2)}, u32[]{:S(2)}) collective-permute-start(bf16[512,768]{1,0:T(8,128)(2,1)} %pad_maximum_fusion.7), channel_id=1, source_target_pairs={{0,1},{1,0},{2,3},{3,2},{4,5},{5,4},{6,7},{7,6},{8,9},{9,8},{10,11... | collective-permute-start | bytes 2359304 | tf_op jit(solution)/shard_map/ppermute | solution.py:484
  171.8 35.0 %collective-permute-start.25 = (bf16[1024,768]{1,0:T(8,128)(2,1)}, bf16[1024,768]{1,0:T(8,128)(2,1)S(1)}, u32[]{:S(2)}, u32[]{:S(2)}) collective-permute-start(bf16[1024,768]{1,0:T(8,128)(2,1)} %project.5.refs_7_), channel_id=1, source_target_pairs={{0,1},{1,0},{2,3},{3,2},{4,5},{5,4},{6,7},{7,6},{8,9},{9,8},{10,11... | collective-permute-start | bytes 4718600 | tf_op jit(solution)/shard_map/ppermute | solution.py:484
  171.8 14.4 %collective-permute-start.16 = (bf16[256,512]{1,0:T(8,128)(2,1)S(1)}, bf16[256,512]{1,0:T(8,128)(2,1)S(1)}, u32[]{:S(2)}, u32[]{:S(2)}) collective-permute-start(bf16[256,512]{1,0:T(8,128)(2,1)S(1)} %copy-done.29), channel_id=1, source_target_pairs={{0,8},{1,9},{2,10},{3,11},{4,12},{5,13},{6,14},{7,15},{8,0},{9,1},... | collective-permute-start | bytes 786440 | tf_op jit(solution)/shard_map/ppermute | solution.py:484
  194.6 12.1 %collective-permute-start = (f32[2]{0:T(128)S(1)}, f32[2]{0:T(128)S(1)}, u32[]{:S(2)}, u32[]{:S(2)}) collective-permute-start(f32[2]{0:T(128)S(1)} %copy-done.34), channel_id=1, source_target_pairs={{0,1},{1,0},{2,3},{3,2},{4,5},{5,4},{6,7},{7,6},{8,9},{9,8},{10,11... | collective-permute-start | bytes 32 | tf_op jit(solution)/shard_map/ppermute | solution.py:484
  196.5 10.2 %collective-permute-start.1 = (f32[4]{0:T(128)S(1)}, f32[4]{0:T(128)S(1)}, u32[]{:S(2)}, u32[]{:S(2)}) collective-permute-start(f32[4]{0:T(128)S(1)} %copy-done.35), channel_id=1, source_target_pairs={{0,1},{1,0},{2,3},{3,2},{4,5},{5,4},{6,7},{7,6},{8,9},{9,8},{10,11... | collective-permute-start | bytes 56 | tf_op jit(solution)/shard_map/ppermute | solution.py:484
  216.9 13.2 %collective-permute-start.32 = (bf16[128,512]{1,0:T(8,128)(2,1)}, bf16[128,512]{1,0:T(8,128)(2,1)S(1)}, u32[]{:S(2)}, u32[]{:S(2)}) collective-permute-start(bf16[128,512]{1,0:T(8,128)(2,1)} %get-tuple-element.23), channel_id=1, source_target_pairs={{0,8},{1,9},{2,10},{3,11},{4,12},{5,13},{6,14},{7,15},{8,0},{9,1},... | collective-permute-start | bytes 393224 | tf_op jit(solution)/shard_map/ppermute | solution.py:484
  219.7 10.5 %collective-permute-start.33 = (bf16[128,512]{1,0:T(8,128)(2,1)}, bf16[128,512]{1,0:T(8,128)(2,1)S(1)}, u32[]{:S(2)}, u32[]{:S(2)}) collective-permute-start(bf16[128,512]{1,0:T(8,128)(2,1)} %get-tuple-element.24), channel_id=1, source_target_pairs={{0,12},{1,13},{2,14},{3,15},{4,8},{5,9},{6,10},{7,11},{8,4},{9,5},... | collective-permute-start | bytes 393224 | tf_op jit(solution)/shard_map/ppermute | solution.py:484
  238.2 34.8 %collective-permute-start.35 = (bf16[128,3072]{1,0:T(8,128)(2,1)}, bf16[128,3072]{1,0:T(8,128)(2,1)S(1)}, u32[]{:S(2)}, u32[]{:S(2)}) collective-permute-start(bf16[128,3072]{1,0:T(8,128)(2,1)} %output.5), channel_id=1, source_target_pairs={{0,2},{1,3},{2,0},{3,1},{4,6},{5,7},{6,4},{7,5},{8,10},{9,11},{10,... | collective-permute-start | bytes 2359304 | tf_op jit(solution)/shard_map/ppermute | solution.py:484
  248.7 9.3 %collective-permute-start.26 = (bf16[128,512]{1,0:T(8,128)(2,1)}, bf16[128,512]{1,0:T(8,128)(2,1)S(1)}, u32[]{:S(2)}, u32[]{:S(2)}) collective-permute-start(bf16[128,512]{1,0:T(8,128)(2,1)} %get-tuple-element.18), channel_id=1, source_target_pairs={{0,4},{1,5},{2,6},{3,7},{4,0},{5,1},{6,2},{7,3},{8,12},{9,13},{10,... | collective-permute-start | bytes 393224 | tf_op jit(solution)/shard_map/ppermute | solution.py:484
  251.2 12.2 %collective-permute-start.27 = (bf16[128,512]{1,0:T(8,128)(2,1)}, bf16[128,512]{1,0:T(8,128)(2,1)S(1)}, u32[]{:S(2)}, u32[]{:S(2)}) collective-permute-start(bf16[128,512]{1,0:T(8,128)(2,1)} %get-tuple-element.19), channel_id=1, source_target_pairs={{0,8},{1,9},{2,10},{3,11},{4,12},{5,13},{6,14},{7,15},{8,0},{9,1},... | collective-permute-start | bytes 393224 | tf_op jit(solution)/shard_map/ppermute | solution.py:484
  252.0 11.4 %collective-permute-start.28 = (bf16[128,512]{1,0:T(8,128)(2,1)}, bf16[128,512]{1,0:T(8,128)(2,1)S(1)}, u32[]{:S(2)}, u32[]{:S(2)}) collective-permute-start(bf16[128,512]{1,0:T(8,128)(2,1)} %get-tuple-element.20), channel_id=1, source_target_pairs={{0,12},{1,13},{2,14},{3,15},{4,8},{5,9},{6,10},{7,11},{8,4},{9,5},... | collective-permute-start | bytes 393224 | tf_op jit(solution)/shard_map/ppermute | solution.py:484
  257.4 15.5 %collective-permute-start.34 = (bf16[128,1024]{1,0:T(8,128)(2,1)}, bf16[128,1024]{1,0:T(8,128)(2,1)S(1)}, u32[]{:S(2)}, u32[]{:S(2)}) collective-permute-start(bf16[128,1024]{1,0:T(8,128)(2,1)} %output.4), channel_id=1, source_target_pairs={{0,2},{1,3},{2,0},{3,1},{4,6},{5,7},{6,4},{7,5},{8,10},{9,11},{10,... | collective-permute-start | bytes 786440 | tf_op jit(solution)/shard_map/ppermute | solution.py:484
  (42 other events, 359.7 us)

commit v2 on v1

--- a/solution.py
+++ b/solution.py
@@ -266,7 +266,9 @@
         + [whole, whole],
         out_specs=[block] * sp,
         out_shape=[jax.ShapeDtypeStruct((WINDOW, 2 * VDIM), BF)] * sp,
-        compiler_params=pltpu.CompilerParams(dimension_semantics=("arbitrary",)),
+        compiler_params=pltpu.CompilerParams(
+            dimension_semantics=("arbitrary",), vmem_limit_bytes=20 * 2**20
+        ),
         cost_estimate=pl.CostEstimate(
             flops=4 * sp * WINDOW * rows * 2 * 384,
             bytes_accessed=4 * 2**20,
@@ -324,7 +326,9 @@
             scratch_shapes=[pltpu.VMEM((wide, cols), BF)],
         ),
         out_shape=[jax.ShapeDtypeStruct((rows, w), F32) for w in widths],
-        compiler_params=pltpu.CompilerParams(dimension_semantics=("arbitrary",)),
+        compiler_params=pltpu.CompilerParams(
+            dimension_semantics=("arbitrary",), vmem_limit_bytes=26 * 2**20
+        ),
         cost_estimate=pl.CostEstimate(
             flops=4 * rows * wide * cols, bytes_accessed=rows * cols * 8, transcendentals=0
         ),
@@ -398,7 +402,9 @@
             scratch_shapes=[pltpu.VMEM((len(order) * wide, cols), BF)],
         ),
         out_shape=jax.ShapeDtypeStruct((early.shape[0] + late.shape[0], cols), BF),
-        compiler_params=pltpu.CompilerParams(dimension_semantics=("arbitrary",)),
+        compiler_params=pltpu.CompilerParams(
+            dimension_semantics=("arbitrary",), vmem_limit_bytes=36 * 2**20
+        ),
         cost_estimate=pl.CostEstimate(
             flops=2 * (2 * early.shape[0] + 4 * late.shape[0]) * wide * cols,
             bytes_accessed=16 * 2**20,
@@ -445,7 +451,9 @@
         out_specs=pl.BlockSpec((WINDOW, tile), lambda n: (0, n)),
         out_shape=jax.ShapeDtypeStruct((WINDOW, count * tile), kind),
         scratch_shapes=[pltpu.VMEM((sp, WINDOW, 2 * VDIM), BF)],
-        compiler_params=pltpu.CompilerParams(dimension_semantics=("arbitrary",)),
+        compiler_params=pltpu.CompilerParams(
+            dimension_semantics=("arbitrary",), vmem_limit_bytes=16 * 2**20
+        ),
         cost_estimate=pl.CostEstimate(
             flops=2 * WINDOW * 2048 * count * tile,
             bytes_accessed=2048 * count * tile * 2,
@@ -580,7 +588,7 @@
     near_heads = spread(y_near)
     received = []
     tiles = proj_diff.shape[1] // OUT_TILE
-    for begin, end in ((0, 1), (1, tiles)):
+    for begin, end in ((0, tiles // 2), (tiles // 2, tiles)):
         part = output_projection(place, far_heads, weights, begin, end - begin, BF)
         received.append(over_x(part))
     kept = output_projection(place, near_heads, weights, 0, tiles, F32)

time: 277 us -> 258 us (0.931)
  Pallas kernels: 68.5 us -> 46.8 us
  waiting for transfers between devices: 111 us -> 127 us
  other arithmetic: 22.7 us -> 12.4 us
  local copies, waits for them, and re-layouts: 20.3 us -> 15.3 us
    ppermute x36, waiting for transfers between devices: 111 us -> 127 us  [send(): return lax.ppermute(value, AXES, pairs)]
    pallas_call x2, Pallas kernels: 20.9 us -> 13.5 us  [project_rest(): pl.pallas_call(kernel, grid_spec=pltpu.PrefetchScalarGridSpec(num_scalar_...]
    pallas_call x3, Pallas kernels: 20.1 us -> 14 us  [output_projection(): pl.pallas_call(kernel, grid=(count,), in_specs=in_specs, out_specs=pl.Blo...]
    pallas_call x2, Pallas kernels: 18 us -> 13.5 us  [attention(): pl.pallas_call(kernel, grid=(sp // 2,), in_specs=[smem] * 5 + [pl.BlockSp...]
    pallas_call x1, Pallas kernels: 9.44 us -> 5.81 us  [project_early(): pl.pallas_call(kernel, grid_spec=pltpu.PrefetchScalarGridSpec(num_scalar_...]
    concatenate x1, other arithmetic: 3.07 us -> 0.18 us  [chip_body(): late = jnp.concatenate([slot3, tx3], axis=0)]
    unnamed x79 -> x69, local copies, waits for them, and re-layouts: 12.2 us -> 10.2 us
  transfers between devices with their start and end apart: 36 -> 36, of which waited for: 14 -> 15; matrix products, arithmetic and copies ran while one was open for 10% -> 6% of each run, Pallas kernels for 22% -> 17%
where the time goes in v2:
time: 258 us; the launch traced here: 257 us
  waiting for transfers between devices  127 us (49%)
  starting transfers between devices  54.6 us (21%)
  Pallas kernels  46.8 us (18%)
  local copies, waits for them, and re-layouts  15.3 us (6%)
  other arithmetic  12.4 us (5%)
    ppermute x36, waiting for transfers between devices, send(): return lax.ppermute(value, AXES, pairs)  127 us
    ppermute x36, starting transfers between devices, send(): return lax.ppermute(value, AXES, pairs)  54.6 us
    pallas_call x3, Pallas kernels, output_projection(): pl.pallas_call(kernel, grid=(count,), in_specs=in_specs, out_specs=pl.Blo...  14 us
    pallas_call x2, Pallas kernels, attention(): pl.pallas_call(kernel, grid=(sp // 2,), in_specs=[smem] * 5 + [pl.BlockSp...  13.5 us
    pallas_call x2, Pallas kernels, project_rest(): pl.pallas_call(kernel, grid_spec=pltpu.PrefetchScalarGridSpec(num_scalar_...  13.5 us
    unnamed x69, local copies, waits for them, and re-layouts  10.2 us
    pallas_call x1, Pallas kernels, project_early(): pl.pallas_call(kernel, grid_spec=pltpu.PrefetchScalarGridSpec(num_scalar_...  5.81 us
  transfers between devices with their start and end apart: 36, of which 15 were waited for; matrix products, arithmetic and copies ran while one was open for 6% of the time, Pallas kernels for 17%

profile of v2, /device:TPU:0, one launch (start us, length us, event | category | flops | bytes accessed | tf_op | source)
XLA Modules:
  0.0 256.8 jit_solution(13711672356695781807)
XLA Ops:
  0.0 1.7 fusion
  1.7 3.1 %constant_dynamic-update-slice_fusion.5 = (bf16[768,4096]{1,0:T(8,128)(2,1)}, bf16[128,4096]{1,0:T(8,128)(2,1)}) fusion(f32[4096]{0:T(1024)} %param.13, f32[128]{0:T(128)S(1)} %add_rsqrt_fusion, bf16[128,4096]{1,0:T(8,128)(2,1)} %param.12), kind=kLoop, calls=%fused_computation.37 | loop fusion | flops 2097151 | bytes 3162624
  4.8 3.1 %collective-permute-start.2 = (bf16[128,4096]{1,0:T(8,128)(2,1)}, bf16[128,4096]{1,0:T(8,128)(2,1)}, u32[]{:S(2)}, u32[]{:S(2)}) collective-permute-start(bf16[128,4096]{1,0:T(8,128)(2,1)} %get-tuple-element.28), channel_id=1, source_target_pairs={{0,4},{1,5},{2,6},{3,7},{4,0},{5,1},{6,2},{7,3},{8,12},{9,13},{10,... | collective-permute-start | bytes 3145736 | tf_op jit(solution)/shard_map/ppermute | solution.py:492
  7.8 1.6 collective-permute-start.4
  17.5 3.9 %collective-permute-start.9 = (bf16[1024,1024]{1,0:T(8,128)(2,1)}, bf16[1024,1024]{1,0:T(8,128)(2,1)}, u32[]{:S(2)}, u32[]{:S(2)}) collective-permute-start(bf16[1024,1024]{1,0:T(8,128)(2,1)} %pad_maximum_fusion.1), channel_id=1, source_target_pairs={{0,1},{2,3},{4,5},{6,7},{9,8},{11,10},{13,12},{15,14},{16,17},{18,... | collective-permute-start | bytes 6291464 | tf_op jit(solution)/shard_map/ppermute | solution.py:492
  21.4 1.9 dynamic-slice_bitcast_fusion.3
  27.2 4.2 %collective-permute-done.2 = bf16[128,4096]{1,0:T(8,128)(2,1)} collective-permute-done((bf16[128,4096]{1,0:T(8,128)(2,1)}, bf16[128,4096]{1,0:T(8,128)(2,1)}, u32[]{:S(2)}, u32[]{:S(2)}) %collective-permute-start.2) | collective-permute-done | bytes 1048608 | tf_op jit(solution)/shard_map/ppermute | solution.py:492
  33.6 19.8 %collective-permute-done.22.refs_8_ = bf16[256,768]{1,0:T(8,128)(2,1)S(1)} collective-permute-done((bf16[256,768]{1,0:T(8,128)(2,1)S(1)}, bf16[256,768]{1,0:T(8,128)(2,1)S(1)}, u32[]{:S(2)}, u32[]{:S(2)}) %collective-permute-start.22) | collective-permute-done | bytes 393248 | tf_op jit(solution)/shard_map/ppermute | solution.py:492
  56.3 6.0 %collective-permute-done.23.refs_9_ = bf16[256,768]{1,0:T(8,128)(2,1)S(1)} collective-permute-done((bf16[256,768]{1,0:T(8,128)(2,1)S(1)}, bf16[256,768]{1,0:T(8,128)(2,1)S(1)}, u32[]{:S(2)}, u32[]{:S(2)}) %collective-permute-start.23) | collective-permute-done | bytes 393248 | tf_op jit(solution)/shard_map/ppermute | solution.py:492
  62.4 13.0 %collective-permute-start.11 = (bf16[256,1280]{1,0:T(8,128)(2,1)S(1)}, bf16[256,1280]{1,0:T(8,128)(2,1)S(1)}, u32[]{:S(2)}, u32[]{:S(2)}) collective-permute-start(bf16[256,1280]{1,0:T(8,128)(2,1)S(1)} %pad_maximum_fusion.8), channel_id=1, source_target_pairs={{0,4},{1,5},{2,6},{3,7},{4,0},{5,1},{6,2},{7,3},{8,12},{9,13},{10,... | collective-permute-start | bytes 1966088 | tf_op jit(solution)/shard_map/ppermute | solution.py:492
  75.3 2.6 %collective-permute-start.19 = (bf16[256,1280]{1,0:T(8,128)(2,1)S(1)}, bf16[256,1280]{1,0:T(8,128)(2,1)S(1)}, u32[]{:S(2)}, u32[]{:S(2)}) collective-permute-start(bf16[256,1280]{1,0:T(8,128)(2,1)S(1)} %pad_maximum_fusion.9), channel_id=1, source_target_pairs={{0,12},{1,13},{2,14},{3,15},{4,8},{5,9},{6,10},{7,11},{8,4},{9,5},... | collective-permute-start | bytes 1966088 | tf_op jit(solution)/shard_map/ppermute | solution.py:492
  79.8 10.6 %collective-permute-done.11.refs_0_.refs_5_ = bf16[256,1280]{1,0:T(8,128)(2,1)S(1)} collective-permute-done((bf16[256,1280]{1,0:T(8,128)(2,1)S(1)}, bf16[256,1280]{1,0:T(8,128)(2,1)S(1)}, u32[]{:S(2)}, u32[]{:S(2)}) %collective-permute-start.11) | collective-permute-done | bytes 655392 | tf_op jit(solution)/shard_map/ppermute | solution.py:492
  96.6 8.8 %collective-permute-done.19.refs_11_ = bf16[256,1280]{1,0:T(8,128)(2,1)S(1)} collective-permute-done((bf16[256,1280]{1,0:T(8,128)(2,1)S(1)}, bf16[256,1280]{1,0:T(8,128)(2,1)S(1)}, u32[]{:S(2)}, u32[]{:S(2)}) %collective-permute-start.19) | collective-permute-done | bytes 655392 | tf_op jit(solution)/shard_map/ppermute | solution.py:492
  108.7 19.0 %collective-permute-done.14 = bf16[128,4096]{1,0:T(8,128)(2,1)S(1)} collective-permute-done((bf16[128,4096]{1,0:T(8,128)(2,1)S(1)}, bf16[128,4096]{1,0:T(8,128)(2,1)S(1)}, u32[]{:S(2)}, u32[]{:S(2)}) %collective-permute-start.14) | collective-permute-done | bytes 1048608 | tf_op jit(solution)/shard_map/ppermute | solution.py:492
  129.6 3.6 %collective-permute-done.8 = bf16[128,4096]{1,0:T(8,128)(2,1)S(1)} collective-permute-done((bf16[128,4096]{1,0:T(8,128)(2,1)S(1)}, bf16[128,4096]{1,0:T(8,128)(2,1)S(1)}, u32[]{:S(2)}, u32[]{:S(2)}) %collective-permute-start.8) | collective-permute-done | bytes 1048608 | tf_op jit(solution)/shard_map/ppermute | solution.py:492
  133.9 5.8 %project.3 = (f32[768,768]{1,0:T(8,128)S(1)}, f32[768,512]{1,0:T(8,128)S(1)}) custom-call(s32[4]{0:T(128)S(1)} %pad_add_fusion.place_ref.refs_0_, bf16[768,4096]{1,0:T(8,128)(2,1)S(1)} %constant_dynamic-update-slice_fusion.a0.a1.e2.e3, bf16[768,4096]{1,0:T(8,128)(2,1)S(1)} %constant_dynamic-update-slice_fusion.a0.a1.e2.e3, ...), custom_call_target="tpu_custom_call" | custom-call | flops 4026531840 | bytes 7864320 | tf_op jit(solution)/shard_map/project/pallas_call | solution.py:319
  139.7 15.1 %collective-permute-done.15 = bf16[128,4096]{1,0:T(8,128)(2,1)S(1)} collective-permute-done((bf16[128,4096]{1,0:T(8,128)(2,1)S(1)}, bf16[128,4096]{1,0:T(8,128)(2,1)S(1)}, u32[]{:S(2)}, u32[]{:S(2)}) %collective-permute-start.15) | collective-permute-done | bytes 1048608 | tf_op jit(solution)/shard_map/ppermute | solution.py:492
  157.5 7.4 %project.5.refs_7_ = bf16[1024,768]{1,0:T(8,128)(2,1)S(1)} custom-call(s32[4]{0:T(128)S(1)} %pad_add_fusion.place_ref.refs_0_, f32[768,768]{1,0:T(8,128)S(1)} %get-tuple-element.16.acc_ref, bf16[768,4096]{1,0:T(8,128)(2,1)} %copy-done, bf16[768,4096]{1,0:T(8,128)(2,1)} %copy-done, bf16[256,4096]{1,0:T(8,128)(2,1)S(1)} %pad_maximum_fusion.3.refs_0_.refs_1_.refs_2_.refs_3_, ...), custom_call_target="tpu_custom_call" | custom-call | flops 4026531840 | bytes 16777216 | tf_op jit(solution)/shard_map/project/pallas_call | solution.py:395
  165.8 13.3 %collective-permute-done.16.refs_8_ = bf16[256,512]{1,0:T(8,128)(2,1)S(1)} collective-permute-done((bf16[256,512]{1,0:T(8,128)(2,1)S(1)}, bf16[256,512]{1,0:T(8,128)(2,1)S(1)}, u32[]{:S(2)}, u32[]{:S(2)}) %collective-permute-start.16) | collective-permute-done | bytes 262176 | tf_op jit(solution)/shard_map/ppermute | solution.py:492
  180.6 6.8 %collective-permute-done.17.refs_9_ = bf16[256,512]{1,0:T(8,128)(2,1)S(1)} collective-permute-done((bf16[256,512]{1,0:T(8,128)(2,1)S(1)}, bf16[256,512]{1,0:T(8,128)(2,1)S(1)}, u32[]{:S(2)}, u32[]{:S(2)}) %collective-permute-start.17) | collective-permute-done | bytes 262176 | tf_op jit(solution)/shard_map/ppermute | solution.py:492
  191.7 6.1 %project.4.refs_6_ = bf16[1024,512]{1,0:T(8,128)(2,1)S(1)} custom-call(s32[4]{0:T(128)S(1)} %pad_add_fusion.place_ref.refs_0_, f32[768,512]{1,0:T(8,128)S(1)} %get-tuple-element.15.acc_ref, bf16[768,4096]{1,0:T(8,128)(2,1)} %copy-done, bf16[768,4096]{1,0:T(8,128)(2,1)} %copy-done, bf16[256,4096]{1,0:T(8,128)(2,1)S(1)} %pad_maximum_fusion.3.refs_0_.refs_1_.refs_2_.refs_3_, ...), custom_call_target="tpu_custom_call" | custom-call | flops 2684354560 | bytes 16777216 | tf_op jit(solution)/shard_map/project/pallas_call | solution.py:395
  197.9 6.8 %attend.3 = (bf16[128,512]{1,0:T(8,128)(2,1)S(1)}, bf16[128,512]{1,0:T(8,128)(2,1)S(1)}, bf16[128,512]{1,0:T(8,128)(2,1)S(1)}, bf16[128,512]{1,0:T(8,128)(2,1)S(1)}) custom-call(s32[4]{0:T(128)S(1)} %pad_add_fusion.place_ref.refs_0_, f32[2]{0:T(128)S(1)} %copy-done.10, f32[2]{0:T(128)S(1)} %collective-permute-done.refs_2_, f32[4]{0:T(128)S(1)} %copy-done.11, ...), custom_call_target="tpu_custom_call" | custom-call | flops 1610612736 | bytes 4194304 | tf_op jit(solution)/shard_map/attend/pallas_call | solution.py:261
  204.7 3.0 %collective-permute-start.32 = (bf16[128,512]{1,0:T(8,128)(2,1)S(1)}, bf16[128,512]{1,0:T(8,128)(2,1)S(1)}, u32[]{:S(2)}, u32[]{:S(2)}) collective-permute-start(bf16[128,512]{1,0:T(8,128)(2,1)S(1)} %get-tuple-element.23), channel_id=1, source_target_pairs={{0,8},{1,9},{2,10},{3,11},{4,12},{5,13},{6,14},{7,15},{8,0},{9,1},... | collective-permute-start | bytes 393224 | tf_op jit(solution)/shard_map/ppermute | solution.py:492
  209.1 3.8 %collective-permute-done.31.refs_1_ = bf16[128,512]{1,0:T(8,128)(2,1)S(1)} collective-permute-done((bf16[128,512]{1,0:T(8,128)(2,1)S(1)}, bf16[128,512]{1,0:T(8,128)(2,1)S(1)}, u32[]{:S(2)}, u32[]{:S(2)}) %collective-permute-start.31) | collective-permute-done | bytes 131104 | tf_op jit(solution)/shard_map/ppermute | solution.py:492
  212.9 4.8 %collective-permute-done.32.refs_2_ = bf16[128,512]{1,0:T(8,128)(2,1)S(1)} collective-permute-done((bf16[128,512]{1,0:T(8,128)(2,1)S(1)}, bf16[128,512]{1,0:T(8,128)(2,1)S(1)}, u32[]{:S(2)}, u32[]{:S(2)}) %collective-permute-start.32) | collective-permute-done | bytes 131104 | tf_op jit(solution)/shard_map/ppermute | solution.py:492
  217.7 3.7 %output.5 = bf16[128,2048]{1,0:T(8,128)(2,1)S(1)} custom-call(s32[4]{0:T(128)S(1)} %pad_add_fusion.place_ref.refs_0_, bf16[128,512]{1,0:T(8,128)(2,1)S(1)} %get-tuple-element.21.refs_0_, bf16[128,512]{1,0:T(8,128)(2,1)S(1)} %collective-permute-done.31.refs_1_, bf16[128,512]{1,0:T(8,128)(2,1)S(1)} %collective-permute-done.32.refs_2_, ...), custom_call_target="tpu_custom_call" | custom-call | flops 1073741824 | bytes 8388608 | tf_op jit(solution)/shard_map/output/pallas_call | solution.py:447
  223.0 3.7 %output.4 = bf16[128,2048]{1,0:T(8,128)(2,1)S(1)} custom-call(s32[4]{0:T(128)S(1)} %pad_add_fusion.place_ref.refs_0_, bf16[128,512]{1,0:T(8,128)(2,1)S(1)} %get-tuple-element.21.refs_0_, bf16[128,512]{1,0:T(8,128)(2,1)S(1)} %collective-permute-done.31.refs_1_, bf16[128,512]{1,0:T(8,128)(2,1)S(1)} %collective-permute-done.32.refs_2_, ...), custom_call_target="tpu_custom_call" | custom-call | flops 1073741824 | bytes 8388608 | tf_op jit(solution)/shard_map/output/pallas_call | solution.py:447
  227.3 6.7 %attend.2 = (bf16[128,512]{1,0:T(8,128)(2,1)S(1)}, bf16[128,512]{1,0:T(8,128)(2,1)S(1)}, bf16[128,512]{1,0:T(8,128)(2,1)S(1)}, bf16[128,512]{1,0:T(8,128)(2,1)S(1)}) custom-call(s32[4]{0:T(128)S(1)} %pad_add_fusion.place_ref.refs_0_, f32[2]{0:T(128)S(1)} %copy-done.10, f32[2]{0:T(128)S(1)} %collective-permute-done.refs_2_, f32[4]{0:T(128)S(1)} %copy-done.11, ...), custom_call_target="tpu_custom_call" | custom-call | flops 1610612736 | bytes 4194304 | tf_op jit(solution)/shard_map/attend/pallas_call | solution.py:261
  234.0 2.8 %collective-permute-start.26 = (bf16[128,512]{1,0:T(8,128)(2,1)S(1)}, bf16[128,512]{1,0:T(8,128)(2,1)S(1)}, u32[]{:S(2)}, u32[]{:S(2)}) collective-permute-start(bf16[128,512]{1,0:T(8,128)(2,1)S(1)} %get-tuple-element.18), channel_id=1, source_target_pairs={{0,4},{1,5},{2,6},{3,7},{4,0},{5,1},{6,2},{7,3},{8,12},{9,13},{10,... | collective-permute-start | bytes 393224 | tf_op jit(solution)/shard_map/ppermute | solution.py:492
  239.3 1.8 collective-permute-done.26.refs_1_
  241.1 7.8 %collective-permute-done.27.refs_2_ = bf16[128,512]{1,0:T(8,128)(2,1)S(1)} collective-permute-done((bf16[128,512]{1,0:T(8,128)(2,1)S(1)}, bf16[128,512]{1,0:T(8,128)(2,1)S(1)}, u32[]{:S(2)}, u32[]{:S(2)}) %collective-permute-start.27) | collective-permute-done | bytes 131104 | tf_op jit(solution)/shard_map/ppermute | solution.py:492
  248.9 6.6 %output.3 = f32[128,4096]{1,0:T(8,128)S(1)} custom-call(s32[4]{0:T(128)S(1)} %pad_add_fusion.place_ref.refs_0_, bf16[128,512]{1,0:T(8,128)(2,1)S(1)} %get-tuple-element.17.refs_0_, bf16[128,512]{1,0:T(8,128)(2,1)S(1)} %collective-permute-done.26.refs_1_, bf16[128,512]{1,0:T(8,128)(2,1)S(1)} %collective-permute-done.27.refs_2_, ...), custom_call_target="tpu_custom_call" | custom-call | flops 2147483648 | bytes 16777216 | tf_op jit(solution)/shard_map/output/pallas_call | solution.py:447
  (154 shorter events, 47.2 us)
Async XLA Ops:
  4.8 26.6 %collective-permute-start.2 = (bf16[128,4096]{1,0:T(8,128)(2,1)}, bf16[128,4096]{1,0:T(8,128)(2,1)}, u32[]{:S(2)}, u32[]{:S(2)}) collective-permute-start(bf16[128,4096]{1,0:T(8,128)(2,1)} %get-tuple-element.28), channel_id=1, source_target_pairs={{0,4},{1,5},{2,6},{3,7},{4,0},{5,1},{6,2},{7,3},{8,12},{9,13},{10,... | collective-permute-start | bytes 3145736 | tf_op jit(solution)/shard_map/ppermute | solution.py:492
  7.8 24.4 %collective-permute-start.4 = (bf16[128,4096]{1,0:T(8,128)(2,1)}, bf16[128,4096]{1,0:T(8,128)(2,1)}, u32[]{:S(2)}, u32[]{:S(2)}) collective-permute-start(bf16[128,4096]{1,0:T(8,128)(2,1)} %get-tuple-element.28), channel_id=1, source_target_pairs={{4,8},{5,9},{6,10},{7,11},{8,4},{9,5},{10,6},{11,7},{20,24},{21,25... | collective-permute-start | bytes 3145736 | tf_op jit(solution)/shard_map/ppermute | solution.py:492
  9.4 68.8 %collective-permute-start.6 = (bf16[128,4096]{1,0:T(8,128)(2,1)}, bf16[128,4096]{1,0:T(8,128)(2,1)}, u32[]{:S(2)}, u32[]{:S(2)}) collective-permute-start(bf16[128,4096]{1,0:T(8,128)(2,1)} %get-tuple-element.28), channel_id=1, source_target_pairs={{0,2},{1,3},{2,0},{3,1},{4,6},{5,7},{6,4},{7,5},{8,10},{9,11},{10,... | collective-permute-start | bytes 3145736 | tf_op jit(solution)/shard_map/ppermute | solution.py:492
  14.3 10.4 %collective-permute-start.10 = (bf16[2,256,1024]{2,1,0:T(8,128)(2,1)}, bf16[2,256,1024]{2,1,0:T(8,128)(2,1)}, u32[]{:S(2)}, u32[]{:S(2)}) collective-permute-start(bf16[2,256,1024]{2,1,0:T(8,128)(2,1)} %pad_maximum_fusion.6), channel_id=1, source_target_pairs={{0,1},{1,0},{2,3},{3,2},{4,5},{5,4},{6,7},{7,6},{8,9},{9,8},{10,11... | collective-permute-start | bytes 3145736 | tf_op jit(solution)/shard_map/ppermute | solution.py:492
  17.5 75.8 %collective-permute-start.9 = (bf16[1024,1024]{1,0:T(8,128)(2,1)}, bf16[1024,1024]{1,0:T(8,128)(2,1)}, u32[]{:S(2)}, u32[]{:S(2)}) collective-permute-start(bf16[1024,1024]{1,0:T(8,128)(2,1)} %pad_maximum_fusion.1), channel_id=1, source_target_pairs={{0,1},{2,3},{4,5},{6,7},{9,8},{11,10},{13,12},{15,14},{16,17},{18,... | collective-permute-start | bytes 6291464 | tf_op jit(solution)/shard_map/ppermute | solution.py:492
  26.5 26.9 %collective-permute-start.22 = (bf16[256,768]{1,0:T(8,128)(2,1)S(1)}, bf16[256,768]{1,0:T(8,128)(2,1)S(1)}, u32[]{:S(2)}, u32[]{:S(2)}) collective-permute-start(bf16[256,768]{1,0:T(8,128)(2,1)S(1)} %pad_maximum_fusion.11), channel_id=1, source_target_pairs={{0,8},{1,9},{2,10},{3,11},{4,12},{5,13},{6,14},{7,15},{8,0},{9,1},... | collective-permute-start | bytes 1179656 | tf_op jit(solution)/shard_map/ppermute | solution.py:492
  31.4 31.0 %collective-permute-start.3 = (bf16[128,4096]{1,0:T(8,128)(2,1)}, bf16[128,4096]{1,0:T(8,128)(2,1)S(1)}, u32[]{:S(2)}, u32[]{:S(2)}) collective-permute-start(bf16[128,4096]{1,0:T(8,128)(2,1)} %collective-permute-done.2), channel_id=1, source_target_pairs={{4,8},{5,9},{6,10},{7,11},{8,4},{9,5},{10,6},{11,7},{20,24},{21,25... | collective-permute-start | bytes 3145736 | tf_op jit(solution)/shard_map/ppermute | solution.py:492
  32.2 43.1 %collective-permute-start.5 = (bf16[128,4096]{1,0:T(8,128)(2,1)}, bf16[128,4096]{1,0:T(8,128)(2,1)S(1)}, u32[]{:S(2)}, u32[]{:S(2)}) collective-permute-start(bf16[128,4096]{1,0:T(8,128)(2,1)} %collective-permute-done.4), channel_id=1, source_target_pairs={{4,0},{5,1},{6,2},{7,3},{8,12},{9,13},{10,14},{11,15},{20,16},{21,... | collective-permute-start | bytes 3145736 | tf_op jit(solution)/shard_map/ppermute | solution.py:492
  53.4 8.9 %collective-permute-start.23 = (bf16[256,768]{1,0:T(8,128)(2,1)S(1)}, bf16[256,768]{1,0:T(8,128)(2,1)S(1)}, u32[]{:S(2)}, u32[]{:S(2)}) collective-permute-start(bf16[256,768]{1,0:T(8,128)(2,1)S(1)} %collective-permute-done.22.refs_8_), channel_id=1, source_target_pairs={{0,16},{1,17},{2,18},{3,19},{4,20},{5,21},{6,22},{7,23},{8,24},{9,... | collective-permute-start | bytes 1179656 | tf_op jit(solution)/shard_map/ppermute | solution.py:492
  62.3 146.8 %collective-permute-start.29 = (bf16[512,4096]{1,0:T(8,128)(2,1)S(1)}, bf16[512,4096]{1,0:T(8,128)(2,1)}, u32[]{:S(2)}, u32[]{:S(2)}) collective-permute-start(bf16[512,4096]{1,0:T(8,128)(2,1)S(1)} %copy-done.1), channel_id=1, source_target_pairs={{0,1},{1,0},{2,3},{3,2},{4,5},{5,4},{6,7},{7,6},{8,9},{9,8},{10,11... | collective-permute-start | bytes 12582920 | tf_op jit(solution)/shard_map/ppermute | solution.py:492
  62.4 28.1 %collective-permute-start.11 = (bf16[256,1280]{1,0:T(8,128)(2,1)S(1)}, bf16[256,1280]{1,0:T(8,128)(2,1)S(1)}, u32[]{:S(2)}, u32[]{:S(2)}) collective-permute-start(bf16[256,1280]{1,0:T(8,128)(2,1)S(1)} %pad_maximum_fusion.8), channel_id=1, source_target_pairs={{0,4},{1,5},{2,6},{3,7},{4,0},{5,1},{6,2},{7,3},{8,12},{9,13},{10,... | collective-permute-start | bytes 1966088 | tf_op jit(solution)/shard_map/ppermute | solution.py:492
  75.3 30.1 %collective-permute-start.19 = (bf16[256,1280]{1,0:T(8,128)(2,1)S(1)}, bf16[256,1280]{1,0:T(8,128)(2,1)S(1)}, u32[]{:S(2)}, u32[]{:S(2)}) collective-permute-start(bf16[256,1280]{1,0:T(8,128)(2,1)S(1)} %pad_maximum_fusion.9), channel_id=1, source_target_pairs={{0,12},{1,13},{2,14},{3,15},{4,8},{5,9},{6,10},{7,11},{8,4},{9,5},... | collective-permute-start | bytes 1966088 | tf_op jit(solution)/shard_map/ppermute | solution.py:492
  78.2 27.2 %collective-permute-start.7 = (bf16[128,4096]{1,0:T(8,128)(2,1)}, bf16[128,4096]{1,0:T(8,128)(2,1)S(1)}, u32[]{:S(2)}, u32[]{:S(2)}) collective-permute-start(bf16[128,4096]{1,0:T(8,128)(2,1)} %collective-permute-done.2), channel_id=1, source_target_pairs={{0,2},{1,3},{2,0},{3,1},{4,6},{5,7},{6,4},{7,5},{8,10},{9,11},{10,... | collective-permute-start | bytes 3145736 | tf_op jit(solution)/shard_map/ppermute | solution.py:492
  90.4 16.7 %collective-permute-start.12 = (bf16[256,1280]{1,0:T(8,128)(2,1)S(1)}, bf16[256,1280]{1,0:T(8,128)(2,1)S(1)}, u32[]{:S(2)}, u32[]{:S(2)}) collective-permute-start(bf16[256,1280]{1,0:T(8,128)(2,1)S(1)} %collective-permute-done.11.refs_0_.refs_5_), channel_id=1, source_target_pairs={{0,16},{1,17},{2,18},{3,19},{4,20},{5,21},{6,22},{7,23},{8,24},{9,... | collective-permute-start | bytes 1966088 | tf_op jit(solution)/shard_map/ppermute | solution.py:492
  93.3 34.5 %collective-permute-start.14 = (bf16[128,4096]{1,0:T(8,128)(2,1)S(1)}, bf16[128,4096]{1,0:T(8,128)(2,1)S(1)}, u32[]{:S(2)}, u32[]{:S(2)}) collective-permute-start(bf16[128,4096]{1,0:T(8,128)(2,1)S(1)} %collective-permute-done.3), channel_id=1, source_target_pairs={{4,0},{5,1},{6,2},{7,3},{8,12},{9,13},{10,14},{11,15},{20,16},{21,... | collective-permute-start | bytes 3145736 | tf_op jit(solution)/shard_map/ppermute | solution.py:492
  105.4 103.7 %collective-permute-start.30 = (bf16[512,4096]{1,0:T(8,128)(2,1)}, bf16[512,4096]{1,0:T(8,128)(2,1)}, u32[]{:S(2)}, u32[]{:S(2)}) collective-permute-start(bf16[512,4096]{1,0:T(8,128)(2,1)} %refs_5_.5), channel_id=1, source_target_pairs={{0,1},{1,0},{2,3},{3,2},{4,5},{5,4},{6,7},{7,6},{8,9},{9,8},{10,11... | collective-permute-start | bytes 12582920 | tf_op jit(solution)/shard_map/ppermute | solution.py:492
  105.4 22.5 %collective-permute-start.20 = (bf16[256,1280]{1,0:T(8,128)(2,1)S(1)}, bf16[256,1280]{1,0:T(8,128)(2,1)S(1)}, u32[]{:S(2)}, u32[]{:S(2)}) collective-permute-start(bf16[256,1280]{1,0:T(8,128)(2,1)S(1)} %collective-permute-done.19.refs_11_), channel_id=1, source_target_pairs={{0,16},{1,17},{2,18},{3,19},{4,20},{5,21},{6,22},{7,23},{8,24},{9,... | collective-permute-start | bytes 1966088 | tf_op jit(solution)/shard_map/ppermute | solution.py:492
  107.1 26.1 %collective-permute-start.8 = (bf16[128,4096]{1,0:T(8,128)(2,1)S(1)}, bf16[128,4096]{1,0:T(8,128)(2,1)S(1)}, u32[]{:S(2)}, u32[]{:S(2)}) collective-permute-start(bf16[128,4096]{1,0:T(8,128)(2,1)S(1)} %get-tuple-element.26), channel_id=1, source_target_pairs={{0,2},{1,3},{2,0},{3,1},{4,6},{5,7},{6,4},{7,5},{8,10},{9,11},{10,... | collective-permute-start | bytes 3145736 | tf_op jit(solution)/shard_map/ppermute | solution.py:492
  128.0 26.9 %collective-permute-start.15 = (bf16[128,4096]{1,0:T(8,128)(2,1)S(1)}, bf16[128,4096]{1,0:T(8,128)(2,1)S(1)}, u32[]{:S(2)}, u32[]{:S(2)}) collective-permute-start(bf16[128,4096]{1,0:T(8,128)(2,1)S(1)} %broadcast_select_fusion.1), channel_id=1, source_target_pairs={{0,2},{1,3},{2,0},{3,1},{4,6},{5,7},{6,4},{7,5},{8,10},{9,11},{10,... | collective-permute-start | bytes 3145736 | tf_op jit(solution)/shard_map/ppermute | solution.py:492
  133.2 21.9 %collective-permute-start.21 = (bf16[512,1280]{1,0:T(8,128)(2,1)S(1)}, bf16[512,1280]{1,0:T(8,128)(2,1)S(1)}, u32[]{:S(2)}, u32[]{:S(2)}) collective-permute-start(bf16[512,1280]{1,0:T(8,128)(2,1)S(1)} %pad_maximum_fusion.5), channel_id=1, source_target_pairs={{0,1},{1,0},{2,3},{3,2},{4,5},{5,4},{6,7},{7,6},{8,9},{9,8},{10,11... | collective-permute-start | bytes 3932168 | tf_op jit(solution)/shard_map/ppermute | solution.py:492
  133.3 21.7 %collective-permute-start.24 = (bf16[512,768]{1,0:T(8,128)(2,1)S(1)}, bf16[512,768]{1,0:T(8,128)(2,1)S(1)}, u32[]{:S(2)}, u32[]{:S(2)}) collective-permute-start(bf16[512,768]{1,0:T(8,128)(2,1)S(1)} %pad_maximum_fusion.7), channel_id=1, source_target_pairs={{0,1},{1,0},{2,3},{3,2},{4,5},{5,4},{6,7},{7,6},{8,9},{9,8},{10,11... | collective-permute-start | bytes 2359304 | tf_op jit(solution)/shard_map/ppermute | solution.py:492
  164.9 33.0 %collective-permute-start.25 = (bf16[1024,768]{1,0:T(8,128)(2,1)S(1)}, bf16[1024,768]{1,0:T(8,128)(2,1)S(1)}, u32[]{:S(2)}, u32[]{:S(2)}) collective-permute-start(bf16[1024,768]{1,0:T(8,128)(2,1)S(1)} %project.5.refs_7_), channel_id=1, source_target_pairs={{0,1},{1,0},{2,3},{3,2},{4,5},{5,4},{6,7},{7,6},{8,9},{9,8},{10,11... | collective-permute-start | bytes 4718600 | tf_op jit(solution)/shard_map/ppermute | solution.py:492
  164.9 14.2 %collective-permute-start.16 = (bf16[256,512]{1,0:T(8,128)(2,1)S(1)}, bf16[256,512]{1,0:T(8,128)(2,1)S(1)}, u32[]{:S(2)}, u32[]{:S(2)}) collective-permute-start(bf16[256,512]{1,0:T(8,128)(2,1)S(1)} %get-tuple-element.54), channel_id=1, source_target_pairs={{0,8},{1,9},{2,10},{3,11},{4,12},{5,13},{6,14},{7,15},{8,0},{9,1},... | collective-permute-start | bytes 786440 | tf_op jit(solution)/shard_map/ppermute | solution.py:492
  179.1 8.3 %collective-permute-start.17 = (bf16[256,512]{1,0:T(8,128)(2,1)S(1)}, bf16[256,512]{1,0:T(8,128)(2,1)S(1)}, u32[]{:S(2)}, u32[]{:S(2)}) collective-permute-start(bf16[256,512]{1,0:T(8,128)(2,1)S(1)} %collective-permute-done.16.refs_8_), channel_id=1, source_target_pairs={{0,16},{1,17},{2,18},{3,19},{4,20},{5,21},{6,22},{7,23},{8,24},{9,... | collective-permute-start | bytes 786440 | tf_op jit(solution)/shard_map/ppermute | solution.py:492
  187.5 10.3 %collective-permute-start = (f32[2]{0:T(128)S(1)}, f32[2]{0:T(128)S(1)}, u32[]{:S(2)}, u32[]{:S(2)}) collective-permute-start(f32[2]{0:T(128)S(1)} %copy-done.10), channel_id=1, source_target_pairs={{0,1},{1,0},{2,3},{3,2},{4,5},{5,4},{6,7},{7,6},{8,9},{9,8},{10,11... | collective-permute-start | bytes 32 | tf_op jit(solution)/shard_map/ppermute | solution.py:492
  189.4 8.5 %collective-permute-start.1 = (f32[4]{0:T(128)S(1)}, f32[4]{0:T(128)S(1)}, u32[]{:S(2)}, u32[]{:S(2)}) collective-permute-start(f32[4]{0:T(128)S(1)} %copy-done.11), channel_id=1, source_target_pairs={{0,1},{1,0},{2,3},{3,2},{4,5},{5,4},{6,7},{7,6},{8,9},{9,8},{10,11... | collective-permute-start | bytes 56 | tf_op jit(solution)/shard_map/ppermute | solution.py:492
  204.7 13.0 %collective-permute-start.32 = (bf16[128,512]{1,0:T(8,128)(2,1)S(1)}, bf16[128,512]{1,0:T(8,128)(2,1)S(1)}, u32[]{:S(2)}, u32[]{:S(2)}) collective-permute-start(bf16[128,512]{1,0:T(8,128)(2,1)S(1)} %get-tuple-element.23), channel_id=1, source_target_pairs={{0,8},{1,9},{2,10},{3,11},{4,12},{5,13},{6,14},{7,15},{8,0},{9,1},... | collective-permute-start | bytes 393224 | tf_op jit(solution)/shard_map/ppermute | solution.py:492
  207.7 10.0 %collective-permute-start.33 = (bf16[128,512]{1,0:T(8,128)(2,1)S(1)}, bf16[128,512]{1,0:T(8,128)(2,1)S(1)}, u32[]{:S(2)}, u32[]{:S(2)}) collective-permute-start(bf16[128,512]{1,0:T(8,128)(2,1)S(1)} %get-tuple-element.24), channel_id=1, source_target_pairs={{0,12},{1,13},{2,14},{3,15},{4,8},{5,9},{6,10},{7,11},{8,4},{9,5},... | collective-permute-start | bytes 393224 | tf_op jit(solution)/shard_map/ppermute | solution.py:492
  221.4 34.1 %collective-permute-start.35 = (bf16[128,2048]{1,0:T(8,128)(2,1)S(1)}, bf16[128,2048]{1,0:T(8,128)(2,1)S(1)}, u32[]{:S(2)}, u32[]{:S(2)}) collective-permute-start(bf16[128,2048]{1,0:T(8,128)(2,1)S(1)} %output.5), channel_id=1, source_target_pairs={{0,2},{1,3},{2,0},{3,1},{4,6},{5,7},{6,4},{7,5},{8,10},{9,11},{10,... | collective-permute-start | bytes 1572872 | tf_op jit(solution)/shard_map/ppermute | solution.py:492
  226.7 28.9 %collective-permute-start.34 = (bf16[128,2048]{1,0:T(8,128)(2,1)S(1)}, bf16[128,2048]{1,0:T(8,128)(2,1)S(1)}, u32[]{:S(2)}, u32[]{:S(2)}) collective-permute-start(bf16[128,2048]{1,0:T(8,128)(2,1)S(1)} %output.4), channel_id=1, source_target_pairs={{0,2},{1,3},{2,0},{3,1},{4,6},{5,7},{6,4},{7,5},{8,10},{9,11},{10,... | collective-permute-start | bytes 1572872 | tf_op jit(solution)/shard_map/ppermute | solution.py:492
  236.9 12.0 %collective-permute-start.27 = (bf16[128,512]{1,0:T(8,128)(2,1)S(1)}, bf16[128,512]{1,0:T(8,128)(2,1)S(1)}, u32[]{:S(2)}, u32[]{:S(2)}) collective-permute-start(bf16[128,512]{1,0:T(8,128)(2,1)S(1)} %get-tuple-element.19), channel_id=1, source_target_pairs={{0,8},{1,9},{2,10},{3,11},{4,12},{5,13},{6,14},{7,15},{8,0},{9,1},... | collective-permute-start | bytes 393224 | tf_op jit(solution)/shard_map/ppermute | solution.py:492
  237.9 11.0 %collective-permute-start.28 = (bf16[128,512]{1,0:T(8,128)(2,1)S(1)}, bf16[128,512]{1,0:T(8,128)(2,1)S(1)}, u32[]{:S(2)}, u32[]{:S(2)}) collective-permute-start(bf16[128,512]{1,0:T(8,128)(2,1)S(1)} %get-tuple-element.20), channel_id=1, source_target_pairs={{0,12},{1,13},{2,14},{3,15},{4,8},{5,9},{6,10},{7,11},{8,4},{9,5},... | collective-permute-start | bytes 393224 | tf_op jit(solution)/shard_map/ppermute | solution.py:492
  (37 other events, 449.5 us)

commit v3 on v2

--- a/solution.py
+++ b/solution.py
@@ -295,33 +295,49 @@
 ROWS = 256
 
 
-def project_early(place, acts, own, pieces, split):
+def project_sum(place, acts, sums, chunks, split):
     rows = acts.shape[0]
-    wide, cols = own.shape
-
-    def kernel(place_ref, a0, a1, own_ref, *refs):
-        (*ws, left, right, scratch) = refs
+    cols = chunks[0][1][0].shape[1]
+    wide = sum(p.shape[0] for p in chunks[0][1])
+    widths = (split, cols - split)
+
+    def kernel(place_ref, *refs):
+        (*refs, left, right, scratch) = refs
+        before = (refs.pop(0), refs.pop(0)) if sums else None
+        parts = []
+        for _, pieces in chunks:
+            a, ws = refs[0], refs[1 : 1 + len(pieces)]
+            refs = refs[1 + len(pieces) :]
+            parts.append((a, ws))
 
         @pl.when(pl.program_id(0) == 0)
         def _():
-            assemble(scratch, 0, ws, place_ref[3], place_ref[2])
-
-        total = jnp.dot(a0[...], own_ref[...], preferred_element_type=F32)
-        total = total + jnp.dot(a1[...], scratch[...], preferred_element_type=F32)
-        left[...] = total[:, :split]
-        right[...] = total[:, split:]
-
-    def chunk_of(k):
-        return pl.BlockSpec((ROWS, wide), lambda m, at: (m, at[0] ^ k))
-
-    whole = [pl.BlockSpec(p.shape, lambda m, at: (0, 0)) for p in (own, *pieces)]
-    widths = (split, cols - split)
+            for _, ws in parts:
+                if len(ws) > 1:
+                    assemble(scratch, 0, ws, place_ref[3], place_ref[2])
+
+        total = None
+        for a, ws in parts:
+            w = scratch[...] if len(ws) > 1 else ws[0][...]
+            part = jnp.dot(a[...], w, preferred_element_type=F32)
+            total = part if total is None else total + part
+        for out, lo, hi, j in ((left, 0, split, 0), (right, split, cols, 1)):
+            out[...] = total[:, lo:hi] + before[j][...] if before else total[:, lo:hi]
+
+    in_specs, operands = [], []
+    if sums:
+        in_specs += [pl.BlockSpec((ROWS, w), lambda m, at: (m, 0)) for w in widths]
+        operands += sums
+    for k, pieces in chunks:
+        in_specs.append(pl.BlockSpec((ROWS, wide), lambda m, at, k=k: (m, at[0] ^ k)))
+        in_specs += [pl.BlockSpec(p.shape, lambda m, at: (0, 0)) for p in pieces]
+        operands += [acts, *pieces]
     return pl.pallas_call(
         kernel,
         grid_spec=pltpu.PrefetchScalarGridSpec(
             num_scalar_prefetch=1,
             grid=(rows // ROWS,),
-            in_specs=[chunk_of(0), chunk_of(1), *whole],
+            in_specs=in_specs,
             out_specs=[pl.BlockSpec((ROWS, w), lambda m, at: (m, 0)) for w in widths],
             scratch_shapes=[pltpu.VMEM((wide, cols), BF)],
         ),
@@ -330,30 +346,28 @@
             dimension_semantics=("arbitrary",), vmem_limit_bytes=26 * 2**20
         ),
         cost_estimate=pl.CostEstimate(
-            flops=4 * rows * wide * cols, bytes_accessed=rows * cols * 8, transcendentals=0
+            flops=2 * rows * wide * cols * len(chunks),
+            bytes_accessed=rows * cols * 4,
+            transcendentals=0,
         ),
         name="project",
-    )(place, acts, acts, own, *pieces)
-
-
-def project_rest(place, early, late, acc, chunks, begin, cols):
-    wide = sum(p.shape[0] for p in chunks[0][0])
-    steps = early.shape[0] // ROWS
-    order = sorted(chunks)
-    counts = [len(chunks[k][0]) for k in order]
-
-    def kernel(place_ref, acc_ref, e2, e3, *refs):
-        acts = refs[: len(order)]
-        refs = refs[len(order) :]
-        out, scratch = refs[-2], refs[-1]
+    )(place, *operands)
+
+
+def project_rest(place, early, late, acc_early, acc_late, third, second, begin):
+    rows, cols = acc_early.shape
+    wide = sum(p.shape[0] for p in third)
+    steps = rows // ROWS
+
+    def kernel(place_ref, acc_e, acc_l, e2, l2, l3, *refs):
+        (*ws, out, scratch) = refs
         m = pl.program_id(0)
 
         @pl.when(m == 0)
         def _():
-            at = 0
-            for j, n in enumerate(counts):
-                assemble(scratch, j * wide, refs[at : at + n], place_ref[3], place_ref[2])
-                at += n
+            n = len(second)
+            assemble(scratch, 0, ws[:n], place_ref[3], place_ref[2])
+            assemble(scratch, wide, ws[n:], place_ref[3], place_ref[2])
 
         def part(a, j):
             return jnp.dot(
@@ -362,36 +376,27 @@
 
         @pl.when(m < steps)
         def _():
-            out[...] = (acc_ref[...] + part(e2, 2) + part(e3, 3)).astype(BF)
+            out[...] = (acc_e[...] + part(e2, 0)).astype(BF)
 
         @pl.when(m == steps)
         def _():
-            total = part(acts[0], 0)
-            for j in range(1, len(order)):
-                total = total + part(acts[j], j)
-            out[...] = total.astype(BF)
-
-    def early_of(k):
-        return pl.BlockSpec(
-            (ROWS, wide), lambda m, at: (jnp.minimum(m, steps - 1), at[0] ^ k)
-        )
-
-    in_specs = [pl.BlockSpec((ROWS, cols), lambda m, at: (jnp.minimum(m, steps - 1), 0))]
-    in_specs += [early_of(2), early_of(3)]
-    in_specs += [pl.BlockSpec((ROWS, wide), lambda m, at, k=k: (0, at[0] ^ k)) for k in order]
-    operands = [acc, early, early] + [late] * len(order)
-    for k in order:
-        pieces, start = chunks[k]
-        for p in pieces:
-            in_specs.append(
-                pl.BlockSpec(
-                    (pl.Element(p.shape[0]), pl.Element(cols)),
-                    lambda m, at, lo=begin - start: (0, lo),
-                )
-                if p.shape[1] != cols
-                else pl.BlockSpec(p.shape, lambda m, at: (0, 0))
-            )
-            operands.append(p)
+            out[...] = (acc_l[...] + part(l2, 0) + part(l3, 1)).astype(BF)
+
+    def clamped(m):
+        return jnp.minimum(m, steps - 1)
+
+    in_specs = [
+        pl.BlockSpec((ROWS, cols), lambda m, at: (clamped(m), 0)),
+        pl.BlockSpec((ROWS, cols), lambda m, at: (0, 0)),
+        pl.BlockSpec((ROWS, wide), lambda m, at: (clamped(m), at[0] ^ 2)),
+        pl.BlockSpec((ROWS, wide), lambda m, at: (0, at[0] ^ 2)),
+        pl.BlockSpec((ROWS, wide), lambda m, at: (0, at[0] ^ 3)),
+    ]
+    in_specs += [pl.BlockSpec(p.shape, lambda m, at: (0, 0)) for p in second]
+    in_specs += [
+        pl.BlockSpec((pl.Element(p.shape[0]), pl.Element(cols)), lambda m, at: (0, begin))
+        for p in third
+    ]
     return pl.pallas_call(
         kernel,
         grid_spec=pltpu.PrefetchScalarGridSpec(
@@ -399,19 +404,19 @@
             grid=(steps + 1,),
             in_specs=in_specs,
             out_specs=pl.BlockSpec((ROWS, cols), lambda m, at: (m, 0)),
-            scratch_shapes=[pltpu.VMEM((len(order) * wide, cols), BF)],
-        ),
-        out_shape=jax.ShapeDtypeStruct((early.shape[0] + late.shape[0], cols), BF),
+            scratch_shapes=[pltpu.VMEM((2 * wide, cols), BF)],
+        ),
+        out_shape=jax.ShapeDtypeStruct((rows + late.shape[0], cols), BF),
         compiler_params=pltpu.CompilerParams(
-            dimension_semantics=("arbitrary",), vmem_limit_bytes=36 * 2**20
+            dimension_semantics=("arbitrary",), vmem_limit_bytes=26 * 2**20
         ),
         cost_estimate=pl.CostEstimate(
-            flops=2 * (2 * early.shape[0] + 4 * late.shape[0]) * wide * cols,
-            bytes_accessed=16 * 2**20,
+            flops=3 * (rows + late.shape[0]) * wide * cols,
+            bytes_accessed=8 * 2**20,
             transcendentals=0,
         ),
         name="project",
-    )(place, *operands)
+    )(place, acc_early, acc_late, early, late, late, *second, *third)
 
 
 def output_projection(place, heads, weights, first, count, kind):
@@ -565,13 +570,13 @@
     w2a = chunk(jnp.concatenate([four[:, : 2 * VDIM], kv], axis=1), 2)
     w2b = chunk(four[:, 2 * VDIM :], 2)
     split = 3 * VDIM
-    acc_kv, acc_q = project_early(place, early, own, w1, split)
-    every = {0: ([own], 0), 1: (w1, 0), 3: (w3, 0)}
-    kv_own = project_rest(place, early, late, acc_kv, every | {2: (w2a, 0)}, 0, split)
+    first = [(0, [own]), (1, w1)]
+    sums = project_sum(place, early, None, first, split)
+    ends = project_sum(place, late, None, first, split)
+    sums = project_sum(place, early, sums, [(3, w3)], split)
+    kv_own = project_rest(place, early, late, sums[0], ends[0], w3, w2a, 0)
     kv_oth = over_core(kv_own)
-    queries = project_rest(
-        place, early, late, acc_q, every | {2: (w2b, split)}, split, own.shape[1] - split
-    )
+    queries = project_rest(place, early, late, sums[1], ends[1], w3, w2b, split)
 
     scalars = (lam, over_core(lam), sink, over_core(sink))
     gain = output_norm_gain.reshape(1, VDIM)

time: 258 us -> 264 us (1.023)
  waiting for transfers between devices: 127 us -> 147 us
  starting transfers between devices: 54.6 us -> 39.3 us
  other arithmetic: 12.4 us -> 18 us
    ppermute x36, waiting for transfers between devices: 127 us -> 147 us  [send(): return lax.ppermute(value, AXES, pairs)]
    ppermute x36, starting transfers between devices: 54.6 us -> 39.3 us  [send(): return lax.ppermute(value, AXES, pairs)]
    pallas_call x1 -> x3, Pallas kernels: 5.81 us -> 11.6 us  [project_sum(): pl.pallas_call(kernel, grid_spec=pltpu.PrefetchScalarGridSpec(num_scalar_...]
    pallas_call x2, Pallas kernels: 13.5 us -> 8.2 us  [project_rest(): pl.pallas_call(kernel, grid_spec=pltpu.PrefetchScalarGridSpec(num_scalar_...]
    unnamed x69 -> x73, local copies, waits for them, and re-layouts: 10.2 us -> 6.33 us
  transfers between devices with their start and end apart: 36 -> 36, of which waited for: 15 -> 16; matrix products, arithmetic and copies ran while one was open for 6% -> 8% of each run, Pallas kernels for 17% -> 16%
where the time goes in v3:
time: 264 us
  waiting for transfers between devices  147 us (56%)
  Pallas kernels  44.6 us (17%)
  starting transfers between devices  39.3 us (15%)
  other arithmetic  18 us (7%)
  local copies, waits for them, and re-layouts  13.6 us (5%)
    ppermute x36, waiting for transfers between devices, send(): return lax.ppermute(value, AXES, pairs)  147 us
    ppermute x36, starting transfers between devices, send(): return lax.ppermute(value, AXES, pairs)  39.3 us
    pallas_call x2, Pallas kernels, attention(): pl.pallas_call(kernel, grid=(sp // 2,), in_specs=[smem] * 5 + [pl.BlockSp...  13.4 us
    pallas_call x3, Pallas kernels, project_sum(): pl.pallas_call(kernel, grid_spec=pltpu.PrefetchScalarGridSpec(num_scalar_...  11.6 us
    pallas_call x3, Pallas kernels, output_projection(): pl.pallas_call(kernel, grid=(count,), in_specs=in_specs, out_specs=pl.Blo...  11.5 us
    pallas_call x2, Pallas kernels, project_rest(): pl.pallas_call(kernel, grid_spec=pltpu.PrefetchScalarGridSpec(num_scalar_...  8.2 us
    unnamed x73, local copies, waits for them, and re-layouts  6.33 us
  transfers between devices with their start and end apart: 36, of which 16 were waited for; matrix products, arithmetic and copies ran while one was open for 8% of the time, Pallas kernels for 16%

profile of v3, /device:TPU:0, one launch (start us, length us, event | category | flops | bytes accessed | tf_op | source)
XLA Modules:
  0.0 263.7 jit_solution(13267632170501635744)
XLA Ops:
  1.7 3.0 %constant_dynamic-update-slice_fusion.5 = (bf16[768,4096]{1,0:T(8,128)(2,1)}, bf16[128,4096]{1,0:T(8,128)(2,1)}) fusion(f32[4096]{0:T(1024)} %param.13, f32[128]{0:T(128)S(1)} %add_rsqrt_fusion, bf16[128,4096]{1,0:T(8,128)(2,1)} %param.12), kind=kLoop, calls=%fused_computation.37 | loop fusion | flops 2097151 | bytes 3162624
  4.7 3.1 %collective-permute-start.2 = (bf16[128,4096]{1,0:T(8,128)(2,1)}, bf16[128,4096]{1,0:T(8,128)(2,1)}, u32[]{:S(2)}, u32[]{:S(2)}) collective-permute-start(bf16[128,4096]{1,0:T(8,128)(2,1)} %get-tuple-element.36), channel_id=1, source_target_pairs={{0,4},{1,5},{2,6},{3,7},{4,0},{5,1},{6,2},{7,3},{8,12},{9,13},{10,... | collective-permute-start | bytes 3145736 | tf_op jit(solution)/shard_map/ppermute | solution.py:497
  17.4 3.8 %collective-permute-start.9 = (bf16[1024,1024]{1,0:T(8,128)(2,1)}, bf16[1024,1024]{1,0:T(8,128)(2,1)}, u32[]{:S(2)}, u32[]{:S(2)}) collective-permute-start(bf16[1024,1024]{1,0:T(8,128)(2,1)} %pad_maximum_fusion.1), channel_id=1, source_target_pairs={{0,1},{2,3},{4,5},{6,7},{9,8},{11,10},{13,12},{15,14},{16,17},{18,... | collective-permute-start | bytes 6291464 | tf_op jit(solution)/shard_map/ppermute | solution.py:497
  21.2 2.0 dynamic-slice_bitcast_fusion.3
  34.9 18.5 %collective-permute-done.22.refs_0_ = bf16[256,768]{1,0:T(8,128)(2,1)S(1)} collective-permute-done((bf16[256,768]{1,0:T(8,128)(2,1)S(1)}, bf16[256,768]{1,0:T(8,128)(2,1)S(1)}, u32[]{:S(2)}, u32[]{:S(2)}) %collective-permute-start.22) | collective-permute-done | bytes 393248 | tf_op jit(solution)/shard_map/ppermute | solution.py:497
  55.0 7.3 %collective-permute-done.23.refs_1_ = bf16[256,768]{1,0:T(8,128)(2,1)S(1)} collective-permute-done((bf16[256,768]{1,0:T(8,128)(2,1)S(1)}, bf16[256,768]{1,0:T(8,128)(2,1)S(1)}, u32[]{:S(2)}, u32[]{:S(2)}) %collective-permute-start.23) | collective-permute-done | bytes 393248 | tf_op jit(solution)/shard_map/ppermute | solution.py:497
  63.2 2.4 collective-permute-start.14
  65.6 12.3 %collective-permute-done.5 = bf16[128,4096]{1,0:T(8,128)(2,1)S(1)} collective-permute-done((bf16[128,4096]{1,0:T(8,128)(2,1)}, bf16[128,4096]{1,0:T(8,128)(2,1)S(1)}, u32[]{:S(2)}, u32[]{:S(2)}) %collective-permute-start.5) | collective-permute-done | bytes 1048608 | tf_op jit(solution)/shard_map/ppermute | solution.py:497
  81.1 21.7 %collective-permute-done.11.refs_3_ = bf16[256,1280]{1,0:T(8,128)(2,1)S(1)} collective-permute-done((bf16[256,1280]{1,0:T(8,128)(2,1)S(1)}, bf16[256,1280]{1,0:T(8,128)(2,1)S(1)}, u32[]{:S(2)}, u32[]{:S(2)}) %collective-permute-start.11) | collective-permute-done | bytes 655392 | tf_op jit(solution)/shard_map/ppermute | solution.py:497
  107.2 13.3 %collective-permute-done.12.refs_4_ = bf16[256,1280]{1,0:T(8,128)(2,1)S(1)} collective-permute-done((bf16[256,1280]{1,0:T(8,128)(2,1)S(1)}, bf16[256,1280]{1,0:T(8,128)(2,1)S(1)}, u32[]{:S(2)}, u32[]{:S(2)}) %collective-permute-start.12) | collective-permute-done | bytes 655392 | tf_op jit(solution)/shard_map/ppermute | solution.py:497
  122.1 11.9 %collective-permute-done.15.refs_4_ = bf16[256,1280]{1,0:T(8,128)(2,1)S(1)} collective-permute-done((bf16[256,1280]{1,0:T(8,128)(2,1)S(1)}, bf16[256,1280]{1,0:T(8,128)(2,1)S(1)}, u32[]{:S(2)}, u32[]{:S(2)}) %collective-permute-start.15) | collective-permute-done | bytes 655392 | tf_op jit(solution)/shard_map/ppermute | solution.py:497
  135.8 8.8 %collective-permute-done.8 = bf16[128,4096]{1,0:T(8,128)(2,1)S(1)} collective-permute-done((bf16[128,4096]{1,0:T(8,128)(2,1)S(1)}, bf16[128,4096]{1,0:T(8,128)(2,1)S(1)}, u32[]{:S(2)}, u32[]{:S(2)}) %collective-permute-start.8) | collective-permute-done | bytes 1048608 | tf_op jit(solution)/shard_map/ppermute | solution.py:497
  147.5 5.8 %project.5 = (f32[768,768]{1,0:T(8,128)S(1)}, f32[768,512]{1,0:T(8,128)S(1)}) custom-call(s32[4]{0:T(128)S(1)} %pad_add_fusion.place_ref.refs_0_, bf16[768,4096]{1,0:T(8,128)(2,1)S(1)} %constant_dynamic-update-slice_fusion.refs_0_.refs_2_.e2, bf16[1024,1280]{1,0:T(8,128)(2,1)S(1)} %pad_maximum_fusion.refs_1_, ...), custom_call_target="tpu_custom_call" | custom-call | flops 4026531840 | bytes 3932160 | tf_op jit(solution)/shard_map/project/pallas_call | solution.py:335
  153.4 3.5 %project.6 = (f32[768,768]{1,0:T(8,128)S(1)}, f32[768,512]{1,0:T(8,128)S(1)}) custom-call(s32[4]{0:T(128)S(1)} %pad_add_fusion.place_ref.refs_0_, f32[768,768]{1,0:T(8,128)S(1)} %get-tuple-element.19.refs_0_, f32[768,512]{1,0:T(8,128)S(1)} %get-tuple-element.20.refs_1_, bf16[768,4096]{1,0:T(8,128)(2,1)S(1)} %constant_dynamic-update-slice_fusion.refs_0_.refs_2_.e2, ...), custom_call_target="tpu_custom_call" | custom-call | flops 2013265920 | bytes 3932160 | tf_op jit(solution)/shard_map/project/pallas_call | solution.py:335
  156.9 11.2 %collective-permute-done.18 = bf16[128,4096]{1,0:T(8,128)(2,1)} collective-permute-done((bf16[128,4096]{1,0:T(8,128)(2,1)}, bf16[128,4096]{1,0:T(8,128)(2,1)}, u32[]{:S(2)}, u32[]{:S(2)}) %collective-permute-start.18) | collective-permute-done | bytes 1048608 | tf_op jit(solution)/shard_map/ppermute | solution.py:497
  168.1 1.7 pad_maximum_fusion.3.refs_0_.refs_2_.l2.l3
  169.9 2.3 project.7
  174.0 5.0 %project.9.refs_7_ = bf16[1024,768]{1,0:T(8,128)(2,1)S(1)} custom-call(s32[4]{0:T(128)S(1)} %pad_add_fusion.place_ref.refs_0_, f32[768,768]{1,0:T(8,128)S(1)} %copy-done.15, f32[256,768]{1,0:T(8,128)S(1)} %get-tuple-element.24.acc_l, bf16[768,4096]{1,0:T(8,128)(2,1)S(1)} %constant_dynamic-update-slice_fusion.refs_0_.refs_2_.e2, ...), custom_call_target="tpu_custom_call" | custom-call | flops 2415919104 | bytes 8388608 | tf_op jit(solution)/shard_map/project/pallas_call | solution.py:400
  179.2 15.1 %collective-permute-done.19.refs_0_ = bf16[256,512]{1,0:T(8,128)(2,1)S(1)} collective-permute-done((bf16[256,512]{1,0:T(8,128)(2,1)S(1)}, bf16[256,512]{1,0:T(8,128)(2,1)S(1)}, u32[]{:S(2)}, u32[]{:S(2)}) %collective-permute-start.19) | collective-permute-done | bytes 262176 | tf_op jit(solution)/shard_map/ppermute | solution.py:497
  195.8 6.8 %collective-permute-done.20.refs_1_ = bf16[256,512]{1,0:T(8,128)(2,1)S(1)} collective-permute-done((bf16[256,512]{1,0:T(8,128)(2,1)S(1)}, bf16[256,512]{1,0:T(8,128)(2,1)S(1)}, u32[]{:S(2)}, u32[]{:S(2)}) %collective-permute-start.20) | collective-permute-done | bytes 262176 | tf_op jit(solution)/shard_map/ppermute | solution.py:497
  204.7 3.2 %project.8.refs_6_ = bf16[1024,512]{1,0:T(8,128)(2,1)S(1)} custom-call(s32[4]{0:T(128)S(1)} %pad_add_fusion.place_ref.refs_0_, f32[768,512]{1,0:T(8,128)S(1)} %copy-done.17, f32[256,512]{1,0:T(8,128)S(1)} %get-tuple-element.22.acc_l, bf16[768,4096]{1,0:T(8,128)(2,1)S(1)} %constant_dynamic-update-slice_fusion.refs_0_.refs_2_.e2, ...), custom_call_target="tpu_custom_call" | custom-call | flops 1610612736 | bytes 8388608 | tf_op jit(solution)/shard_map/project/pallas_call | solution.py:400
  208.0 6.7 %attend.3 = (bf16[128,512]{1,0:T(8,128)(2,1)S(1)}, bf16[128,512]{1,0:T(8,128)(2,1)S(1)}, bf16[128,512]{1,0:T(8,128)(2,1)S(1)}, bf16[128,512]{1,0:T(8,128)(2,1)S(1)}) custom-call(s32[4]{0:T(128)S(1)} %pad_add_fusion.place_ref.refs_0_, f32[2]{0:T(128)S(1)} %copy-done.19, f32[2]{0:T(128)S(1)} %collective-permute-done.refs_2_, f32[4]{0:T(128)S(1)} %copy-done.20, ...), custom_call_target="tpu_custom_call" | custom-call | flops 1610612736 | bytes 4194304 | tf_op jit(solution)/shard_map/attend/pallas_call | solution.py:261
  216.5 2.6 collective-permute-start.33
  219.1 2.7 %collective-permute-done.31.refs_1_ = bf16[128,512]{1,0:T(8,128)(2,1)S(1)} collective-permute-done((bf16[128,512]{1,0:T(8,128)(2,1)S(1)}, bf16[128,512]{1,0:T(8,128)(2,1)S(1)}, u32[]{:S(2)}, u32[]{:S(2)}) %collective-permute-start.31) | collective-permute-done | bytes 131104 | tf_op jit(solution)/shard_map/ppermute | solution.py:497
  221.8 5.9 %collective-permute-done.32.refs_2_ = bf16[128,512]{1,0:T(8,128)(2,1)S(1)} collective-permute-done((bf16[128,512]{1,0:T(8,128)(2,1)S(1)}, bf16[128,512]{1,0:T(8,128)(2,1)S(1)}, u32[]{:S(2)}, u32[]{:S(2)}) %collective-permute-start.32) | collective-permute-done | bytes 131104 | tf_op jit(solution)/shard_map/ppermute | solution.py:497
  227.7 3.0 %output.5 = bf16[128,2048]{1,0:T(8,128)(2,1)S(1)} custom-call(s32[4]{0:T(128)S(1)} %pad_add_fusion.place_ref.refs_0_, bf16[128,512]{1,0:T(8,128)(2,1)S(1)} %get-tuple-element.29.refs_0_, bf16[128,512]{1,0:T(8,128)(2,1)S(1)} %collective-permute-done.31.refs_1_, bf16[128,512]{1,0:T(8,128)(2,1)S(1)} %collective-permute-done.32.refs_2_, ...), custom_call_target="tpu_custom_call" | custom-call | flops 1073741824 | bytes 8388608 | tf_op jit(solution)/shard_map/output/pallas_call | solution.py:452
  232.3 3.0 %output.4 = bf16[128,2048]{1,0:T(8,128)(2,1)S(1)} custom-call(s32[4]{0:T(128)S(1)} %pad_add_fusion.place_ref.refs_0_, bf16[128,512]{1,0:T(8,128)(2,1)S(1)} %get-tuple-element.29.refs_0_, bf16[128,512]{1,0:T(8,128)(2,1)S(1)} %collective-permute-done.31.refs_1_, bf16[128,512]{1,0:T(8,128)(2,1)S(1)} %collective-permute-done.32.refs_2_, ...), custom_call_target="tpu_custom_call" | custom-call | flops 1073741824 | bytes 8388608 | tf_op jit(solution)/shard_map/output/pallas_call | solution.py:452
  235.9 6.7 %attend.2 = (bf16[128,512]{1,0:T(8,128)(2,1)S(1)}, bf16[128,512]{1,0:T(8,128)(2,1)S(1)}, bf16[128,512]{1,0:T(8,128)(2,1)S(1)}, bf16[128,512]{1,0:T(8,128)(2,1)S(1)}) custom-call(s32[4]{0:T(128)S(1)} %pad_add_fusion.place_ref.refs_0_, f32[2]{0:T(128)S(1)} %copy-done.19, f32[2]{0:T(128)S(1)} %collective-permute-done.refs_2_, f32[4]{0:T(128)S(1)} %copy-done.20, ...), custom_call_target="tpu_custom_call" | custom-call | flops 1610612736 | bytes 4194304 | tf_op jit(solution)/shard_map/attend/pallas_call | solution.py:261
  242.6 2.8 %collective-permute-start.26 = (bf16[128,512]{1,0:T(8,128)(2,1)S(1)}, bf16[128,512]{1,0:T(8,128)(2,1)S(1)}, u32[]{:S(2)}, u32[]{:S(2)}) collective-permute-start(bf16[128,512]{1,0:T(8,128)(2,1)S(1)} %get-tuple-element.26), channel_id=1, source_target_pairs={{0,4},{1,5},{2,6},{3,7},{4,0},{5,1},{6,2},{7,3},{8,12},{9,13},{10,... | collective-permute-start | bytes 393224 | tf_op jit(solution)/shard_map/ppermute | solution.py:497
  245.4 2.4 collective-permute-start.28
  249.3 7.6 %collective-permute-done.27.refs_2_ = bf16[128,512]{1,0:T(8,128)(2,1)S(1)} collective-permute-done((bf16[128,512]{1,0:T(8,128)(2,1)S(1)}, bf16[128,512]{1,0:T(8,128)(2,1)S(1)}, u32[]{:S(2)}, u32[]{:S(2)}) %collective-permute-start.27) | collective-permute-done | bytes 131104 | tf_op jit(solution)/shard_map/ppermute | solution.py:497
  256.9 5.5 %output.3 = f32[128,4096]{1,0:T(8,128)S(1)} custom-call(s32[4]{0:T(128)S(1)} %pad_add_fusion.place_ref.refs_0_, bf16[128,512]{1,0:T(8,128)(2,1)S(1)} %get-tuple-element.25.refs_0_, bf16[128,512]{1,0:T(8,128)(2,1)S(1)} %collective-permute-done.26.refs_1_, bf16[128,512]{1,0:T(8,128)(2,1)S(1)} %collective-permute-done.27.refs_2_, ...), custom_call_target="tpu_custom_call" | custom-call | flops 2147483648 | bytes 16777216 | tf_op jit(solution)/shard_map/output/pallas_call | solution.py:452
  (160 shorter events, 51.2 us)
Async XLA Ops:
  4.7 26.5 %collective-permute-start.2 = (bf16[128,4096]{1,0:T(8,128)(2,1)}, bf16[128,4096]{1,0:T(8,128)(2,1)}, u32[]{:S(2)}, u32[]{:S(2)}) collective-permute-start(bf16[128,4096]{1,0:T(8,128)(2,1)} %get-tuple-element.36), channel_id=1, source_target_pairs={{0,4},{1,5},{2,6},{3,7},{4,0},{5,1},{6,2},{7,3},{8,12},{9,13},{10,... | collective-permute-start | bytes 3145736 | tf_op jit(solution)/shard_map/ppermute | solution.py:497
  7.8 24.3 %collective-permute-start.4 = (bf16[128,4096]{1,0:T(8,128)(2,1)}, bf16[128,4096]{1,0:T(8,128)(2,1)}, u32[]{:S(2)}, u32[]{:S(2)}) collective-permute-start(bf16[128,4096]{1,0:T(8,128)(2,1)} %get-tuple-element.36), channel_id=1, source_target_pairs={{4,8},{5,9},{6,10},{7,11},{8,4},{9,5},{10,6},{11,7},{20,24},{21,25... | collective-permute-start | bytes 3145736 | tf_op jit(solution)/shard_map/ppermute | solution.py:497
  9.4 70.2 %collective-permute-start.6 = (bf16[128,4096]{1,0:T(8,128)(2,1)}, bf16[128,4096]{1,0:T(8,128)(2,1)}, u32[]{:S(2)}, u32[]{:S(2)}) collective-permute-start(bf16[128,4096]{1,0:T(8,128)(2,1)} %get-tuple-element.36), channel_id=1, source_target_pairs={{0,2},{1,3},{2,0},{3,1},{4,6},{5,7},{6,4},{7,5},{8,10},{9,11},{10,... | collective-permute-start | bytes 3145736 | tf_op jit(solution)/shard_map/ppermute | solution.py:497
  14.4 12.4 %collective-permute-start.10 = (bf16[2,256,1024]{2,1,0:T(8,128)(2,1)}, bf16[2,256,1024]{2,1,0:T(8,128)(2,1)}, u32[]{:S(2)}, u32[]{:S(2)}) collective-permute-start(bf16[2,256,1024]{2,1,0:T(8,128)(2,1)} %pad_maximum_fusion.6), channel_id=1, source_target_pairs={{0,1},{1,0},{2,3},{3,2},{4,5},{5,4},{6,7},{7,6},{8,9},{9,8},{10,11... | collective-permute-start | bytes 3145736 | tf_op jit(solution)/shard_map/ppermute | solution.py:497
  17.4 87.6 %collective-permute-start.9 = (bf16[1024,1024]{1,0:T(8,128)(2,1)}, bf16[1024,1024]{1,0:T(8,128)(2,1)}, u32[]{:S(2)}, u32[]{:S(2)}) collective-permute-start(bf16[1024,1024]{1,0:T(8,128)(2,1)} %pad_maximum_fusion.1), channel_id=1, source_target_pairs={{0,1},{2,3},{4,5},{6,7},{9,8},{11,10},{13,12},{15,14},{16,17},{18,... | collective-permute-start | bytes 6291464 | tf_op jit(solution)/shard_map/ppermute | solution.py:497
  29.3 24.1 %collective-permute-start.22 = (bf16[256,768]{1,0:T(8,128)(2,1)S(1)}, bf16[256,768]{1,0:T(8,128)(2,1)S(1)}, u32[]{:S(2)}, u32[]{:S(2)}) collective-permute-start(bf16[256,768]{1,0:T(8,128)(2,1)S(1)} %pad_maximum_fusion.11), channel_id=1, source_target_pairs={{0,8},{1,9},{2,10},{3,11},{4,12},{5,13},{6,14},{7,15},{8,0},{9,1},... | collective-permute-start | bytes 1179656 | tf_op jit(solution)/shard_map/ppermute | solution.py:497
  31.3 31.9 %collective-permute-start.3 = (bf16[128,4096]{1,0:T(8,128)(2,1)}, bf16[128,4096]{1,0:T(8,128)(2,1)S(1)}, u32[]{:S(2)}, u32[]{:S(2)}) collective-permute-start(bf16[128,4096]{1,0:T(8,128)(2,1)} %collective-permute-done.2), channel_id=1, source_target_pairs={{4,8},{5,9},{6,10},{7,11},{8,4},{9,5},{10,6},{11,7},{20,24},{21,25... | collective-permute-start | bytes 3145736 | tf_op jit(solution)/shard_map/ppermute | solution.py:497
  32.1 45.8 %collective-permute-start.5 = (bf16[128,4096]{1,0:T(8,128)(2,1)}, bf16[128,4096]{1,0:T(8,128)(2,1)S(1)}, u32[]{:S(2)}, u32[]{:S(2)}) collective-permute-start(bf16[128,4096]{1,0:T(8,128)(2,1)} %collective-permute-done.4), channel_id=1, source_target_pairs={{4,0},{5,1},{6,2},{7,3},{8,12},{9,13},{10,14},{11,15},{20,16},{21,... | collective-permute-start | bytes 3145736 | tf_op jit(solution)/shard_map/ppermute | solution.py:497
  53.4 8.9 %collective-permute-start.23 = (bf16[256,768]{1,0:T(8,128)(2,1)S(1)}, bf16[256,768]{1,0:T(8,128)(2,1)S(1)}, u32[]{:S(2)}, u32[]{:S(2)}) collective-permute-start(bf16[256,768]{1,0:T(8,128)(2,1)S(1)} %collective-permute-done.22.refs_0_), channel_id=1, source_target_pairs={{0,16},{1,17},{2,18},{3,19},{4,20},{5,21},{6,22},{7,23},{8,24},{9,... | collective-permute-start | bytes 1179656 | tf_op jit(solution)/shard_map/ppermute | solution.py:497
  62.2 40.5 %collective-permute-start.11 = (bf16[256,1280]{1,0:T(8,128)(2,1)S(1)}, bf16[256,1280]{1,0:T(8,128)(2,1)S(1)}, u32[]{:S(2)}, u32[]{:S(2)}) collective-permute-start(bf16[256,1280]{1,0:T(8,128)(2,1)S(1)} %pad_maximum_fusion.8), channel_id=1, source_target_pairs={{0,4},{1,5},{2,6},{3,7},{4,0},{5,1},{6,2},{7,3},{8,12},{9,13},{10,... | collective-permute-start | bytes 1966088 | tf_op jit(solution)/shard_map/ppermute | solution.py:497
  63.2 39.6 %collective-permute-start.14 = (bf16[256,1280]{1,0:T(8,128)(2,1)S(1)}, bf16[256,1280]{1,0:T(8,128)(2,1)S(1)}, u32[]{:S(2)}, u32[]{:S(2)}) collective-permute-start(bf16[256,1280]{1,0:T(8,128)(2,1)S(1)} %pad_maximum_fusion.9), channel_id=1, source_target_pairs={{0,12},{1,13},{2,14},{3,15},{4,8},{5,9},{6,10},{7,11},{8,4},{9,5},... | collective-permute-start | bytes 1966088 | tf_op jit(solution)/shard_map/ppermute | solution.py:497
  77.9 26.5 %collective-permute-start.7 = (bf16[128,4096]{1,0:T(8,128)(2,1)}, bf16[128,4096]{1,0:T(8,128)(2,1)S(1)}, u32[]{:S(2)}, u32[]{:S(2)}) collective-permute-start(bf16[128,4096]{1,0:T(8,128)(2,1)} %collective-permute-done.2), channel_id=1, source_target_pairs={{0,2},{1,3},{2,0},{3,1},{4,6},{5,7},{6,4},{7,5},{8,10},{9,11},{10,... | collective-permute-start | bytes 3145736 | tf_op jit(solution)/shard_map/ppermute | solution.py:497
  79.6 139.5 %collective-permute-start.29 = (bf16[512,4096]{1,0:T(8,128)(2,1)S(1)}, bf16[512,4096]{1,0:T(8,128)(2,1)S(1)}, u32[]{:S(2)}, u32[]{:S(2)}) collective-permute-start(bf16[512,4096]{1,0:T(8,128)(2,1)S(1)} %copy-done), channel_id=1, source_target_pairs={{0,1},{1,0},{2,3},{3,2},{4,5},{5,4},{6,7},{7,6},{8,9},{9,8},{10,11... | collective-permute-start | bytes 12582920 | tf_op jit(solution)/shard_map/ppermute | solution.py:497
  102.8 116.3 %collective-permute-start.30 = (bf16[512,4096]{1,0:T(8,128)(2,1)S(1)}, bf16[512,4096]{1,0:T(8,128)(2,1)}, u32[]{:S(2)}, u32[]{:S(2)}) collective-permute-start(bf16[512,4096]{1,0:T(8,128)(2,1)S(1)} %copy-done.1), channel_id=1, source_target_pairs={{0,1},{1,0},{2,3},{3,2},{4,5},{5,4},{6,7},{7,6},{8,9},{9,8},{10,11... | collective-permute-start | bytes 12582920 | tf_op jit(solution)/shard_map/ppermute | solution.py:497
  102.8 17.7 %collective-permute-start.12 = (bf16[256,1280]{1,0:T(8,128)(2,1)S(1)}, bf16[256,1280]{1,0:T(8,128)(2,1)S(1)}, u32[]{:S(2)}, u32[]{:S(2)}) collective-permute-start(bf16[256,1280]{1,0:T(8,128)(2,1)S(1)} %collective-permute-done.11.refs_3_), channel_id=1, source_target_pairs={{0,16},{1,17},{2,18},{3,19},{4,20},{5,21},{6,22},{7,23},{8,24},{9,... | collective-permute-start | bytes 1966088 | tf_op jit(solution)/shard_map/ppermute | solution.py:497
  104.4 29.6 %collective-permute-start.15 = (bf16[256,1280]{1,0:T(8,128)(2,1)S(1)}, bf16[256,1280]{1,0:T(8,128)(2,1)S(1)}, u32[]{:S(2)}, u32[]{:S(2)}) collective-permute-start(bf16[256,1280]{1,0:T(8,128)(2,1)S(1)} %collective-permute-done.14.refs_3_), channel_id=1, source_target_pairs={{0,16},{1,17},{2,18},{3,19},{4,20},{5,21},{6,22},{7,23},{8,24},{9,... | collective-permute-start | bytes 1966088 | tf_op jit(solution)/shard_map/ppermute | solution.py:497
  105.0 29.1 %collective-permute-start.17 = (bf16[128,4096]{1,0:T(8,128)(2,1)S(1)}, bf16[128,4096]{1,0:T(8,128)(2,1)S(1)}, u32[]{:S(2)}, u32[]{:S(2)}) collective-permute-start(bf16[128,4096]{1,0:T(8,128)(2,1)S(1)} %collective-permute-done.3), channel_id=1, source_target_pairs={{4,0},{5,1},{6,2},{7,3},{8,12},{9,13},{10,14},{11,15},{20,16},{21,... | collective-permute-start | bytes 3145736 | tf_op jit(solution)/shard_map/ppermute | solution.py:497
  120.5 24.1 %collective-permute-start.8 = (bf16[128,4096]{1,0:T(8,128)(2,1)S(1)}, bf16[128,4096]{1,0:T(8,128)(2,1)S(1)}, u32[]{:S(2)}, u32[]{:S(2)}) collective-permute-start(bf16[128,4096]{1,0:T(8,128)(2,1)S(1)} %get-tuple-element.34), channel_id=1, source_target_pairs={{0,2},{1,3},{2,0},{3,1},{4,6},{5,7},{6,4},{7,5},{8,10},{9,11},{10,... | collective-permute-start | bytes 3145736 | tf_op jit(solution)/shard_map/ppermute | solution.py:497
  134.0 13.4 %collective-permute-start.13 = (bf16[512,1280]{1,0:T(8,128)(2,1)S(1)}, bf16[512,1280]{1,0:T(8,128)(2,1)S(1)}, u32[]{:S(2)}, u32[]{:S(2)}) collective-permute-start(bf16[512,1280]{1,0:T(8,128)(2,1)S(1)} %pad_maximum_fusion.4), channel_id=1, source_target_pairs={{0,1},{1,0},{2,3},{3,2},{4,5},{5,4},{6,7},{7,6},{8,9},{9,8},{10,11... | collective-permute-start | bytes 3932168 | tf_op jit(solution)/shard_map/ppermute | solution.py:497
  134.1 19.2 %collective-permute-start.16 = (bf16[512,1280]{1,0:T(8,128)(2,1)S(1)}, bf16[512,1280]{1,0:T(8,128)(2,1)S(1)}, u32[]{:S(2)}, u32[]{:S(2)}) collective-permute-start(bf16[512,1280]{1,0:T(8,128)(2,1)S(1)} %pad_maximum_fusion.5), channel_id=1, source_target_pairs={{0,1},{1,0},{2,3},{3,2},{4,5},{5,4},{6,7},{7,6},{8,9},{9,8},{10,11... | collective-permute-start | bytes 3932168 | tf_op jit(solution)/shard_map/ppermute | solution.py:497
  144.6 23.5 %collective-permute-start.18 = (bf16[128,4096]{1,0:T(8,128)(2,1)}, bf16[128,4096]{1,0:T(8,128)(2,1)}, u32[]{:S(2)}, u32[]{:S(2)}) collective-permute-start(bf16[128,4096]{1,0:T(8,128)(2,1)} %broadcast_select_fusion.1), channel_id=1, source_target_pairs={{0,2},{1,3},{2,0},{3,1},{4,6},{5,7},{6,4},{7,5},{8,10},{9,11},{10,... | collective-permute-start | bytes 3145736 | tf_op jit(solution)/shard_map/ppermute | solution.py:497
  147.4 24.9 %collective-permute-start.24 = (bf16[512,768]{1,0:T(8,128)(2,1)}, bf16[512,768]{1,0:T(8,128)(2,1)}, u32[]{:S(2)}, u32[]{:S(2)}) collective-permute-start(bf16[512,768]{1,0:T(8,128)(2,1)} %pad_maximum_fusion.7), channel_id=1, source_target_pairs={{0,1},{1,0},{2,3},{3,2},{4,5},{5,4},{6,7},{7,6},{8,9},{9,8},{10,11... | collective-permute-start | bytes 2359304 | tf_op jit(solution)/shard_map/ppermute | solution.py:497
  179.0 29.0 %collective-permute-start.25 = (bf16[1024,768]{1,0:T(8,128)(2,1)S(1)}, bf16[1024,768]{1,0:T(8,128)(2,1)S(1)}, u32[]{:S(2)}, u32[]{:S(2)}) collective-permute-start(bf16[1024,768]{1,0:T(8,128)(2,1)S(1)} %project.9.refs_7_), channel_id=1, source_target_pairs={{0,1},{1,0},{2,3},{3,2},{4,5},{5,4},{6,7},{7,6},{8,9},{9,8},{10,11... | collective-permute-start | bytes 4718600 | tf_op jit(solution)/shard_map/ppermute | solution.py:497
  179.1 15.2 %collective-permute-start.19 = (bf16[256,512]{1,0:T(8,128)(2,1)S(1)}, bf16[256,512]{1,0:T(8,128)(2,1)S(1)}, u32[]{:S(2)}, u32[]{:S(2)}) collective-permute-start(bf16[256,512]{1,0:T(8,128)(2,1)S(1)} %copy-done.32), channel_id=1, source_target_pairs={{0,8},{1,9},{2,10},{3,11},{4,12},{5,13},{6,14},{7,15},{8,0},{9,1},... | collective-permute-start | bytes 786440 | tf_op jit(solution)/shard_map/ppermute | solution.py:497
  194.3 8.3 %collective-permute-start.20 = (bf16[256,512]{1,0:T(8,128)(2,1)S(1)}, bf16[256,512]{1,0:T(8,128)(2,1)S(1)}, u32[]{:S(2)}, u32[]{:S(2)}) collective-permute-start(bf16[256,512]{1,0:T(8,128)(2,1)S(1)} %collective-permute-done.19.refs_0_), channel_id=1, source_target_pairs={{0,16},{1,17},{2,18},{3,19},{4,20},{5,21},{6,22},{7,23},{8,24},{9,... | collective-permute-start | bytes 786440 | tf_op jit(solution)/shard_map/ppermute | solution.py:497
  214.7 7.2 %collective-permute-start.31 = (bf16[128,512]{1,0:T(8,128)(2,1)S(1)}, bf16[128,512]{1,0:T(8,128)(2,1)S(1)}, u32[]{:S(2)}, u32[]{:S(2)}) collective-permute-start(bf16[128,512]{1,0:T(8,128)(2,1)S(1)} %get-tuple-element.30), channel_id=1, source_target_pairs={{0,4},{1,5},{2,6},{3,7},{4,0},{5,1},{6,2},{7,3},{8,12},{9,13},{10,... | collective-permute-start | bytes 393224 | tf_op jit(solution)/shard_map/ppermute | solution.py:497
  214.7 13.0 %collective-permute-start.32 = (bf16[128,512]{1,0:T(8,128)(2,1)S(1)}, bf16[128,512]{1,0:T(8,128)(2,1)S(1)}, u32[]{:S(2)}, u32[]{:S(2)}) collective-permute-start(bf16[128,512]{1,0:T(8,128)(2,1)S(1)} %get-tuple-element.31), channel_id=1, source_target_pairs={{0,8},{1,9},{2,10},{3,11},{4,12},{5,13},{6,14},{7,15},{8,0},{9,1},... | collective-permute-start | bytes 393224 | tf_op jit(solution)/shard_map/ppermute | solution.py:497
  216.5 11.3 %collective-permute-start.33 = (bf16[128,512]{1,0:T(8,128)(2,1)S(1)}, bf16[128,512]{1,0:T(8,128)(2,1)S(1)}, u32[]{:S(2)}, u32[]{:S(2)}) collective-permute-start(bf16[128,512]{1,0:T(8,128)(2,1)S(1)} %get-tuple-element.32), channel_id=1, source_target_pairs={{0,12},{1,13},{2,14},{3,15},{4,8},{5,9},{6,10},{7,11},{8,4},{9,5},... | collective-permute-start | bytes 393224 | tf_op jit(solution)/shard_map/ppermute | solution.py:497
  230.7 31.7 %collective-permute-start.35 = (bf16[128,2048]{1,0:T(8,128)(2,1)S(1)}, bf16[128,2048]{1,0:T(8,128)(2,1)S(1)}, u32[]{:S(2)}, u32[]{:S(2)}) collective-permute-start(bf16[128,2048]{1,0:T(8,128)(2,1)S(1)} %output.5), channel_id=1, source_target_pairs={{0,2},{1,3},{2,0},{3,1},{4,6},{5,7},{6,4},{7,5},{8,10},{9,11},{10,... | collective-permute-start | bytes 1572872 | tf_op jit(solution)/shard_map/ppermute | solution.py:497
  235.3 27.2 %collective-permute-start.34 = (bf16[128,2048]{1,0:T(8,128)(2,1)S(1)}, bf16[128,2048]{1,0:T(8,128)(2,1)S(1)}, u32[]{:S(2)}, u32[]{:S(2)}) collective-permute-start(bf16[128,2048]{1,0:T(8,128)(2,1)S(1)} %output.4), channel_id=1, source_target_pairs={{0,2},{1,3},{2,0},{3,1},{4,6},{5,7},{6,4},{7,5},{8,10},{9,11},{10,... | collective-permute-start | bytes 1572872 | tf_op jit(solution)/shard_map/ppermute | solution.py:497
  245.4 11.5 %collective-permute-start.27 = (bf16[128,512]{1,0:T(8,128)(2,1)S(1)}, bf16[128,512]{1,0:T(8,128)(2,1)S(1)}, u32[]{:S(2)}, u32[]{:S(2)}) collective-permute-start(bf16[128,512]{1,0:T(8,128)(2,1)S(1)} %get-tuple-element.27), channel_id=1, source_target_pairs={{0,8},{1,9},{2,10},{3,11},{4,12},{5,13},{6,14},{7,15},{8,0},{9,1},... | collective-permute-start | bytes 393224 | tf_op jit(solution)/shard_map/ppermute | solution.py:497
  245.4 11.5 %collective-permute-start.28 = (bf16[128,512]{1,0:T(8,128)(2,1)S(1)}, bf16[128,512]{1,0:T(8,128)(2,1)S(1)}, u32[]{:S(2)}, u32[]{:S(2)}) collective-permute-start(bf16[128,512]{1,0:T(8,128)(2,1)S(1)} %get-tuple-element.28), channel_id=1, source_target_pairs={{0,12},{1,13},{2,14},{3,15},{4,8},{5,9},{6,10},{7,11},{8,4},{9,5},... | collective-permute-start | bytes 393224 | tf_op jit(solution)/shard_map/ppermute | solution.py:497
  (39 other events, 566.3 us)

commit v4 on v3

--- a/solution.py
+++ b/solution.py
@@ -165,7 +165,7 @@
 
 
 def attention_kernel(
-    place, lam_a, lam_b, sink_a, sink_b, gain, q_ref, own_ref, oth_ref, *outs, nx, flip
+    place, lam_a, lam_b, sink_a, sink_b, gain, q_ref, own_ref, oth_ref, *outs, nx, flip, first
 ):
     step = pl.program_id(0)
     s, x, c = place[0], place[1], place[2]
@@ -178,7 +178,7 @@
         jnp.where(swapped, sink_b[(s % 2) * 2 + h], sink_a[(s % 2) * 2 + h]) for h in range(2)
     ]
     nt = (((1,), (1,)), ((), ()))
-    at = [((step * blocks + j) ^ s) * nx + (x ^ flip) for j in range(blocks)]
+    at = [((step * blocks + j + first) ^ s) * nx + (x ^ flip) for j in range(blocks)]
     places = [row_of(i, s, x, nx, rows) for i in at]
 
     def q_of(lanes):
@@ -249,28 +249,28 @@
                 out[:, VDIM + HEAD : VDIM + 2 * HEAD] = wins[2 * j + 1]
 
 
-def attention(place, scalars, gain, q, own, oth, sp, nx, flip):
+def attention(place, scalars, gain, q, own, oth, nx, flip, first, count):
     rows = own.shape[0]
     smem = pl.BlockSpec(memory_space=pltpu.SMEM)
     whole = pl.BlockSpec(own.shape, lambda i: (0, 0))
     block = pl.BlockSpec((WINDOW, 2 * VDIM), lambda i: (0, 0))
 
     def kernel(*refs):
-        attention_kernel(*refs, nx=nx, flip=flip)
+        attention_kernel(*refs, nx=nx, flip=flip, first=first)
 
     return pl.pallas_call(
         kernel,
-        grid=(sp // 2,),
+        grid=(count // 2,),
         in_specs=[smem] * 5
         + [pl.BlockSpec((1, VDIM), lambda i: (0, 0)), pl.BlockSpec(q.shape, lambda i: (0, 0))]
         + [whole, whole],
-        out_specs=[block] * sp,
-        out_shape=[jax.ShapeDtypeStruct((WINDOW, 2 * VDIM), BF)] * sp,
+        out_specs=[block] * count,
+        out_shape=[jax.ShapeDtypeStruct((WINDOW, 2 * VDIM), BF)] * count,
         compiler_params=pltpu.CompilerParams(
             dimension_semantics=("arbitrary",), vmem_limit_bytes=20 * 2**20
         ),
         cost_estimate=pl.CostEstimate(
-            flops=4 * sp * WINDOW * rows * 2 * 384,
+            flops=4 * count * WINDOW * rows * 2 * 384,
             bytes_accessed=4 * 2**20,
             transcendentals=0,
         ),
@@ -582,18 +582,19 @@
     gain = output_norm_gain.reshape(1, VDIM)
     weights = [proj_diff, proj_win, over_core(proj_diff), over_core(proj_win)]
 
-    def spread(ys):
-        return [ys[0]] + [over_z(ys[k], k) for k in range(1, sp)]
-
-    def attend(flip):
-        return attention(place, scalars, gain, queries, kv_own, kv_oth, sp, nx, flip)
-
-    far_heads = spread(attend(1))
-    y_near = attend(0)
-    near_heads = spread(y_near)
+    def attend(flip, first, count):
+        return attention(
+            place, scalars, gain, queries, kv_own, kv_oth, nx, flip, first, count
+        )
+
+    high = [over_z(y, k) for k, y in zip((2, 3), attend(1, 2, sp - 2))]
+    low = attend(1, 0, 2)
+    far_heads = [low[0], over_z(low[1], 1), *high]
+    y_near = attend(0, 0, sp)
+    near_heads = [y_near[0]] + [over_z(y_near[k], k) for k in range(1, sp)]
     received = []
     tiles = proj_diff.shape[1] // OUT_TILE
-    for begin, end in ((0, tiles // 2), (tiles // 2, tiles)):
+    for begin, end in ((0, 1), (1, tiles // 2), (tiles // 2, tiles)):
         part = output_projection(place, far_heads, weights, begin, end - begin, BF)
         received.append(over_x(part))
     kept = output_projection(place, near_heads, weights, 0, tiles, F32)

time: 264 us -> 262 us (level)
  waiting for transfers between devices: 147 us -> 141 us
    ppermute x36 -> x37, waiting for transfers between devices: 147 us -> 141 us  [send(): return lax.ppermute(value, AXES, pairs)]
    ppermute x36 -> x37, starting transfers between devices: 39.3 us -> 41.1 us  [send(): return lax.ppermute(value, AXES, pairs)]
    pallas_call x3 -> x4, Pallas kernels: 11.5 us -> 12.8 us  [output_projection(): pl.pallas_call(kernel, grid=(count,), in_specs=in_specs, out_specs=pl.Blo...]
    pallas_call x2 -> x3, Pallas kernels: 13.4 us -> 14 us  [attention(): pl.pallas_call(kernel, grid=(count // 2,), in_specs=[smem] * 5 + [pl.Bloc...]
  transfers between devices with their start and end apart: 36 -> 37, of which waited for: 16 -> 14; matrix products, arithmetic and copies ran while one was open for 8% -> 9% of each run, Pallas kernels for 16% -> 17%
where the time goes in v4:
time: 262 us; the launch traced here: 261 us
  waiting for transfers between devices  141 us (54%)
  Pallas kernels  46.6 us (18%)
  starting transfers between devices  41.1 us (16%)
  other arithmetic  18 us (7%)
  local copies, waits for them, and re-layouts  13.6 us (5%)
    ppermute x37, waiting for transfers between devices, send(): return lax.ppermute(value, AXES, pairs)  141 us
    ppermute x37, starting transfers between devices, send(): return lax.ppermute(value, AXES, pairs)  41.1 us
    pallas_call x3, Pallas kernels, attention(): pl.pallas_call(kernel, grid=(count // 2,), in_specs=[smem] * 5 + [pl.Bloc...  14 us
    pallas_call x4, Pallas kernels, output_projection(): pl.pallas_call(kernel, grid=(count,), in_specs=in_specs, out_specs=pl.Blo...  12.8 us
    pallas_call x3, Pallas kernels, project_sum(): pl.pallas_call(kernel, grid_spec=pltpu.PrefetchScalarGridSpec(num_scalar_...  11.4 us
    pallas_call x2, Pallas kernels, project_rest(): pl.pallas_call(kernel, grid_spec=pltpu.PrefetchScalarGridSpec(num_scalar_...  8.42 us
    unnamed x73, local copies, waits for them, and re-layouts  6.32 us
  transfers between devices with their start and end apart: 37, of which 14 were waited for; matrix products, arithmetic and copies ran while one was open for 9% of the time, Pallas kernels for 17%

profile of v4, /device:TPU:0, one launch (start us, length us, event | category | flops | bytes accessed | tf_op | source)
XLA Modules:
  0.0 261.2 jit_solution(7486957405121316737)
XLA Ops:
  1.7 3.0 %constant_dynamic-update-slice_fusion.5 = (bf16[768,4096]{1,0:T(8,128)(2,1)}, bf16[128,4096]{1,0:T(8,128)(2,1)}) fusion(f32[4096]{0:T(1024)} %param.13, f32[128]{0:T(128)S(1)} %add_rsqrt_fusion, bf16[128,4096]{1,0:T(8,128)(2,1)} %param.12), kind=kLoop, calls=%fused_computation.37 | loop fusion | flops 2097151 | bytes 3162624
  4.7 3.1 %collective-permute-start.2 = (bf16[128,4096]{1,0:T(8,128)(2,1)}, bf16[128,4096]{1,0:T(8,128)(2,1)}, u32[]{:S(2)}, u32[]{:S(2)}) collective-permute-start(bf16[128,4096]{1,0:T(8,128)(2,1)} %get-tuple-element.36), channel_id=1, source_target_pairs={{0,4},{1,5},{2,6},{3,7},{4,0},{5,1},{6,2},{7,3},{8,12},{9,13},{10,... | collective-permute-start | bytes 3145736 | tf_op jit(solution)/shard_map/ppermute | solution.py:497
  17.4 3.8 %collective-permute-start.9 = (bf16[1024,1024]{1,0:T(8,128)(2,1)}, bf16[1024,1024]{1,0:T(8,128)(2,1)}, u32[]{:S(2)}, u32[]{:S(2)}) collective-permute-start(bf16[1024,1024]{1,0:T(8,128)(2,1)} %pad_maximum_fusion.1), channel_id=1, source_target_pairs={{0,1},{2,3},{4,5},{6,7},{9,8},{11,10},{13,12},{15,14},{16,17},{18,... | collective-permute-start | bytes 6291464 | tf_op jit(solution)/shard_map/ppermute | solution.py:497
  21.2 2.0 dynamic-slice_bitcast_fusion.3
  34.9 18.5 %collective-permute-done.22.refs_0_ = bf16[256,768]{1,0:T(8,128)(2,1)S(1)} collective-permute-done((bf16[256,768]{1,0:T(8,128)(2,1)S(1)}, bf16[256,768]{1,0:T(8,128)(2,1)S(1)}, u32[]{:S(2)}, u32[]{:S(2)}) %collective-permute-start.22) | collective-permute-done | bytes 393248 | tf_op jit(solution)/shard_map/ppermute | solution.py:497
  55.0 7.3 %collective-permute-done.23.refs_1_ = bf16[256,768]{1,0:T(8,128)(2,1)S(1)} collective-permute-done((bf16[256,768]{1,0:T(8,128)(2,1)S(1)}, bf16[256,768]{1,0:T(8,128)(2,1)S(1)}, u32[]{:S(2)}, u32[]{:S(2)}) %collective-permute-start.23) | collective-permute-done | bytes 393248 | tf_op jit(solution)/shard_map/ppermute | solution.py:497
  63.2 2.4 collective-permute-start.14
  65.6 12.3 %collective-permute-done.5 = bf16[128,4096]{1,0:T(8,128)(2,1)S(1)} collective-permute-done((bf16[128,4096]{1,0:T(8,128)(2,1)}, bf16[128,4096]{1,0:T(8,128)(2,1)S(1)}, u32[]{:S(2)}, u32[]{:S(2)}) %collective-permute-start.5) | collective-permute-done | bytes 1048608 | tf_op jit(solution)/shard_map/ppermute | solution.py:497
  81.1 21.7 %collective-permute-done.11.refs_3_ = bf16[256,1280]{1,0:T(8,128)(2,1)S(1)} collective-permute-done((bf16[256,1280]{1,0:T(8,128)(2,1)S(1)}, bf16[256,1280]{1,0:T(8,128)(2,1)S(1)}, u32[]{:S(2)}, u32[]{:S(2)}) %collective-permute-start.11) | collective-permute-done | bytes 655392 | tf_op jit(solution)/shard_map/ppermute | solution.py:497
  107.4 13.1 %collective-permute-done.12.refs_4_ = bf16[256,1280]{1,0:T(8,128)(2,1)S(1)} collective-permute-done((bf16[256,1280]{1,0:T(8,128)(2,1)S(1)}, bf16[256,1280]{1,0:T(8,128)(2,1)S(1)}, u32[]{:S(2)}, u32[]{:S(2)}) %collective-permute-start.12) | collective-permute-done | bytes 655392 | tf_op jit(solution)/shard_map/ppermute | solution.py:497
  122.1 11.9 %collective-permute-done.15.refs_4_ = bf16[256,1280]{1,0:T(8,128)(2,1)S(1)} collective-permute-done((bf16[256,1280]{1,0:T(8,128)(2,1)S(1)}, bf16[256,1280]{1,0:T(8,128)(2,1)S(1)}, u32[]{:S(2)}, u32[]{:S(2)}) %collective-permute-start.15) | collective-permute-done | bytes 655392 | tf_op jit(solution)/shard_map/ppermute | solution.py:497
  135.8 8.8 %collective-permute-done.8 = bf16[128,4096]{1,0:T(8,128)(2,1)S(1)} collective-permute-done((bf16[128,4096]{1,0:T(8,128)(2,1)S(1)}, bf16[128,4096]{1,0:T(8,128)(2,1)S(1)}, u32[]{:S(2)}, u32[]{:S(2)}) %collective-permute-start.8) | collective-permute-done | bytes 1048608 | tf_op jit(solution)/shard_map/ppermute | solution.py:497
  147.5 5.6 %project.5 = (f32[768,768]{1,0:T(8,128)S(1)}, f32[768,512]{1,0:T(8,128)S(1)}) custom-call(s32[4]{0:T(128)S(1)} %pad_add_fusion.place_ref.refs_0_, bf16[768,4096]{1,0:T(8,128)(2,1)S(1)} %constant_dynamic-update-slice_fusion.refs_0_.refs_2_.e2, bf16[1024,1280]{1,0:T(8,128)(2,1)S(1)} %pad_maximum_fusion.refs_1_, ...), custom_call_target="tpu_custom_call" | custom-call | flops 4026531840 | bytes 3932160 | tf_op jit(solution)/shard_map/project/pallas_call | solution.py:335
  153.2 3.5 %project.6 = (f32[768,768]{1,0:T(8,128)S(1)}, f32[768,512]{1,0:T(8,128)S(1)}) custom-call(s32[4]{0:T(128)S(1)} %pad_add_fusion.place_ref.refs_0_, f32[768,768]{1,0:T(8,128)S(1)} %get-tuple-element.19.refs_0_, f32[768,512]{1,0:T(8,128)S(1)} %get-tuple-element.20.refs_1_, bf16[768,4096]{1,0:T(8,128)(2,1)S(1)} %constant_dynamic-update-slice_fusion.refs_0_.refs_2_.e2, ...), custom_call_target="tpu_custom_call" | custom-call | flops 2013265920 | bytes 3932160 | tf_op jit(solution)/shard_map/project/pallas_call | solution.py:335
  156.8 11.4 %collective-permute-done.18 = bf16[128,4096]{1,0:T(8,128)(2,1)} collective-permute-done((bf16[128,4096]{1,0:T(8,128)(2,1)}, bf16[128,4096]{1,0:T(8,128)(2,1)}, u32[]{:S(2)}, u32[]{:S(2)}) %collective-permute-start.18) | collective-permute-done | bytes 1048608 | tf_op jit(solution)/shard_map/ppermute | solution.py:497
  169.9 2.3 project.7
  174.0 5.0 %project.9.refs_7_ = bf16[1024,768]{1,0:T(8,128)(2,1)S(1)} custom-call(s32[4]{0:T(128)S(1)} %pad_add_fusion.place_ref.refs_0_, f32[768,768]{1,0:T(8,128)S(1)} %copy-done.15, f32[256,768]{1,0:T(8,128)S(1)} %get-tuple-element.24.acc_l, bf16[768,4096]{1,0:T(8,128)(2,1)S(1)} %constant_dynamic-update-slice_fusion.refs_0_.refs_2_.e2, ...), custom_call_target="tpu_custom_call" | custom-call | flops 2415919104 | bytes 8388608 | tf_op jit(solution)/shard_map/project/pallas_call | solution.py:400
  179.2 15.1 %collective-permute-done.19.refs_0_ = bf16[256,512]{1,0:T(8,128)(2,1)S(1)} collective-permute-done((bf16[256,512]{1,0:T(8,128)(2,1)S(1)}, bf16[256,512]{1,0:T(8,128)(2,1)S(1)}, u32[]{:S(2)}, u32[]{:S(2)}) %collective-permute-start.19) | collective-permute-done | bytes 262176 | tf_op jit(solution)/shard_map/ppermute | solution.py:497
  195.8 6.8 %collective-permute-done.20.refs_1_ = bf16[256,512]{1,0:T(8,128)(2,1)S(1)} collective-permute-done((bf16[256,512]{1,0:T(8,128)(2,1)S(1)}, bf16[256,512]{1,0:T(8,128)(2,1)S(1)}, u32[]{:S(2)}, u32[]{:S(2)}) %collective-permute-start.20) | collective-permute-done | bytes 262176 | tf_op jit(solution)/shard_map/ppermute | solution.py:497
  204.7 3.4 %project.8.refs_6_ = bf16[1024,512]{1,0:T(8,128)(2,1)S(1)} custom-call(s32[4]{0:T(128)S(1)} %pad_add_fusion.place_ref.refs_0_, f32[768,512]{1,0:T(8,128)S(1)} %copy-done.17, f32[256,512]{1,0:T(8,128)S(1)} %get-tuple-element.22.acc_l, bf16[768,4096]{1,0:T(8,128)(2,1)S(1)} %constant_dynamic-update-slice_fusion.refs_0_.refs_2_.e2, ...), custom_call_target="tpu_custom_call" | custom-call | flops 1610612736 | bytes 8388608 | tf_op jit(solution)/shard_map/project/pallas_call | solution.py:400
  208.2 3.6 %attend.4 = (bf16[128,512]{1,0:T(8,128)(2,1)S(1)}, bf16[128,512]{1,0:T(8,128)(2,1)S(1)}) custom-call(s32[4]{0:T(128)S(1)} %pad_add_fusion.place_ref.refs_0_, f32[2]{0:T(128)S(1)} %copy-done.19, f32[2]{0:T(128)S(1)} %collective-permute-done.refs_2_, f32[4]{0:T(128)S(1)} %copy-done.20, f32[4]{0:T(128)S(1)} %collective-permute-done.1.refs_4_, ...), custom_call_target="tpu_custom_call" | custom-call | flops 805306368 | bytes 4194304 | tf_op jit(solution)/shard_map/attend/pallas_call | solution.py:261
  211.9 3.6 %attend.5 = (bf16[128,512]{1,0:T(8,128)(2,1)S(1)}, bf16[128,512]{1,0:T(8,128)(2,1)S(1)}) custom-call(s32[4]{0:T(128)S(1)} %pad_add_fusion.place_ref.refs_0_, f32[2]{0:T(128)S(1)} %copy-done.19, f32[2]{0:T(128)S(1)} %collective-permute-done.refs_2_, f32[4]{0:T(128)S(1)} %copy-done.20, f32[4]{0:T(128)S(1)} %collective-permute-done.1.refs_4_, ...), custom_call_target="tpu_custom_call" | custom-call | flops 805306368 | bytes 4194304 | tf_op jit(solution)/shard_map/attend/pallas_call | solution.py:261
  217.3 2.6 %collective-permute-start.33 = (bf16[128,512]{1,0:T(8,128)(2,1)S(1)}, bf16[128,512]{1,0:T(8,128)(2,1)S(1)}, u32[]{:S(2)}, u32[]{:S(2)}) collective-permute-start(bf16[128,512]{1,0:T(8,128)(2,1)S(1)} %get-tuple-element.32), channel_id=1, source_target_pairs={{0,12},{1,13},{2,14},{3,15},{4,8},{5,9},{6,10},{7,11},{8,4},{9,5},... | collective-permute-start | bytes 393224 | tf_op jit(solution)/shard_map/ppermute | solution.py:497
  219.9 8.5 %collective-permute-done.32.refs_2_ = bf16[128,512]{1,0:T(8,128)(2,1)S(1)} collective-permute-done((bf16[128,512]{1,0:T(8,128)(2,1)S(1)}, bf16[128,512]{1,0:T(8,128)(2,1)S(1)}, u32[]{:S(2)}, u32[]{:S(2)}) %collective-permute-start.32) | collective-permute-done | bytes 131104 | tf_op jit(solution)/shard_map/ppermute | solution.py:497
  228.4 3.0 %output.7 = bf16[128,2048]{1,0:T(8,128)(2,1)S(1)} custom-call(s32[4]{0:T(128)S(1)} %pad_add_fusion.place_ref.refs_0_, bf16[128,512]{1,0:T(8,128)(2,1)S(1)} %get-tuple-element.29.refs_0_, bf16[128,512]{1,0:T(8,128)(2,1)S(1)} %collective-permute-done.31.refs_1_, bf16[128,512]{1,0:T(8,128)(2,1)S(1)} %collective-permute-done.32.refs_2_, ...), custom_call_target="tpu_custom_call" | custom-call | flops 1073741824 | bytes 8388608 | tf_op jit(solution)/shard_map/output/pallas_call | solution.py:452
  233.0 6.8 %attend.3 = (bf16[128,512]{1,0:T(8,128)(2,1)S(1)}, bf16[128,512]{1,0:T(8,128)(2,1)S(1)}, bf16[128,512]{1,0:T(8,128)(2,1)S(1)}, bf16[128,512]{1,0:T(8,128)(2,1)S(1)}) custom-call(s32[4]{0:T(128)S(1)} %pad_add_fusion.place_ref.refs_0_, f32[2]{0:T(128)S(1)} %copy-done.19, f32[2]{0:T(128)S(1)} %collective-permute-done.refs_2_, f32[4]{0:T(128)S(1)} %copy-done.20, ...), custom_call_target="tpu_custom_call" | custom-call | flops 1610612736 | bytes 4194304 | tf_op jit(solution)/shard_map/attend/pallas_call | solution.py:261
  239.8 2.8 %collective-permute-start.26 = (bf16[128,512]{1,0:T(8,128)(2,1)S(1)}, bf16[128,512]{1,0:T(8,128)(2,1)S(1)}, u32[]{:S(2)}, u32[]{:S(2)}) collective-permute-start(bf16[128,512]{1,0:T(8,128)(2,1)S(1)} %get-tuple-element.26), channel_id=1, source_target_pairs={{0,4},{1,5},{2,6},{3,7},{4,0},{5,1},{6,2},{7,3},{8,12},{9,13},{10,... | collective-permute-start | bytes 393224 | tf_op jit(solution)/shard_map/ppermute | solution.py:497
  242.7 2.4 collective-permute-start.28
  245.0 2.2 output.6
  247.8 2.1 output.5
  251.5 2.9 %collective-permute-done.27.refs_2_ = bf16[128,512]{1,0:T(8,128)(2,1)S(1)} collective-permute-done((bf16[128,512]{1,0:T(8,128)(2,1)S(1)}, bf16[128,512]{1,0:T(8,128)(2,1)S(1)}, u32[]{:S(2)}, u32[]{:S(2)}) %collective-permute-start.27) | collective-permute-done | bytes 131104 | tf_op jit(solution)/shard_map/ppermute | solution.py:497
  254.4 5.5 %output.4 = f32[128,4096]{1,0:T(8,128)S(1)} custom-call(s32[4]{0:T(128)S(1)} %pad_add_fusion.place_ref.refs_0_, bf16[128,512]{1,0:T(8,128)(2,1)S(1)} %get-tuple-element.25.refs_0_, bf16[128,512]{1,0:T(8,128)(2,1)S(1)} %collective-permute-done.26.refs_1_, bf16[128,512]{1,0:T(8,128)(2,1)S(1)} %collective-permute-done.27.refs_2_, ...), custom_call_target="tpu_custom_call" | custom-call | flops 2147483648 | bytes 16777216 | tf_op jit(solution)/shard_map/output/pallas_call | solution.py:452
  (164 shorter events, 53.4 us)
Async XLA Ops:
  4.7 26.5 %collective-permute-start.2 = (bf16[128,4096]{1,0:T(8,128)(2,1)}, bf16[128,4096]{1,0:T(8,128)(2,1)}, u32[]{:S(2)}, u32[]{:S(2)}) collective-permute-start(bf16[128,4096]{1,0:T(8,128)(2,1)} %get-tuple-element.36), channel_id=1, source_target_pairs={{0,4},{1,5},{2,6},{3,7},{4,0},{5,1},{6,2},{7,3},{8,12},{9,13},{10,... | collective-permute-start | bytes 3145736 | tf_op jit(solution)/shard_map/ppermute | solution.py:497
  7.8 24.3 %collective-permute-start.4 = (bf16[128,4096]{1,0:T(8,128)(2,1)}, bf16[128,4096]{1,0:T(8,128)(2,1)}, u32[]{:S(2)}, u32[]{:S(2)}) collective-permute-start(bf16[128,4096]{1,0:T(8,128)(2,1)} %get-tuple-element.36), channel_id=1, source_target_pairs={{4,8},{5,9},{6,10},{7,11},{8,4},{9,5},{10,6},{11,7},{20,24},{21,25... | collective-permute-start | bytes 3145736 | tf_op jit(solution)/shard_map/ppermute | solution.py:497
  9.4 70.2 %collective-permute-start.6 = (bf16[128,4096]{1,0:T(8,128)(2,1)}, bf16[128,4096]{1,0:T(8,128)(2,1)}, u32[]{:S(2)}, u32[]{:S(2)}) collective-permute-start(bf16[128,4096]{1,0:T(8,128)(2,1)} %get-tuple-element.36), channel_id=1, source_target_pairs={{0,2},{1,3},{2,0},{3,1},{4,6},{5,7},{6,4},{7,5},{8,10},{9,11},{10,... | collective-permute-start | bytes 3145736 | tf_op jit(solution)/shard_map/ppermute | solution.py:497
  14.4 12.4 %collective-permute-start.10 = (bf16[2,256,1024]{2,1,0:T(8,128)(2,1)}, bf16[2,256,1024]{2,1,0:T(8,128)(2,1)}, u32[]{:S(2)}, u32[]{:S(2)}) collective-permute-start(bf16[2,256,1024]{2,1,0:T(8,128)(2,1)} %pad_maximum_fusion.6), channel_id=1, source_target_pairs={{0,1},{1,0},{2,3},{3,2},{4,5},{5,4},{6,7},{7,6},{8,9},{9,8},{10,11... | collective-permute-start | bytes 3145736 | tf_op jit(solution)/shard_map/ppermute | solution.py:497
  17.4 87.6 %collective-permute-start.9 = (bf16[1024,1024]{1,0:T(8,128)(2,1)}, bf16[1024,1024]{1,0:T(8,128)(2,1)}, u32[]{:S(2)}, u32[]{:S(2)}) collective-permute-start(bf16[1024,1024]{1,0:T(8,128)(2,1)} %pad_maximum_fusion.1), channel_id=1, source_target_pairs={{0,1},{2,3},{4,5},{6,7},{9,8},{11,10},{13,12},{15,14},{16,17},{18,... | collective-permute-start | bytes 6291464 | tf_op jit(solution)/shard_map/ppermute | solution.py:497
  29.3 24.1 %collective-permute-start.22 = (bf16[256,768]{1,0:T(8,128)(2,1)S(1)}, bf16[256,768]{1,0:T(8,128)(2,1)S(1)}, u32[]{:S(2)}, u32[]{:S(2)}) collective-permute-start(bf16[256,768]{1,0:T(8,128)(2,1)S(1)} %pad_maximum_fusion.11), channel_id=1, source_target_pairs={{0,8},{1,9},{2,10},{3,11},{4,12},{5,13},{6,14},{7,15},{8,0},{9,1},... | collective-permute-start | bytes 1179656 | tf_op jit(solution)/shard_map/ppermute | solution.py:497
  31.3 31.9 %collective-permute-start.3 = (bf16[128,4096]{1,0:T(8,128)(2,1)}, bf16[128,4096]{1,0:T(8,128)(2,1)S(1)}, u32[]{:S(2)}, u32[]{:S(2)}) collective-permute-start(bf16[128,4096]{1,0:T(8,128)(2,1)} %collective-permute-done.2), channel_id=1, source_target_pairs={{4,8},{5,9},{6,10},{7,11},{8,4},{9,5},{10,6},{11,7},{20,24},{21,25... | collective-permute-start | bytes 3145736 | tf_op jit(solution)/shard_map/ppermute | solution.py:497
  32.1 45.8 %collective-permute-start.5 = (bf16[128,4096]{1,0:T(8,128)(2,1)}, bf16[128,4096]{1,0:T(8,128)(2,1)S(1)}, u32[]{:S(2)}, u32[]{:S(2)}) collective-permute-start(bf16[128,4096]{1,0:T(8,128)(2,1)} %collective-permute-done.4), channel_id=1, source_target_pairs={{4,0},{5,1},{6,2},{7,3},{8,12},{9,13},{10,14},{11,15},{20,16},{21,... | collective-permute-start | bytes 3145736 | tf_op jit(solution)/shard_map/ppermute | solution.py:497
  53.4 8.9 %collective-permute-start.23 = (bf16[256,768]{1,0:T(8,128)(2,1)S(1)}, bf16[256,768]{1,0:T(8,128)(2,1)S(1)}, u32[]{:S(2)}, u32[]{:S(2)}) collective-permute-start(bf16[256,768]{1,0:T(8,128)(2,1)S(1)} %collective-permute-done.22.refs_0_), channel_id=1, source_target_pairs={{0,16},{1,17},{2,18},{3,19},{4,20},{5,21},{6,22},{7,23},{8,24},{9,... | collective-permute-start | bytes 1179656 | tf_op jit(solution)/shard_map/ppermute | solution.py:497
  62.3 40.5 %collective-permute-start.11 = (bf16[256,1280]{1,0:T(8,128)(2,1)S(1)}, bf16[256,1280]{1,0:T(8,128)(2,1)S(1)}, u32[]{:S(2)}, u32[]{:S(2)}) collective-permute-start(bf16[256,1280]{1,0:T(8,128)(2,1)S(1)} %pad_maximum_fusion.8), channel_id=1, source_target_pairs={{0,4},{1,5},{2,6},{3,7},{4,0},{5,1},{6,2},{7,3},{8,12},{9,13},{10,... | collective-permute-start | bytes 1966088 | tf_op jit(solution)/shard_map/ppermute | solution.py:497
  63.2 39.6 %collective-permute-start.14 = (bf16[256,1280]{1,0:T(8,128)(2,1)S(1)}, bf16[256,1280]{1,0:T(8,128)(2,1)S(1)}, u32[]{:S(2)}, u32[]{:S(2)}) collective-permute-start(bf16[256,1280]{1,0:T(8,128)(2,1)S(1)} %pad_maximum_fusion.9), channel_id=1, source_target_pairs={{0,12},{1,13},{2,14},{3,15},{4,8},{5,9},{6,10},{7,11},{8,4},{9,5},... | collective-permute-start | bytes 1966088 | tf_op jit(solution)/shard_map/ppermute | solution.py:497
  77.9 26.5 %collective-permute-start.7 = (bf16[128,4096]{1,0:T(8,128)(2,1)}, bf16[128,4096]{1,0:T(8,128)(2,1)S(1)}, u32[]{:S(2)}, u32[]{:S(2)}) collective-permute-start(bf16[128,4096]{1,0:T(8,128)(2,1)} %collective-permute-done.2), channel_id=1, source_target_pairs={{0,2},{1,3},{2,0},{3,1},{4,6},{5,7},{6,4},{7,5},{8,10},{9,11},{10,... | collective-permute-start | bytes 3145736 | tf_op jit(solution)/shard_map/ppermute | solution.py:497
  79.6 140.3 %collective-permute-start.29 = (bf16[512,4096]{1,0:T(8,128)(2,1)S(1)}, bf16[512,4096]{1,0:T(8,128)(2,1)S(1)}, u32[]{:S(2)}, u32[]{:S(2)}) collective-permute-start(bf16[512,4096]{1,0:T(8,128)(2,1)S(1)} %copy-done), channel_id=1, source_target_pairs={{0,1},{1,0},{2,3},{3,2},{4,5},{5,4},{6,7},{7,6},{8,9},{9,8},{10,11... | collective-permute-start | bytes 12582920 | tf_op jit(solution)/shard_map/ppermute | solution.py:497
  102.8 117.2 %collective-permute-start.30 = (bf16[512,4096]{1,0:T(8,128)(2,1)S(1)}, bf16[512,4096]{1,0:T(8,128)(2,1)}, u32[]{:S(2)}, u32[]{:S(2)}) collective-permute-start(bf16[512,4096]{1,0:T(8,128)(2,1)S(1)} %copy-done.1), channel_id=1, source_target_pairs={{0,1},{1,0},{2,3},{3,2},{4,5},{5,4},{6,7},{7,6},{8,9},{9,8},{10,11... | collective-permute-start | bytes 12582920 | tf_op jit(solution)/shard_map/ppermute | solution.py:497
  102.8 17.7 %collective-permute-start.12 = (bf16[256,1280]{1,0:T(8,128)(2,1)S(1)}, bf16[256,1280]{1,0:T(8,128)(2,1)S(1)}, u32[]{:S(2)}, u32[]{:S(2)}) collective-permute-start(bf16[256,1280]{1,0:T(8,128)(2,1)S(1)} %collective-permute-done.11.refs_3_), channel_id=1, source_target_pairs={{0,16},{1,17},{2,18},{3,19},{4,20},{5,21},{6,22},{7,23},{8,24},{9,... | collective-permute-start | bytes 1966088 | tf_op jit(solution)/shard_map/ppermute | solution.py:497
  104.4 29.6 %collective-permute-start.15 = (bf16[256,1280]{1,0:T(8,128)(2,1)S(1)}, bf16[256,1280]{1,0:T(8,128)(2,1)S(1)}, u32[]{:S(2)}, u32[]{:S(2)}) collective-permute-start(bf16[256,1280]{1,0:T(8,128)(2,1)S(1)} %collective-permute-done.14.refs_3_), channel_id=1, source_target_pairs={{0,16},{1,17},{2,18},{3,19},{4,20},{5,21},{6,22},{7,23},{8,24},{9,... | collective-permute-start | bytes 1966088 | tf_op jit(solution)/shard_map/ppermute | solution.py:497
  105.0 29.1 %collective-permute-start.17 = (bf16[128,4096]{1,0:T(8,128)(2,1)S(1)}, bf16[128,4096]{1,0:T(8,128)(2,1)S(1)}, u32[]{:S(2)}, u32[]{:S(2)}) collective-permute-start(bf16[128,4096]{1,0:T(8,128)(2,1)S(1)} %collective-permute-done.3), channel_id=1, source_target_pairs={{4,0},{5,1},{6,2},{7,3},{8,12},{9,13},{10,14},{11,15},{20,16},{21,... | collective-permute-start | bytes 3145736 | tf_op jit(solution)/shard_map/ppermute | solution.py:497
  120.5 24.1 %collective-permute-start.8 = (bf16[128,4096]{1,0:T(8,128)(2,1)S(1)}, bf16[128,4096]{1,0:T(8,128)(2,1)S(1)}, u32[]{:S(2)}, u32[]{:S(2)}) collective-permute-start(bf16[128,4096]{1,0:T(8,128)(2,1)S(1)} %get-tuple-element.34), channel_id=1, source_target_pairs={{0,2},{1,3},{2,0},{3,1},{4,6},{5,7},{6,4},{7,5},{8,10},{9,11},{10,... | collective-permute-start | bytes 3145736 | tf_op jit(solution)/shard_map/ppermute | solution.py:497
  134.0 13.4 %collective-permute-start.13 = (bf16[512,1280]{1,0:T(8,128)(2,1)S(1)}, bf16[512,1280]{1,0:T(8,128)(2,1)S(1)}, u32[]{:S(2)}, u32[]{:S(2)}) collective-permute-start(bf16[512,1280]{1,0:T(8,128)(2,1)S(1)} %pad_maximum_fusion.4), channel_id=1, source_target_pairs={{0,1},{1,0},{2,3},{3,2},{4,5},{5,4},{6,7},{7,6},{8,9},{9,8},{10,11... | collective-permute-start | bytes 3932168 | tf_op jit(solution)/shard_map/ppermute | solution.py:497
  134.1 19.1 %collective-permute-start.16 = (bf16[512,1280]{1,0:T(8,128)(2,1)S(1)}, bf16[512,1280]{1,0:T(8,128)(2,1)S(1)}, u32[]{:S(2)}, u32[]{:S(2)}) collective-permute-start(bf16[512,1280]{1,0:T(8,128)(2,1)S(1)} %pad_maximum_fusion.5), channel_id=1, source_target_pairs={{0,1},{1,0},{2,3},{3,2},{4,5},{5,4},{6,7},{7,6},{8,9},{9,8},{10,11... | collective-permute-start | bytes 3932168 | tf_op jit(solution)/shard_map/ppermute | solution.py:497
  144.6 23.5 %collective-permute-start.18 = (bf16[128,4096]{1,0:T(8,128)(2,1)}, bf16[128,4096]{1,0:T(8,128)(2,1)}, u32[]{:S(2)}, u32[]{:S(2)}) collective-permute-start(bf16[128,4096]{1,0:T(8,128)(2,1)} %broadcast_select_fusion.1), channel_id=1, source_target_pairs={{0,2},{1,3},{2,0},{3,1},{4,6},{5,7},{6,4},{7,5},{8,10},{9,11},{10,... | collective-permute-start | bytes 3145736 | tf_op jit(solution)/shard_map/ppermute | solution.py:497
  147.4 24.9 %collective-permute-start.24 = (bf16[512,768]{1,0:T(8,128)(2,1)}, bf16[512,768]{1,0:T(8,128)(2,1)}, u32[]{:S(2)}, u32[]{:S(2)}) collective-permute-start(bf16[512,768]{1,0:T(8,128)(2,1)} %pad_maximum_fusion.7), channel_id=1, source_target_pairs={{0,1},{1,0},{2,3},{3,2},{4,5},{5,4},{6,7},{7,6},{8,9},{9,8},{10,11... | collective-permute-start | bytes 2359304 | tf_op jit(solution)/shard_map/ppermute | solution.py:497
  179.0 29.2 %collective-permute-start.25 = (bf16[1024,768]{1,0:T(8,128)(2,1)S(1)}, bf16[1024,768]{1,0:T(8,128)(2,1)S(1)}, u32[]{:S(2)}, u32[]{:S(2)}) collective-permute-start(bf16[1024,768]{1,0:T(8,128)(2,1)S(1)} %project.9.refs_7_), channel_id=1, source_target_pairs={{0,1},{1,0},{2,3},{3,2},{4,5},{5,4},{6,7},{7,6},{8,9},{9,8},{10,11... | collective-permute-start | bytes 4718600 | tf_op jit(solution)/shard_map/ppermute | solution.py:497
  179.1 15.2 %collective-permute-start.19 = (bf16[256,512]{1,0:T(8,128)(2,1)S(1)}, bf16[256,512]{1,0:T(8,128)(2,1)S(1)}, u32[]{:S(2)}, u32[]{:S(2)}) collective-permute-start(bf16[256,512]{1,0:T(8,128)(2,1)S(1)} %copy-done.32), channel_id=1, source_target_pairs={{0,8},{1,9},{2,10},{3,11},{4,12},{5,13},{6,14},{7,15},{8,0},{9,1},... | collective-permute-start | bytes 786440 | tf_op jit(solution)/shard_map/ppermute | solution.py:497
  215.5 13.0 %collective-permute-start.32 = (bf16[128,512]{1,0:T(8,128)(2,1)S(1)}, bf16[128,512]{1,0:T(8,128)(2,1)S(1)}, u32[]{:S(2)}, u32[]{:S(2)}) collective-permute-start(bf16[128,512]{1,0:T(8,128)(2,1)S(1)} %get-tuple-element.31), channel_id=1, source_target_pairs={{0,8},{1,9},{2,10},{3,11},{4,12},{5,13},{6,14},{7,15},{8,0},{9,1},... | collective-permute-start | bytes 393224 | tf_op jit(solution)/shard_map/ppermute | solution.py:497
  217.3 11.2 %collective-permute-start.33 = (bf16[128,512]{1,0:T(8,128)(2,1)S(1)}, bf16[128,512]{1,0:T(8,128)(2,1)S(1)}, u32[]{:S(2)}, u32[]{:S(2)}) collective-permute-start(bf16[128,512]{1,0:T(8,128)(2,1)S(1)} %get-tuple-element.32), channel_id=1, source_target_pairs={{0,12},{1,13},{2,14},{3,15},{4,8},{5,9},{6,10},{7,11},{8,4},{9,5},... | collective-permute-start | bytes 393224 | tf_op jit(solution)/shard_map/ppermute | solution.py:497
  231.4 28.5 %collective-permute-start.36 = (bf16[128,2048]{1,0:T(8,128)(2,1)S(1)}, bf16[128,2048]{1,0:T(8,128)(2,1)S(1)}, u32[]{:S(2)}, u32[]{:S(2)}) collective-permute-start(bf16[128,2048]{1,0:T(8,128)(2,1)S(1)} %output.7), channel_id=1, source_target_pairs={{0,2},{1,3},{2,0},{3,1},{4,6},{5,7},{6,4},{7,5},{8,10},{9,11},{10,... | collective-permute-start | bytes 1572872 | tf_op jit(solution)/shard_map/ppermute | solution.py:497
  239.8 10.2 %collective-permute-start.26 = (bf16[128,512]{1,0:T(8,128)(2,1)S(1)}, bf16[128,512]{1,0:T(8,128)(2,1)S(1)}, u32[]{:S(2)}, u32[]{:S(2)}) collective-permute-start(bf16[128,512]{1,0:T(8,128)(2,1)S(1)} %get-tuple-element.26), channel_id=1, source_target_pairs={{0,4},{1,5},{2,6},{3,7},{4,0},{5,1},{6,2},{7,3},{8,12},{9,13},{10,... | collective-permute-start | bytes 393224 | tf_op jit(solution)/shard_map/ppermute | solution.py:497
  242.6 11.8 %collective-permute-start.27 = (bf16[128,512]{1,0:T(8,128)(2,1)S(1)}, bf16[128,512]{1,0:T(8,128)(2,1)S(1)}, u32[]{:S(2)}, u32[]{:S(2)}) collective-permute-start(bf16[128,512]{1,0:T(8,128)(2,1)S(1)} %get-tuple-element.27), channel_id=1, source_target_pairs={{0,8},{1,9},{2,10},{3,11},{4,12},{5,13},{6,14},{7,15},{8,0},{9,1},... | collective-permute-start | bytes 393224 | tf_op jit(solution)/shard_map/ppermute | solution.py:497
  242.7 11.8 %collective-permute-start.28 = (bf16[128,512]{1,0:T(8,128)(2,1)S(1)}, bf16[128,512]{1,0:T(8,128)(2,1)S(1)}, u32[]{:S(2)}, u32[]{:S(2)}) collective-permute-start(bf16[128,512]{1,0:T(8,128)(2,1)S(1)} %get-tuple-element.28), channel_id=1, source_target_pairs={{0,12},{1,13},{2,14},{3,15},{4,8},{5,9},{6,10},{7,11},{8,4},{9,5},... | collective-permute-start | bytes 393224 | tf_op jit(solution)/shard_map/ppermute | solution.py:497
  247.2 12.8 %collective-permute-start.35 = (bf16[128,1024]{1,0:T(8,128)(2,1)S(1)}, bf16[128,1024]{1,0:T(8,128)(2,1)S(1)}, u32[]{:S(2)}, u32[]{:S(2)}) collective-permute-start(bf16[128,1024]{1,0:T(8,128)(2,1)S(1)} %output.6), channel_id=1, source_target_pairs={{0,2},{1,3},{2,0},{3,1},{4,6},{5,7},{6,4},{7,5},{8,10},{9,11},{10,... | collective-permute-start | bytes 786440 | tf_op jit(solution)/shard_map/ppermute | solution.py:497
  250.0 10.0 %collective-permute-start.34 = (bf16[128,1024]{1,0:T(8,128)(2,1)S(1)}, bf16[128,1024]{1,0:T(8,128)(2,1)S(1)}, u32[]{:S(2)}, u32[]{:S(2)}) collective-permute-start(bf16[128,1024]{1,0:T(8,128)(2,1)S(1)} %output.5), channel_id=1, source_target_pairs={{0,2},{1,3},{2,0},{3,1},{4,6},{5,7},{6,4},{7,5},{8,10},{9,11},{10,... | collective-permute-start | bytes 786440 | tf_op jit(solution)/shard_map/ppermute | solution.py:497
  (40 other events, 577.3 us)
